TPU v7x, 256 devices: a 4x2x16 block of a 4x16x16 slice. The times are simulated.
256 devices in a mesh: grp: 2 (over y), sp: 32 (over z, core), tp: 4 (over x).
Axes of the slice: x: 4, y: 2, z: 16, core: 2. Of those that a mesh axis runs over, the one named last changes fastest.
The devices are a block of a 4x16x16 slice.
Arguments:
- residual: bfloat16 [32768, 2048], P(('grp', 'sp', 'tp')), parts along dimension 0, may hold values from -6 to 6
- state_input: bfloat16 [32768, 1024], P(('grp', 'sp'), 'tp'), parts along dimension 0, may hold values from -6 to 6
- gate_input: bfloat16 [32768, 2048], P(('grp', 'sp'), 'tp'), parts along dimension 0, may hold values from -6 to 6
- decay_real: float32 [64, 64], P('tp'), may hold values from -0.2 to 0, as said below
- frequency: float32 [64, 64], P('tp'), as said below
- log_step: float32 [64], P('tp'), as said below
- drive_real: float32 [64, 64, 16], P('tp'), may hold values from -1 to 1
- drive_imag: float32 [64, 64, 16], P('tp'), may hold values from -1 to 1
- read_real: float32 [64, 16, 64], P('tp'), may hold values from -0.75 to 0.75
- read_imag: float32 [64, 16, 64], P('tp'), may hold values from -0.75 to 0.75
- skip_gain: float32 [1024], P('tp'), may hold values from -4 to 4
- value_weight: bfloat16 [1024, 2048], P(None, 'tp'), may hold values from -0.1875 to 0.1875
- glu_weight: bfloat16 [1024, 2048], P(None, 'tp'), may hold values from -0.1875 to 0.1875
- mix_weight: bfloat16 [2048, 2048], P('tp'), may hold values from -0.125 to 0.125
- norm_gain: float32 [2048], replicated, may hold values from 0.1 to 1.9
- mlp_gate: bfloat16 [2048, 3072], P('sp', 'tp'), may hold values from -0.125 to 0.125
- mlp_up: bfloat16 [2048, 3072], P('sp', 'tp'), may hold values from -0.125 to 0.125
- mlp_down: bfloat16 [3072, 2048], P('tp', 'sp'), may hold values from -0.109375 to 0.109375
Outputs:
- result: bfloat16 [32768, 2048], P(('grp', 'sp', 'tp')), parts along dimension 0
There are 2 independent parts, one for each index of `grp`. A program takes and returns all parts, laid end to end along the dimension named above; an argument that names none is the same for every part. Nothing has to cross between parts.
Inputs may be any that keep to these rules, and one draw needn't show every extreme that they name: `decay_real`: negative in every entry. `frequency`: never zero: its magnitude times exp(log_step) of its group lies between 0.05 and 0.5. Every group's time step exp(log_step) is at most one.
All inputs are finite; a program needn't handle non-finite values.
Results may differ from a plain program's by a relative error of at most 0.012.
Values may be sent and summed in bfloat16 or wider, within the bound.
No kernel may reach another device: no remote copies, remote signals or barrier semaphores. Data moves between devices by JAX's collectives and lax.ppermute only.
A program may use at most 128 MiB of HBM per device.

v0:
```python
import jax
import jax.numpy as jnp
from jax import lax
from jax.experimental import pallas as pl
from jax.experimental.pallas import tpu as pltpu
from jax.sharding import PartitionSpec as P

EPSILON = 1e-06
SEGMENTS = 8
LANES = 128
F32 = jnp.float32
BF16 = jnp.bfloat16
NT = (((1,), (1,)), ((), ()))


def times(a, b):
    return a[0] * b[0] - a[1] * b[1], a[0] * b[1] + a[1] * b[0]


def plus(a, b):
    return a[0] + b[0], a[1] + b[1]


def squared(a, count):
    for _ in range(count):
        a = times(a, a)
    return a


def iota(shape, dim):
    return lax.broadcasted_iota(jnp.int32, shape, dim)


def bits(size):
    assert size & (size - 1) == 0
    return size.bit_length() - 1


def along_lanes(x, count):
    while x.shape[1] % 128 and count > 1:
        x, count = jnp.concatenate([x, x], axis=1), count // 2
    return jnp.concatenate([x] * count, axis=1) if count > 1 else x


def as_row(x):
    groups, states = x.shape
    wide = along_lanes(x, groups)
    own = iota(wide.shape, 1) >> bits(states) == iota(wide.shape, 0)
    return jnp.sum(jnp.where(own, wide, 0.0), axis=0, keepdims=True)


def rates(decay_ref, freq_ref, log_step_ref):
    decay, freq = decay_ref[...], freq_ref[...]
    groups = decay.shape[0]
    wide = jnp.broadcast_to(log_step_ref[...], (groups, groups))
    same = iota(wide.shape, 0) == iota(wide.shape, 1)
    step = jnp.exp(jnp.sum(jnp.where(same, wide, 0.0), axis=1, keepdims=True))
    size = jnp.exp(decay * step)
    x = freq * step
    q = x * x
    cos = 1.0 + q * (-1 / 2 + q * (1 / 24 + q * (-1 / 720 + q * (1 / 40320 - q / 3628800))))
    sin = x * (1.0 + q * (-1 / 6 + q * (1 / 120 + q * (-1 / 5040 + q / 362880))))
    bar = size * cos, size * sin
    modulus = decay * decay + freq * freq
    ratio = (
        ((bar[0] - 1.0) * decay + bar[1] * freq) / modulus,
        (bar[1] * decay - (bar[0] - 1.0) * freq) / modulus,
    )
    return (as_row(bar[0]), as_row(bar[1])), (as_row(ratio[0]), as_row(ratio[1]))


def fill_drive(x_ref, b_re_ref, b_im_ref, xf_ref, xp_ref, d_re_ref, d_im_ref):
    rows, chans = x_ref.shape
    states = b_re_ref.shape[1]
    flat = d_re_ref.shape[1]
    groups = flat // states
    length = rows // SEGMENTS
    for i in range(chans // LANES):
        at = slice(i * LANES, (i + 1) * LANES)
        xf_ref[i] = x_ref[:, at].astype(F32)

        def permute(j, _, i=i, at=at):
            to = pl.ds(pl.multiple_of(j * SEGMENTS, SEGMENTS), SEGMENTS)
            xp_ref[to, at] = xf_ref[i, pl.ds(j, SEGMENTS, stride=length), :]
            return 0

        lax.fori_loop(0, length, permute, 0, unroll=8)
    x = xp_ref[...].astype(BF16)
    shape = (chans, flat)
    own = iota(shape, 0) >> bits(chans // groups) == iota(shape, 1) >> bits(states)
    for b_ref, d_ref in ((b_re_ref, d_re_ref), (b_im_ref, d_im_ref)):
        wide = jnp.where(own, along_lanes(b_ref[...], groups), 0.0).astype(BF16)
        d_ref[...] = jnp.dot(x, wide, preferred_element_type=F32)


def wide_read(c_re_ref, c_im_ref, factor):
    chans, states = c_re_ref.shape
    flat = factor[0].shape[1]
    groups = flat // states
    width = chans // groups
    shape = (chans, flat)
    own = iota(shape, 0) >> bits(width) == iota(shape, 1) >> bits(states)
    c = along_lanes(c_re_ref[...], groups), along_lanes(c_im_ref[...], groups)
    re, im = times(c, factor)
    return jnp.concatenate(
        [jnp.where(own, re, 0.0).astype(BF16), jnp.where(own, -im, 0.0).astype(BF16)], axis=1
    )


def as_tile(row):
    return jnp.concatenate(
        [row[:, i : i + LANES] for i in range(0, row.shape[1], LANES)], axis=0
    )


def from_tile(tile):
    return jnp.concatenate([tile[i : i + 1, :] for i in range(tile.shape[0])], axis=1)


def ends_kernel(
    me_ref, decay_ref, freq_ref, log_step_ref, x_ref, b_re_ref, b_im_ref,
    gate_ref, up_ref, down_ref,
    end_ref, seg_ref, row_ref, weight_ref,
    xf_ref, xp_ref, d_re_ref, d_im_ref,
):
    rows, flat = d_re_ref.shape
    length = rows // SEGMENTS
    at = 0
    for ref in (gate_ref, up_ref, down_ref):
        weight_ref[:, at : at + ref.shape[1]] = ref[...]
        at += ref.shape[1]
    bar, ratio = rates(decay_ref, freq_ref, log_step_ref)
    fill_drive(x_ref, b_re_ref, b_im_ref, xf_ref, xp_ref, d_re_ref, d_im_ref)
    lam = tuple(jnp.broadcast_to(part, (SEGMENTS, flat)) for part in bar)

    def advance(j, state):
        at = pl.ds(pl.multiple_of(j * SEGMENTS, SEGMENTS), SEGMENTS)
        return plus(times(lam, state), (d_re_ref[at, :], d_im_ref[at, :]))

    zero = jnp.zeros((SEGMENTS, flat), F32)
    ends = lax.fori_loop(0, length, advance, (zero, zero), unroll=4)
    over = squared(bar, bits(length))
    carry = jnp.zeros((1, flat), F32), jnp.zeros((1, flat), F32)
    for s in range(SEGMENTS):
        seg_ref[0, s : s + 1, :], seg_ref[1, s : s + 1, :] = carry
        carry = plus(times(over, carry), tuple(part[s : s + 1, :] for part in ends))
    for i, part in enumerate((*bar, *ratio)):
        row_ref[i : i + 1, :] = part
    block = tuple(as_tile(part) for part in squared(over, bits(SEGMENTS)))
    state = tuple(as_tile(part) for part in carry)
    me = me_ref[0]
    for place in range(end_ref.shape[0]):
        later = place > me
        sent = jnp.concatenate(state, axis=0)
        end_ref[place] = jnp.where(later, sent, 0.0).astype(BF16)
        state = tuple(
            jnp.where(later, new, old) for new, old in zip(times(block, state), state)
        )


def local_kernel(
    row_ref, seg_ref, x_ref, b_re_ref, b_im_ref, c_re_ref, c_im_ref, skip_ref,
    y_ref, power_ref,
    xf_ref, xp_ref, d_re_ref, d_im_ref, s_ref, w_ref,
):
    rows, flat = d_re_ref.shape
    length = rows // SEGMENTS
    fill_drive(x_ref, b_re_ref, b_im_ref, xf_ref, xp_ref, d_re_ref, d_im_ref)
    bar = row_ref[0:1, :], row_ref[1:2, :]
    ratio = row_ref[2:3, :], row_ref[3:4, :]
    lam = tuple(jnp.broadcast_to(part, (SEGMENTS, flat)) for part in bar)

    def advance(j, state):
        at = pl.ds(pl.multiple_of(j * 2 * SEGMENTS, 2 * SEGMENTS), 2 * SEGMENTS)
        d_re, d_im = d_re_ref[at, :], d_im_ref[at, :]
        first = plus(times(lam, state), (d_re[:SEGMENTS], d_im[:SEGMENTS]))
        second = plus(times(lam, first), (d_re[SEGMENTS:], d_im[SEGMENTS:]))
        for i in (0, 1):
            both = jnp.concatenate([first[i], second[i]], axis=0)
            s_ref[at, i * flat : (i + 1) * flat] = both.astype(BF16)
        return second

    lax.fori_loop(0, length // 2, advance, (seg_ref[0], seg_ref[1]), unroll=2)
    over = squared(bar, bits(length))
    power = jnp.ones((1, flat), F32), jnp.zeros((1, flat), F32)
    for s in range(SEGMENTS):
        w_ref[0, s : s + 1, :], w_ref[1, s : s + 1, :] = power
        power = times(power, over)

    def raise_power(j, power):
        at = pl.ds(pl.multiple_of(j * 2 * SEGMENTS, 2 * SEGMENTS), 2 * SEGMENTS)
        first = times(lam, power)
        second = times(lam, first)
        for i in (0, 1):
            both = jnp.concatenate([first[i], second[i]], axis=0)
            power_ref[at, i * flat : (i + 1) * flat] = both.astype(BF16)
        return second

    lax.fori_loop(0, length // 2, raise_power, (w_ref[0], w_ref[1]), unroll=2)
    read = wide_read(c_re_ref, c_im_ref, ratio)
    out = lax.dot_general(s_ref[...], read, NT, preferred_element_type=F32)
    y_ref[...] = out + skip_ref[...] * xp_ref[...]


def finish_kernel(
    piece_ref, row_ref, c_re_ref, c_im_ref, y_ref, power_ref, out_ref, t_ref
):
    pieces = jnp.sum(piece_ref[...].astype(F32), axis=0)
    half = pieces.shape[0] // 2
    total = from_tile(pieces[:half]), from_tile(pieces[half:])
    ratio = row_ref[2:3, :], row_ref[3:4, :]
    read = wide_read(c_re_ref, c_im_ref, times(ratio, total))
    y = y_ref[...] + lax.dot_general(power_ref[...], read, NT, preferred_element_type=F32)
    y = jax.nn.gelu(y, approximate=True)
    length = y.shape[0] // SEGMENTS
    for i in range(y.shape[1] // LANES):
        at = slice(i * LANES, (i + 1) * LANES)
        for j in range(length):
            t_ref[i, pl.ds(j, SEGMENTS, stride=length), :] = y[
                j * SEGMENTS : (j + 1) * SEGMENTS, at
            ]
        out_ref[:, at] = t_ref[i].astype(BF16)


def shaped(*shape, dtype=F32):
    return jax.ShapeDtypeStruct(shape, dtype)


def activations(
    state_input, decay_real, frequency, log_step, drive_real, drive_imag,
    read_real, read_imag, skip_gain, weights,
):
    rows, chans = state_input.shape
    groups, states = decay_real.shape
    flat = groups * states
    peers = lax.axis_size("sp")
    me = lax.axis_index("sp").reshape(1)
    log_row = log_step.reshape(1, groups)
    b = [part.transpose(0, 2, 1).reshape(chans, states) for part in (drive_real, drive_imag)]
    c = [part.reshape(chans, states) for part in (read_real, read_imag)]
    skip = skip_gain.reshape(1, chans)
    drive_scratch = [
        pltpu.VMEM((chans // LANES, rows, LANES), F32),
        pltpu.VMEM((rows, chans), F32),
        pltpu.VMEM((rows, flat), F32),
        pltpu.VMEM((rows, flat), F32),
    ]
    whole = pl.BlockSpec(memory_space=pltpu.VMEM)
    end, seg, row, weight = pl.pallas_call(
        ends_kernel,
        out_shape=(
            shaped(peers, 2 * flat // LANES, LANES, dtype=BF16),
            shaped(2, SEGMENTS, flat),
            shaped(4, flat),
            shaped(weights[0].shape[0], sum(w.shape[1] for w in weights), dtype=BF16),
        ),
        in_specs=[pl.BlockSpec(memory_space=pltpu.SMEM), *[whole] * 9],
        scratch_shapes=drive_scratch,
        name="ssm_ends",
    )(me, decay_real, frequency, log_row, state_input, *b, *weights)
    weight = lax.all_gather(weight, "sp", axis=0, tiled=True)
    pieces = lax.all_to_all(end, "sp", 0, 0, tiled=True)
    local, power = pl.pallas_call(
        local_kernel,
        out_shape=(shaped(rows, chans), shaped(rows, 2 * flat, dtype=BF16)),
        scratch_shapes=[
            *drive_scratch,
            pltpu.VMEM((rows, 2 * flat), BF16),
            pltpu.VMEM((2, SEGMENTS, flat), F32),
        ],
        cost_estimate=pl.CostEstimate(
            flops=8 * rows * flat * chans, bytes_accessed=8 * rows * flat, transcendentals=0
        ),
        name="ssm_local",
    )(row, seg, state_input, *b, *c, skip)
    acts = pl.pallas_call(
        finish_kernel,
        out_shape=shaped(rows, chans, dtype=BF16),
        scratch_shapes=[pltpu.VMEM((chans // LANES, rows, LANES), F32)],
        name="ssm_finish",
    )(pieces, row, *c, local, power)
    return acts, weight


def ring(array, by):
    peers = lax.axis_size("tp")
    return lax.ppermute(array, "tp", [(i, (i + by) % peers) for i in range(peers)])


def rows_at(array, index, size):
    return lax.dynamic_slice_in_dim(array, index * size, size, 0)


def gathered(own):
    half = own.shape[0] // 2
    left = ring(own, 1)
    right = ring(own, -1)
    far_top = ring(left[:half], 1)
    far_low = ring(right[half:], -1)
    return own, left, right, jnp.concatenate([far_top, far_low], axis=0)


def summed(product, me, peers):
    far = product((me + 2) % peers).astype(BF16)
    half = far.shape[0] // 2
    from_left, from_right = ring(far[:half], 1), ring(far[half:], -1)
    right = product((me + 1) % peers)
    left = product((me + 3) % peers)
    right = right + jnp.pad(from_left, ((0, half), (0, 0))).astype(F32)
    left = left + jnp.pad(from_right, ((half, 0), (0, 0))).astype(F32)
    from_left, from_right = ring(right.astype(BF16), 1), ring(left.astype(BF16), -1)
    return product(me) + from_left.astype(F32) + from_right.astype(F32)


def shards(
    residual, state_input, gate_input, decay_real, frequency, log_step,
    drive_real, drive_imag, read_real, read_imag, skip_gain,
    value_weight, glu_weight, mix_weight, norm_gain, mlp_gate, mlp_up, mlp_down,
):
    peers, me = lax.axis_size("tp"), lax.axis_index("tp")
    assert peers == 4
    hidden_width = mlp_gate.shape[1]
    chans = state_input.shape[1]
    acts, weight = activations(
        state_input, decay_real, frequency, log_step, drive_real, drive_imag,
        read_real, read_imag, skip_gain, (mlp_gate, mlp_up, mlp_down.T),
    )
    both, down_weight = weight[:, : 2 * hidden_width], weight[:, 2 * hidden_width :]
    places = dict(zip((0, 3, 1, 2), (acts, ring(acts, 1), ring(acts, -1), ring(acts, 2))))

    def project(w):
        total = None
        for place, rows in places.items():
            part = jnp.dot(
                rows, rows_at(w, (me + place) % peers, chans), preferred_element_type=F32
            )
            total = part if total is None else total + part
        return total

    value, gated = project(value_weight), project(glu_weight)
    mixed = (jax.nn.sigmoid(gate_input.astype(F32)) * value * jax.nn.sigmoid(gated)).astype(BF16)

    owned = residual.shape[0]
    branch = summed(
        lambda q: jnp.dot(rows_at(mixed, q, owned), mix_weight, preferred_element_type=F32),
        me, peers,
    )
    inner = residual.astype(F32) + branch
    scale = lax.rsqrt(jnp.mean(inner * inner, axis=-1, keepdims=True) + EPSILON)
    normed = (inner * scale * norm_gain).astype(BF16)
    own, left, right, far = gathered(normed)

    def feed(rows):
        hidden = jnp.dot(rows, both, preferred_element_type=F32)
        hidden = (jax.nn.silu(hidden[:, :hidden_width]) * hidden[:, hidden_width:]).astype(BF16)
        return lax.dot_general(hidden, down_weight, NT, preferred_element_type=F32)

    near = feed(own)
    sides = feed(jnp.concatenate([left, right], axis=0))
    products = {0: near, 1: sides[owned:], 2: feed(far), 3: sides[:owned]}
    down = summed(lambda q: products[q], 0, peers)
    return (inner + 0.5 * down).astype(BF16)


def solution(mesh):
    placed = (
        P(("grp", "sp", "tp"), None),
        P(("grp", "sp"), "tp"),
        P(("grp", "sp"), "tp"),
        P("tp", None),
        P("tp", None),
        P("tp"),
        P("tp", None, None),
        P("tp", None, None),
        P("tp", None, None),
        P("tp", None, None),
        P("tp"),
        P(None, "tp"),
        P(None, "tp"),
        P("tp", None),
        P(),
        P("sp", "tp"),
        P("sp", "tp"),
        P("tp", "sp"),
    )

    return jax.shard_map(
        shards, mesh=mesh, in_specs=placed, out_specs=P(("grp", "sp", "tp"), None), check_vma=False
    )
```

profile of v0, /device:TPU:40, one launch (start us, length us, event | category | flops | bytes accessed | tf_op | source)
XLA Modules:
  0.0 160.7 jit_solution(15934179728281554544)
XLA Ops:
  6.6 4.4 %ssm_ends.1 = (bf16[32,16,128]{2,1,0:T(8,128)(2,1)}, f32[2,8,1024]{2,1,0:T(8,128)}, f32[4,1024]{1,0:T(4,128)}, bf16[64,2304]{1,0:T(8,128)(2,1)}) custom-call(s32[1]{0:T(128)} %bitcast.me_ref, f32[16,64]{1,0:T(8,128)} %decay_ref.1, f32[16,64]{1,0:T(8,128)} %freq_ref.1, f32[1,16]{1,0:T(1,128)} %bitcast.34, bf16[512,256]{1,0:T(8,128)(2,1)} %x_ref.3, ...), custom_call_target="tpu_custom_call" | custom-call | tf_op jit(solution)/shard_map/ssm_ends/pallas_call | solution.py:249
  11.0 24.8 %all-to-all-start = ((bf16[32,16,128]{2,1,0:T(8,128)(2,1)}), bf16[32,16,128]{2,1,0:T(8,128)(2,1)S(1)}, u32[]{:S(2)}, u32[]{:S(2)}) async-start(bf16[32,16,128]{2,1,0:T(8,128)(2,1)} %get-tuple-element.11), calls=%async_computation | async-start | bytes 262144 | tf_op jit(solution)/shard_map/all_to_all | solution.py:262
  35.9 6.2 %ssm_local.1 = (f32[512,256]{1,0:T(8,128)}, bf16[512,2048]{1,0:T(8,128)(2,1)}) custom-call(f32[4,1024]{1,0:T(4,128)} %get-tuple-element.12.row_ref, f32[2,8,1024]{2,1,0:T(8,128)} %get-tuple-element.13.seg_ref, bf16[512,256]{1,0:T(8,128)(2,1)} %x_ref.3, f32[256,64]{1,0:T(8,128)} %bitcast.26, f32[256,64]{1,0:T(8,128)} %bitcast.28, f32[256,64]{1,0:T(8,128)} %bitcast.29, ...), custom_call_target="tpu_custom_call" | custom-call | flops 1073741824 | bytes 4194304 | tf_op jit(solution)/shard_map/ssm_local/pallas_call | solution.py:263
  42.1 10.7 %all-to-all-done.piece_ref = bf16[32,16,128]{2,1,0:T(8,128)(2,1)S(1)} async-done(((bf16[32,16,128]{2,1,0:T(8,128)(2,1)}), bf16[32,16,128]{2,1,0:T(8,128)(2,1)S(1)}, u32[]{:S(2)}, u32[]{:S(2)}) %all-to-all-start) | async-done | bytes 131104 | tf_op jit(solution)/shard_map/all_to_all | solution.py:262
  53.4 4.0 %ssm_finish.1 = bf16[512,256]{1,0:T(8,128)(2,1)} custom-call(bf16[32,16,128]{2,1,0:T(8,128)(2,1)} %copy-done.3, f32[4,1024]{1,0:T(4,128)} %get-tuple-element.12.row_ref, f32[256,64]{1,0:T(8,128)} %bitcast.30, f32[256,64]{1,0:T(8,128)} %bitcast.32, f32[512,256]{1,0:T(8,128)} %get-tuple-element.14.y_ref, bf16[512,2048]{1,0:T(8,128)(2,1)} %get-tuple-element.15.power_ref), custom_call_target="tpu_custom_call" | custom-call | tf_op jit(solution)/shard_map/ssm_finish/pallas_call | solution.py:276
  57.4 3.4 %collective-permute-start.2 = (bf16[512,256]{1,0:T(8,128)(2,1)}, bf16[512,256]{1,0:T(8,128)(2,1)S(1)}, u32[]{:S(2)}, u32[]{:S(2)}) collective-permute-start(bf16[512,256]{1,0:T(8,128)(2,1)} %ssm_finish.1), channel_id=1, source_target_pairs={{0,2},{1,3},{2,0},{3,1},{4,6},{5,7},{6,4},{7,5},{8,10},{9,11},{10,... | collective-permute-start | bytes 786440 | tf_op jit(solution)/shard_map/ppermute | solution.py:287
  61.8 1.1 collective-permute-start
  62.9 1.3 fusion.37
  64.1 1.4 fusion.43
  65.5 6.3 %collective-permute-done = bf16[512,256]{1,0:T(8,128)(2,1)S(1)} collective-permute-done((bf16[512,256]{1,0:T(8,128)(2,1)}, bf16[512,256]{1,0:T(8,128)(2,1)S(1)}, u32[]{:S(2)}, u32[]{:S(2)}) %collective-permute-start) | collective-permute-done | bytes 262176 | tf_op jit(solution)/shard_map/ppermute | solution.py:287
  75.5 1.6 %collective-permute-start.5 = (bf16[64,2048]{1,0:T(8,128)(2,1)S(1)}, bf16[64,2048]{1,0:T(8,128)(2,1)S(1)}, u32[]{:S(2)}, u32[]{:S(2)}) collective-permute-start(bf16[64,2048]{1,0:T(8,128)(2,1)S(1)} %get-tuple-element.24), channel_id=1, source_target_pairs={{0,3},{1,0},{2,1},{3,2},{4,7},{5,4},{6,5},{7,6},{8,11},{9,8},{10,9... | collective-permute-start | bytes 786440 | tf_op jit(solution)/shard_map/ppermute | solution.py:287
  77.5 5.4 %collective-permute-done.5 = bf16[64,2048]{1,0:T(8,128)(2,1)S(1)} collective-permute-done((bf16[64,2048]{1,0:T(8,128)(2,1)S(1)}, bf16[64,2048]{1,0:T(8,128)(2,1)S(1)}, u32[]{:S(2)}, u32[]{:S(2)}) %collective-permute-start.5) | collective-permute-done | bytes 262176 | tf_op jit(solution)/shard_map/ppermute | solution.py:287
  83.4 3.8 %collective-permute-start.6 = (bf16[128,2048]{1,0:T(8,128)(2,1)S(1)}, bf16[128,2048]{1,0:T(8,128)(2,1)}, u32[]{:S(2)}, u32[]{:S(2)}) collective-permute-start(bf16[128,2048]{1,0:T(8,128)(2,1)S(1)} %add_convert_fusion.1), channel_id=1, source_target_pairs={{0,3},{1,0},{2,1},{3,2},{4,7},{5,4},{6,5},{7,6},{8,11},{9,8},{10,9... | collective-permute-start | bytes 1572872 | tf_op jit(solution)/shard_map/ppermute | solution.py:287
  87.2 1.2 add_convert_fusion.2
  88.9 9.0 %collective-permute-done.6 = bf16[128,2048]{1,0:T(8,128)(2,1)} collective-permute-done((bf16[128,2048]{1,0:T(8,128)(2,1)S(1)}, bf16[128,2048]{1,0:T(8,128)(2,1)}, u32[]{:S(2)}, u32[]{:S(2)}) %collective-permute-start.6) | collective-permute-done | bytes 524320 | tf_op jit(solution)/shard_map/ppermute | solution.py:287
  98.0 5.0 %collective-permute-done.4 = bf16[128,2048]{1,0:T(8,128)(2,1)} collective-permute-done((bf16[128,2048]{1,0:T(8,128)(2,1)}, bf16[128,2048]{1,0:T(8,128)(2,1)}, u32[]{:S(2)}, u32[]{:S(2)}) %collective-permute-start.4) | collective-permute-done | bytes 524320 | tf_op jit(solution)/shard_map/ppermute | solution.py:287
  102.9 1.6 multiply_reduce_fusion
  105.5 1.4 collective-permute-start.7
  106.9 10.0 %collective-permute-done.8 = bf16[128,2048]{1,0:T(8,128)(2,1)S(1)} collective-permute-done((bf16[128,2048]{1,0:T(8,128)(2,1)S(1)}, bf16[128,2048]{1,0:T(8,128)(2,1)S(1)}, u32[]{:S(2)}, u32[]{:S(2)}) %collective-permute-start.8) | collective-permute-done | bytes 524320 | tf_op jit(solution)/shard_map/ppermute | solution.py:287
  116.9 1.6 %collective-permute-start.10 = (bf16[64,2048]{1,0:T(8,128)(2,1)S(1)}, bf16[64,2048]{1,0:T(8,128)(2,1)S(1)}, u32[]{:S(2)}, u32[]{:S(2)}) collective-permute-start(bf16[64,2048]{1,0:T(8,128)(2,1)S(1)} %slice.74), channel_id=1, source_target_pairs={{0,3},{1,0},{2,1},{3,2},{4,7},{5,4},{6,5},{7,6},{8,11},{9,8},{10,9... | collective-permute-start | bytes 786440 | tf_op jit(solution)/shard_map/ppermute | solution.py:287
  119.2 4.2 %collective-permute-done.10 = bf16[64,2048]{1,0:T(8,128)(2,1)S(1)} collective-permute-done((bf16[64,2048]{1,0:T(8,128)(2,1)S(1)}, bf16[64,2048]{1,0:T(8,128)(2,1)S(1)}, u32[]{:S(2)}, u32[]{:S(2)}) %collective-permute-start.10) | collective-permute-done | bytes 262176 | tf_op jit(solution)/shard_map/ppermute | solution.py:287
  123.4 3.2 %collective-permute-done.9 = bf16[64,2048]{1,0:T(8,128)(2,1)} collective-permute-done((bf16[64,2048]{1,0:T(8,128)(2,1)S(1)}, bf16[64,2048]{1,0:T(8,128)(2,1)}, u32[]{:S(2)}, u32[]{:S(2)}) %collective-permute-start.9) | collective-permute-done | bytes 262176 | tf_op jit(solution)/shard_map/ppermute | solution.py:287
  126.6 4.0 %fusion = f32[128,1536]{1,0:T(8,128)S(1)} fusion(bf16[2048,2304]{1,0:T(8,128)(2,1)} %all-gather.2.cloned.1.call-done, bf16[64,2048]{1,0:T(8,128)(2,1)S(1)} %collective-permute-done.10, bf16[64,2048]{1,0:T(8,128)(2,1)} %collective-permute-done.9), kind=kOutput, calls=%fused_computation | convolution fusion | flops 806354944 | bytes 7602176 | tf_op jit(solution)/shard_map/dot_general | solution.py:354
  130.6 1.6 copy-done.12
  132.2 1.1 convolution_convert_fusion
  133.5 3.2 %collective-permute-start.13 = (bf16[64,2048]{1,0:T(8,128)(2,1)S(1)}, bf16[64,2048]{1,0:T(8,128)(2,1)S(1)}, u32[]{:S(2)}, u32[]{:S(2)}) collective-permute-start(bf16[64,2048]{1,0:T(8,128)(2,1)S(1)} %get-tuple-element.22), channel_id=1, source_target_pairs={{0,3},{1,0},{2,1},{3,2},{4,7},{5,4},{6,5},{7,6},{8,11},{9,8},{10,9... | collective-permute-start | bytes 786440 | tf_op jit(solution)/shard_map/ppermute | solution.py:287
  136.7 1.8 %fusion.2 = f32[256,1536]{1,0:T(8,128)S(1)} fusion(bf16[2048,2304]{1,0:T(8,128)(2,1)S(1)} %copy-done.12, bf16[128,2048]{1,0:T(8,128)(2,1)S(1)} %copy-done.8, bf16[128,2048]{1,0:T(8,128)(2,1)S(1)} %copy-done.10), kind=kOutput, calls=%fused_computation.2 | convolution fusion | flops 1612709888 | bytes 8912896 | tf_op jit(solution)/shard_map/dot_general | solution.py:354
  139.6 2.1 %collective-permute-done.11 = bf16[64,2048]{1,0:T(8,128)(2,1)S(1)} collective-permute-done((bf16[64,2048]{1,0:T(8,128)(2,1)S(1)}, bf16[64,2048]{1,0:T(8,128)(2,1)S(1)}, u32[]{:S(2)}, u32[]{:S(2)}) %collective-permute-start.11) | collective-permute-done | bytes 262176 | tf_op jit(solution)/shard_map/ppermute | solution.py:287
  142.2 3.5 %collective-permute-start.14 = (bf16[128,2048]{1,0:T(8,128)(2,1)S(1)}, bf16[128,2048]{1,0:T(8,128)(2,1)S(1)}, u32[]{:S(2)}, u32[]{:S(2)}) collective-permute-start(bf16[128,2048]{1,0:T(8,128)(2,1)S(1)} %get-tuple-element.20), channel_id=1, source_target_pairs={{0,3},{1,0},{2,1},{3,2},{4,7},{5,4},{6,5},{7,6},{8,11},{9,8},{10,9... | collective-permute-start | bytes 1572872 | tf_op jit(solution)/shard_map/ppermute | solution.py:287
  146.7 1.1 fusion.9
  147.8 4.9 %collective-permute-done.12 = bf16[128,2048]{1,0:T(8,128)(2,1)S(1)} collective-permute-done((bf16[128,2048]{1,0:T(8,128)(2,1)S(1)}, bf16[128,2048]{1,0:T(8,128)(2,1)S(1)}, u32[]{:S(2)}, u32[]{:S(2)}) %collective-permute-start.12) | collective-permute-done | bytes 524320 | tf_op jit(solution)/shard_map/ppermute | solution.py:287
  152.7 1.1 add_convert_fusion
  (61 shorter events, 10.9 us)
Async XLA Ops:
  6.5 67.7 %copy-start = (bf16[512,2048]{1,0:T(8,128)(2,1)S(1)}, bf16[512,2048]{1,0:T(8,128)(2,1)}, u32[]{:S(2)}) copy-start(bf16[512,2048]{1,0:T(8,128)(2,1)} %param.31) | copy-start | bytes 6291460
  6.6 120.0 %all-gather.2.cloned.1.call-start = ((), (), s32[]{:S(2)}) async-start(), calls=%async_computation.1 | async-start | bytes 9732096 | tf_op jit(solution)/shard_map/all_gather | solution.py:261
  11.0 41.7 %all-to-all-start = ((bf16[32,16,128]{2,1,0:T(8,128)(2,1)}), bf16[32,16,128]{2,1,0:T(8,128)(2,1)S(1)}, u32[]{:S(2)}, u32[]{:S(2)}) async-start(bf16[32,16,128]{2,1,0:T(8,128)(2,1)} %get-tuple-element.11), calls=%async_computation | async-start | bytes 262144 | tf_op jit(solution)/shard_map/all_to_all | solution.py:262
  35.8 27.0 %copy-start.1 = (bf16[1024,512]{1,0:T(8,128)(2,1)S(1)}, bf16[1024,512]{1,0:T(8,128)(2,1)}, u32[]{:S(2)}) copy-start(bf16[1024,512]{1,0:T(8,128)(2,1)} %param.30) | copy-start | bytes 3145732
  52.8 0.6 copy-start.3
  57.4 14.7 %copy-start.2 = (bf16[1024,512]{1,0:T(8,128)(2,1)S(1)}, bf16[1024,512]{1,0:T(8,128)(2,1)}, u32[]{:S(2)}) copy-start(bf16[1024,512]{1,0:T(8,128)(2,1)} %param.29) | copy-start | bytes 3145732
  57.4 15.0 %collective-permute-start.2 = (bf16[512,256]{1,0:T(8,128)(2,1)}, bf16[512,256]{1,0:T(8,128)(2,1)S(1)}, u32[]{:S(2)}, u32[]{:S(2)}) collective-permute-start(bf16[512,256]{1,0:T(8,128)(2,1)} %ssm_finish.1), channel_id=1, source_target_pairs={{0,2},{1,3},{2,0},{3,1},{4,6},{5,7},{6,4},{7,5},{8,10},{9,11},{10,... | collective-permute-start | bytes 786440 | tf_op jit(solution)/shard_map/ppermute | solution.py:287
  60.8 12.2 %collective-permute-start.1 = (bf16[512,256]{1,0:T(8,128)(2,1)}, bf16[512,256]{1,0:T(8,128)(2,1)S(1)}, u32[]{:S(2)}, u32[]{:S(2)}) collective-permute-start(bf16[512,256]{1,0:T(8,128)(2,1)} %ssm_finish.1), channel_id=1, source_target_pairs={{0,3},{1,0},{2,1},{3,2},{4,7},{5,4},{6,5},{7,6},{8,11},{9,8},{10,9... | collective-permute-start | bytes 786440 | tf_op jit(solution)/shard_map/ppermute | solution.py:287
  61.8 10.0 %collective-permute-start = (bf16[512,256]{1,0:T(8,128)(2,1)}, bf16[512,256]{1,0:T(8,128)(2,1)S(1)}, u32[]{:S(2)}, u32[]{:S(2)}) collective-permute-start(bf16[512,256]{1,0:T(8,128)(2,1)} %ssm_finish.1), channel_id=1, source_target_pairs={{0,1},{1,2},{2,3},{3,0},{4,5},{5,6},{6,7},{7,4},{8,9},{9,10},{10,1... | collective-permute-start | bytes 786440 | tf_op jit(solution)/shard_map/ppermute | solution.py:287
  72.7 1.1 copy-start.13
  75.5 7.5 %collective-permute-start.5 = (bf16[64,2048]{1,0:T(8,128)(2,1)S(1)}, bf16[64,2048]{1,0:T(8,128)(2,1)S(1)}, u32[]{:S(2)}, u32[]{:S(2)}) collective-permute-start(bf16[64,2048]{1,0:T(8,128)(2,1)S(1)} %get-tuple-element.24), channel_id=1, source_target_pairs={{0,3},{1,0},{2,1},{3,2},{4,7},{5,4},{6,5},{7,6},{8,11},{9,8},{10,9... | collective-permute-start | bytes 786440 | tf_op jit(solution)/shard_map/ppermute | solution.py:287
  77.1 10.1 %collective-permute-start.3 = (bf16[64,2048]{1,0:T(8,128)(2,1)}, bf16[64,2048]{1,0:T(8,128)(2,1)S(1)}, u32[]{:S(2)}, u32[]{:S(2)}) collective-permute-start(bf16[64,2048]{1,0:T(8,128)(2,1)} %get-tuple-element.23), channel_id=1, source_target_pairs={{0,1},{1,2},{2,3},{3,0},{4,5},{5,6},{6,7},{7,4},{8,9},{9,10},{10,1... | collective-permute-start | bytes 786440 | tf_op jit(solution)/shard_map/ppermute | solution.py:287
  83.4 14.5 %collective-permute-start.6 = (bf16[128,2048]{1,0:T(8,128)(2,1)S(1)}, bf16[128,2048]{1,0:T(8,128)(2,1)}, u32[]{:S(2)}, u32[]{:S(2)}) collective-permute-start(bf16[128,2048]{1,0:T(8,128)(2,1)S(1)} %add_convert_fusion.1), channel_id=1, source_target_pairs={{0,3},{1,0},{2,1},{3,2},{4,7},{5,4},{6,5},{7,6},{8,11},{9,8},{10,9... | collective-permute-start | bytes 1572872 | tf_op jit(solution)/shard_map/ppermute | solution.py:287
  88.5 14.5 %collective-permute-start.4 = (bf16[128,2048]{1,0:T(8,128)(2,1)}, bf16[128,2048]{1,0:T(8,128)(2,1)}, u32[]{:S(2)}, u32[]{:S(2)}) collective-permute-start(bf16[128,2048]{1,0:T(8,128)(2,1)} %add_convert_fusion.2), channel_id=1, source_target_pairs={{0,1},{1,2},{2,3},{3,0},{4,5},{5,6},{6,7},{7,4},{8,9},{9,10},{10,1... | collective-permute-start | bytes 1572872 | tf_op jit(solution)/shard_map/ppermute | solution.py:287
  88.5 14.5 %copy-start.6 = (bf16[128,2048]{1,0:T(8,128)(2,1)S(1)}, bf16[128,2048]{1,0:T(8,128)(2,1)}, u32[]{:S(2)}) copy-start(bf16[128,2048]{1,0:T(8,128)(2,1)} %param.18) | copy-start | bytes 1572868
  88.5 16.0 %copy-start.11 = (f32[2048]{0:T(1024)S(1)}, f32[2048]{0:T(1024)}, u32[]{:S(2)}) copy-start(f32[2048]{0:T(1024)} %param.32) | copy-start | bytes 24580
  104.7 0.8 copy-start.4
  104.7 12.2 %collective-permute-start.8 = (bf16[128,2048]{1,0:T(8,128)(2,1)S(1)}, bf16[128,2048]{1,0:T(8,128)(2,1)S(1)}, u32[]{:S(2)}, u32[]{:S(2)}) collective-permute-start(bf16[128,2048]{1,0:T(8,128)(2,1)S(1)} %multiply_convert_fusion), channel_id=1, source_target_pairs={{0,3},{1,0},{2,1},{3,2},{4,7},{5,4},{6,5},{7,6},{8,11},{9,8},{10,9... | collective-permute-start | bytes 1572872 | tf_op jit(solution)/shard_map/ppermute | solution.py:287
  105.5 13.3 %collective-permute-start.7 = (bf16[128,2048]{1,0:T(8,128)(2,1)S(1)}, bf16[128,2048]{1,0:T(8,128)(2,1)S(1)}, u32[]{:S(2)}, u32[]{:S(2)}) collective-permute-start(bf16[128,2048]{1,0:T(8,128)(2,1)S(1)} %multiply_convert_fusion), channel_id=1, source_target_pairs={{0,1},{1,2},{2,3},{3,0},{4,5},{5,6},{6,7},{7,4},{8,9},{9,10},{10,1... | collective-permute-start | bytes 1572872 | tf_op jit(solution)/shard_map/ppermute | solution.py:287
  116.9 1.6 %copy-start.7 = (bf16[128,2048]{1,0:T(8,128)(2,1)}, bf16[128,2048]{1,0:T(8,128)(2,1)S(1)}, u32[]{:S(2)}) copy-start(bf16[128,2048]{1,0:T(8,128)(2,1)S(1)} %collective-permute-done.8) | copy-start | bytes 1572868
  116.9 6.5 %collective-permute-start.10 = (bf16[64,2048]{1,0:T(8,128)(2,1)S(1)}, bf16[64,2048]{1,0:T(8,128)(2,1)S(1)}, u32[]{:S(2)}, u32[]{:S(2)}) collective-permute-start(bf16[64,2048]{1,0:T(8,128)(2,1)S(1)} %slice.74), channel_id=1, source_target_pairs={{0,3},{1,0},{2,1},{3,2},{4,7},{5,4},{6,5},{7,6},{8,11},{9,8},{10,9... | collective-permute-start | bytes 786440 | tf_op jit(solution)/shard_map/ppermute | solution.py:287
  118.8 4.6 %copy-start.9 = (bf16[128,2048]{1,0:T(8,128)(2,1)}, bf16[128,2048]{1,0:T(8,128)(2,1)S(1)}, u32[]{:S(2)}) copy-start(bf16[128,2048]{1,0:T(8,128)(2,1)S(1)} %collective-permute-done.7) | copy-start | bytes 1572868
  118.8 7.8 %collective-permute-start.9 = (bf16[64,2048]{1,0:T(8,128)(2,1)S(1)}, bf16[64,2048]{1,0:T(8,128)(2,1)}, u32[]{:S(2)}, u32[]{:S(2)}) collective-permute-start(bf16[64,2048]{1,0:T(8,128)(2,1)S(1)} %slice.73), channel_id=1, source_target_pairs={{0,1},{1,2},{2,3},{3,0},{4,5},{5,6},{6,7},{7,4},{8,9},{9,10},{10,1... | collective-permute-start | bytes 786440 | tf_op jit(solution)/shard_map/ppermute | solution.py:287
  126.6 5.6 %copy-start.12 = (bf16[2048,2304]{1,0:T(8,128)(2,1)S(1)}, bf16[2048,2304]{1,0:T(8,128)(2,1)}, u32[]{:S(2)}) copy-start(bf16[2048,2304]{1,0:T(8,128)(2,1)} %all-gather.2.cloned.1.call-done) | copy-start | bytes 28311556
  132.1 4.5 %copy-start.8 = (bf16[128,2048]{1,0:T(8,128)(2,1)S(1)}, bf16[128,2048]{1,0:T(8,128)(2,1)}, u32[]{:S(2)}) copy-start(bf16[128,2048]{1,0:T(8,128)(2,1)} %copy-done.7) | copy-start | bytes 1572868
  132.1 4.5 %copy-start.10 = (bf16[128,2048]{1,0:T(8,128)(2,1)S(1)}, bf16[128,2048]{1,0:T(8,128)(2,1)}, u32[]{:S(2)}) copy-start(bf16[128,2048]{1,0:T(8,128)(2,1)} %copy-done.9) | copy-start | bytes 1572868
  133.3 8.3 %collective-permute-start.11 = (bf16[64,2048]{1,0:T(8,128)(2,1)S(1)}, bf16[64,2048]{1,0:T(8,128)(2,1)S(1)}, u32[]{:S(2)}, u32[]{:S(2)}) collective-permute-start(bf16[64,2048]{1,0:T(8,128)(2,1)S(1)} %get-tuple-element.21), channel_id=1, source_target_pairs={{0,1},{1,2},{2,3},{3,0},{4,5},{5,6},{6,7},{7,4},{8,9},{9,10},{10,1... | collective-permute-start | bytes 786440 | tf_op jit(solution)/shard_map/ppermute | solution.py:287
  133.5 8.1 %collective-permute-start.13 = (bf16[64,2048]{1,0:T(8,128)(2,1)S(1)}, bf16[64,2048]{1,0:T(8,128)(2,1)S(1)}, u32[]{:S(2)}, u32[]{:S(2)}) collective-permute-start(bf16[64,2048]{1,0:T(8,128)(2,1)S(1)} %get-tuple-element.22), channel_id=1, source_target_pairs={{0,3},{1,0},{2,1},{3,2},{4,7},{5,4},{6,5},{7,6},{8,11},{9,8},{10,9... | collective-permute-start | bytes 786440 | tf_op jit(solution)/shard_map/ppermute | solution.py:287
  139.5 6.1 %copy-start.5 = (bf16[128,2048]{1,0:T(8,128)(2,1)S(1)}, bf16[128,2048]{1,0:T(8,128)(2,1)}, u32[]{:S(2)}) copy-start(bf16[128,2048]{1,0:T(8,128)(2,1)} %copy-done.4) | copy-start | bytes 1572868
  141.8 10.9 %collective-permute-start.12 = (bf16[128,2048]{1,0:T(8,128)(2,1)S(1)}, bf16[128,2048]{1,0:T(8,128)(2,1)S(1)}, u32[]{:S(2)}, u32[]{:S(2)}) collective-permute-start(bf16[128,2048]{1,0:T(8,128)(2,1)S(1)} %get-tuple-element.19), channel_id=1, source_target_pairs={{0,1},{1,2},{2,3},{3,0},{4,5},{5,6},{6,7},{7,4},{8,9},{9,10},{10,1... | collective-permute-start | bytes 1572872 | tf_op jit(solution)/shard_map/ppermute | solution.py:287
  142.2 10.5 %collective-permute-start.14 = (bf16[128,2048]{1,0:T(8,128)(2,1)S(1)}, bf16[128,2048]{1,0:T(8,128)(2,1)S(1)}, u32[]{:S(2)}, u32[]{:S(2)}) collective-permute-start(bf16[128,2048]{1,0:T(8,128)(2,1)S(1)} %get-tuple-element.20), channel_id=1, source_target_pairs={{0,3},{1,0},{2,1},{3,2},{4,7},{5,4},{6,5},{7,6},{8,11},{9,8},{10,9... | collective-permute-start | bytes 1572872 | tf_op jit(solution)/shard_map/ppermute | solution.py:287
Sparse Core Ops, SparseCore 0:
  11.1 92.9 all-gather.1
where the time goes:
time: 161 us
  waiting for transfers between devices  61.1 us (38%)
  starting transfers between devices  46.7 us (29%)
  matrix products  17.4 us (11%)
  Pallas kernels  14.6 us (9%)
  between operations  13.8 us (9%)
  local copies, waits for them, and re-layouts  3.95 us (2%)
  other arithmetic  3.01 us (2%)
    ppermute x15, waiting for transfers between devices, ring(): lax.ppermute(array, 'tp', [(i, (i + by) % peers) for i in range(peers)])  50.3 us
    all_to_all x1, starting transfers between devices, activations(): pieces = lax.all_to_all(end, 'sp', 0, 0, tiled=True)  24.8 us
    ppermute x15, starting transfers between devices, ring(): lax.ppermute(array, 'tp', [(i, (i + by) % peers) for i in range(peers)])  22 us
    all_to_all x1, waiting for transfers between devices, activations(): pieces = lax.all_to_all(end, 'sp', 0, 0, tiled=True)  10.7 us
    dot_general x3, matrix products, feed(): hidden = jnp.dot(rows, both, preferred_element_type=F32)  6.8 us
    pallas_call x1, Pallas kernels, activations(): pl.pallas_call(local_kernel, out_shape=(shaped(rows, chans), shaped(rows,...  6.2 us
    dot_general x8, matrix products, project(): jnp.dot(rows, rows_at(w, (me + place) % peers, chans), preferred_element_...  4.75 us
    pallas_call x1, Pallas kernels, activations(): pl.pallas_call(ends_kernel, out_shape=(shaped(peers, 2 * flat // LANES, L...  4.4 us
  transfers between devices with their start and end apart: 17, of which 11 were waited for; matrix products, arithmetic and copies ran while one was open for 9% of the time, Pallas kernels for 6%

commit v1 on v0

--- a/solution.py
+++ b/solution.py
@@ -300,16 +300,18 @@
     return own, left, right, jnp.concatenate([far_top, far_low], axis=0)
 
 
-def summed(product, me, peers):
-    far = product((me + 2) % peers).astype(BF16)
-    half = far.shape[0] // 2
-    from_left, from_right = ring(far[:half], 1), ring(far[half:], -1)
-    right = product((me + 1) % peers)
-    left = product((me + 3) % peers)
-    right = right + jnp.pad(from_left, ((0, half), (0, 0))).astype(F32)
-    left = left + jnp.pad(from_right, ((half, 0), (0, 0))).astype(F32)
-    from_left, from_right = ring(right.astype(BF16), 1), ring(left.astype(BF16), -1)
-    return product(me) + from_left.astype(F32) + from_right.astype(F32)
+def summed(far, right, left, own):
+    half = own.shape[0] // 2
+    from_left_low = ring(right[half:].astype(BF16), 1)
+    from_right_top = ring(left[:half].astype(BF16), -1)
+    far = far.astype(BF16)
+    passing_up = ring(far[:half], 1)
+    passing_down = ring(far[half:], -1)
+    from_left_top = ring((right[:half] + passing_up.astype(F32)).astype(BF16), 1)
+    from_right_low = ring((left[half:] + passing_down.astype(F32)).astype(BF16), -1)
+    top = own[:half] + from_right_top.astype(F32) + from_left_top.astype(F32)
+    low = own[half:] + from_left_low.astype(F32) + from_right_low.astype(F32)
+    return jnp.concatenate([top, low], axis=0)
 
 
 def shards(
@@ -341,10 +343,13 @@
     mixed = (jax.nn.sigmoid(gate_input.astype(F32)) * value * jax.nn.sigmoid(gated)).astype(BF16)
 
     owned = residual.shape[0]
-    branch = summed(
-        lambda q: jnp.dot(rows_at(mixed, q, owned), mix_weight, preferred_element_type=F32),
-        me, peers,
-    )
+
+    def mix(place):
+        rows = rows_at(mixed, (me + place) % peers, owned)
+        return jnp.dot(rows, mix_weight, preferred_element_type=F32)
+
+    far = mix(2)
+    branch = summed(far, mix(1), mix(3), mix(0))
     inner = residual.astype(F32) + branch
     scale = lax.rsqrt(jnp.mean(inner * inner, axis=-1, keepdims=True) + EPSILON)
     normed = (inner * scale * norm_gain).astype(BF16)
@@ -357,8 +362,8 @@
 
     near = feed(own)
     sides = feed(jnp.concatenate([left, right], axis=0))
-    products = {0: near, 1: sides[owned:], 2: feed(far), 3: sides[:owned]}
-    down = summed(lambda q: products[q], 0, peers)
+    sides = lax.optimization_barrier(sides)
+    down = summed(feed(far), sides[owned:], sides[:owned], near)
     return (inner + 0.5 * down).astype(BF16)
 
 

time: 161 us -> 154 us (0.957)
  waiting for transfers between devices: 61.1 us -> 48.8 us
  starting transfers between devices: 46.7 us -> 54.8 us
    ppermute x15 -> x19, waiting for transfers between devices: 50.3 us -> 38.1 us  [ring(): lax.ppermute(array, 'tp', [(i, (i + by) % peers) for i in range(peers)])]
    ppermute x15 -> x19, starting transfers between devices: 22 us -> 30.1 us  [ring(): lax.ppermute(array, 'tp', [(i, (i + by) % peers) for i in range(peers)])]
  transfers between devices with their start and end apart: 17 -> 21, of which waited for: 11 -> 13; matrix products, arithmetic and copies ran while one was open for 9% -> 8% of each run, Pallas kernels for 6% -> 7%
where the time goes in v1:
time: 154 us
  starting transfers between devices  54.8 us (36%)
  waiting for transfers between devices  48.8 us (32%)
  matrix products  16.6 us (11%)
  Pallas kernels  14.7 us (10%)
  between operations  13.9 us (9%)
  local copies, waits for them, and re-layouts  2.76 us (2%)
  other arithmetic  2.22 us (1%)
    ppermute x19, waiting for transfers between devices, ring(): lax.ppermute(array, 'tp', [(i, (i + by) % peers) for i in range(peers)])  38.1 us
    ppermute x19, starting transfers between devices, ring(): lax.ppermute(array, 'tp', [(i, (i + by) % peers) for i in range(peers)])  30.1 us
    all_to_all x1, starting transfers between devices, activations(): pieces = lax.all_to_all(end, 'sp', 0, 0, tiled=True)  24.8 us
    all_to_all x1, waiting for transfers between devices, activations(): pieces = lax.all_to_all(end, 'sp', 0, 0, tiled=True)  10.7 us
    dot_general x3, matrix products, feed(): hidden = jnp.dot(rows, both, preferred_element_type=F32)  6.77 us
    pallas_call x1, Pallas kernels, activations(): pl.pallas_call(local_kernel, out_shape=(shaped(rows, chans), shaped(rows,...  6.19 us
    dot_general x8, matrix products, project(): jnp.dot(rows, rows_at(w, (me + place) % peers, chans), preferred_element_...  4.73 us
    pallas_call x1, Pallas kernels, activations(): pl.pallas_call(ends_kernel, out_shape=(shaped(peers, 2 * flat // LANES, L...  4.43 us
  transfers between devices with their start and end apart: 21, of which 13 were waited for; matrix products, arithmetic and copies ran while one was open for 8% of the time, Pallas kernels for 7%

profile of v1, /device:TPU:40, one launch (start us, length us, event | category | flops | bytes accessed | tf_op | source)
XLA Modules:
  0.0 153.7 jit_solution(15026828047605150789)
XLA Ops:
  6.6 4.4 %ssm_ends.1 = (bf16[32,16,128]{2,1,0:T(8,128)(2,1)}, f32[2,8,1024]{2,1,0:T(8,128)}, f32[4,1024]{1,0:T(4,128)}, bf16[64,2304]{1,0:T(8,128)(2,1)}) custom-call(s32[1]{0:T(128)} %bitcast.me_ref, f32[16,64]{1,0:T(8,128)} %decay_ref.1, f32[16,64]{1,0:T(8,128)} %freq_ref.1, f32[1,16]{1,0:T(1,128)} %bitcast.34, bf16[512,256]{1,0:T(8,128)(2,1)} %x_ref.3, ...), custom_call_target="tpu_custom_call" | custom-call | tf_op jit(solution)/shard_map/ssm_ends/pallas_call | solution.py:249
  11.0 24.8 %all-to-all-start = ((bf16[32,16,128]{2,1,0:T(8,128)(2,1)}), bf16[32,16,128]{2,1,0:T(8,128)(2,1)S(1)}, u32[]{:S(2)}, u32[]{:S(2)}) async-start(bf16[32,16,128]{2,1,0:T(8,128)(2,1)} %get-tuple-element.11), calls=%async_computation | async-start | bytes 262144 | tf_op jit(solution)/shard_map/all_to_all | solution.py:262
  35.9 6.2 %ssm_local.1 = (f32[512,256]{1,0:T(8,128)}, bf16[512,2048]{1,0:T(8,128)(2,1)}) custom-call(f32[4,1024]{1,0:T(4,128)} %get-tuple-element.12.row_ref, f32[2,8,1024]{2,1,0:T(8,128)} %get-tuple-element.13.seg_ref, bf16[512,256]{1,0:T(8,128)(2,1)} %x_ref.3, f32[256,64]{1,0:T(8,128)} %bitcast.26, f32[256,64]{1,0:T(8,128)} %bitcast.28, f32[256,64]{1,0:T(8,128)} %bitcast.29, ...), custom_call_target="tpu_custom_call" | custom-call | flops 1073741824 | bytes 4194304 | tf_op jit(solution)/shard_map/ssm_local/pallas_call | solution.py:263
  42.1 10.7 %all-to-all-done.piece_ref = bf16[32,16,128]{2,1,0:T(8,128)(2,1)S(1)} async-done(((bf16[32,16,128]{2,1,0:T(8,128)(2,1)}), bf16[32,16,128]{2,1,0:T(8,128)(2,1)S(1)}, u32[]{:S(2)}, u32[]{:S(2)}) %all-to-all-start) | async-done | bytes 131104 | tf_op jit(solution)/shard_map/all_to_all | solution.py:262
  53.4 4.0 %ssm_finish.1 = bf16[512,256]{1,0:T(8,128)(2,1)} custom-call(bf16[32,16,128]{2,1,0:T(8,128)(2,1)} %copy-done.7, f32[4,1024]{1,0:T(4,128)} %get-tuple-element.12.row_ref, f32[256,64]{1,0:T(8,128)} %bitcast.30, f32[256,64]{1,0:T(8,128)} %bitcast.32, f32[512,256]{1,0:T(8,128)} %get-tuple-element.14.y_ref, bf16[512,2048]{1,0:T(8,128)(2,1)} %get-tuple-element.15.power_ref), custom_call_target="tpu_custom_call" | custom-call | tf_op jit(solution)/shard_map/ssm_finish/pallas_call | solution.py:276
  57.5 3.4 %collective-permute-start.2 = (bf16[512,256]{1,0:T(8,128)(2,1)}, bf16[512,256]{1,0:T(8,128)(2,1)S(1)}, u32[]{:S(2)}, u32[]{:S(2)}) collective-permute-start(bf16[512,256]{1,0:T(8,128)(2,1)} %ssm_finish.1), channel_id=1, source_target_pairs={{0,2},{1,3},{2,0},{3,1},{4,6},{5,7},{6,4},{7,5},{8,10},{9,11},{10,... | collective-permute-start | bytes 786440 | tf_op jit(solution)/shard_map/ppermute | solution.py:287
  62.9 1.3 fusion.45
  64.2 1.4 fusion.51
  65.6 6.3 %collective-permute-done = bf16[512,256]{1,0:T(8,128)(2,1)S(1)} collective-permute-done((bf16[512,256]{1,0:T(8,128)(2,1)}, bf16[512,256]{1,0:T(8,128)(2,1)S(1)}, u32[]{:S(2)}, u32[]{:S(2)}) %collective-permute-start) | collective-permute-done | bytes 262176 | tf_op jit(solution)/shard_map/ppermute | solution.py:287
  74.8 1.9 %collective-permute-start.4 = (bf16[64,2048]{1,0:T(8,128)(2,1)S(1)}, bf16[64,2048]{1,0:T(8,128)(2,1)S(1)}, u32[]{:S(2)}, u32[]{:S(2)}) collective-permute-start(bf16[64,2048]{1,0:T(8,128)(2,1)S(1)} %get-tuple-element.27), channel_id=1, source_target_pairs={{0,1},{1,2},{2,3},{3,0},{4,5},{5,6},{6,7},{7,4},{8,9},{9,10},{10,1... | collective-permute-start | bytes 786440 | tf_op jit(solution)/shard_map/ppermute | solution.py:287
  76.7 1.5 collective-permute-start.7
  79.8 2.8 %collective-permute-start.3 = (bf16[64,2048]{1,0:T(8,128)(2,1)S(1)}, bf16[64,2048]{1,0:T(8,128)(2,1)S(1)}, u32[]{:S(2)}, u32[]{:S(2)}) collective-permute-start(bf16[64,2048]{1,0:T(8,128)(2,1)S(1)} %slice.197), channel_id=1, source_target_pairs={{0,3},{1,0},{2,1},{3,2},{4,7},{5,4},{6,5},{7,6},{8,11},{9,8},{10,9... | collective-permute-start | bytes 786440 | tf_op jit(solution)/shard_map/ppermute | solution.py:287
  82.6 2.6 %collective-permute-done.4 = bf16[64,2048]{1,0:T(8,128)(2,1)S(1)} collective-permute-done((bf16[64,2048]{1,0:T(8,128)(2,1)S(1)}, bf16[64,2048]{1,0:T(8,128)(2,1)S(1)}, u32[]{:S(2)}, u32[]{:S(2)}) %collective-permute-start.4) | collective-permute-done | bytes 262176 | tf_op jit(solution)/shard_map/ppermute | solution.py:287
  86.1 2.6 %collective-permute-start.8 = (bf16[64,2048]{1,0:T(8,128)(2,1)S(1)}, bf16[64,2048]{1,0:T(8,128)(2,1)S(1)}, u32[]{:S(2)}, u32[]{:S(2)}) collective-permute-start(bf16[64,2048]{1,0:T(8,128)(2,1)S(1)} %fusion.30), channel_id=1, source_target_pairs={{0,3},{1,0},{2,1},{3,2},{4,7},{5,4},{6,5},{7,6},{8,11},{9,8},{10,9... | collective-permute-start | bytes 786440 | tf_op jit(solution)/shard_map/ppermute | solution.py:287
  89.3 1.6 %collective-permute-done.6 = bf16[64,2048]{1,0:T(8,128)(2,1)S(1)} collective-permute-done((bf16[64,2048]{1,0:T(8,128)(2,1)S(1)}, bf16[64,2048]{1,0:T(8,128)(2,1)S(1)}, u32[]{:S(2)}, u32[]{:S(2)}) %collective-permute-start.6) | collective-permute-done | bytes 262176 | tf_op jit(solution)/shard_map/ppermute | solution.py:287
  91.5 2.9 %collective-permute-done.5 = bf16[64,2048]{1,0:T(8,128)(2,1)S(1)} collective-permute-done((bf16[64,2048]{1,0:T(8,128)(2,1)S(1)}, bf16[64,2048]{1,0:T(8,128)(2,1)S(1)}, u32[]{:S(2)}, u32[]{:S(2)}) %collective-permute-start.5) | collective-permute-done | bytes 262176 | tf_op jit(solution)/shard_map/ppermute | solution.py:287
  94.4 1.2 collective-permute-done.8
  96.3 2.2 %collective-permute-start.10 = (bf16[128,2048]{1,0:T(8,128)(2,1)S(1)}, bf16[128,2048]{1,0:T(8,128)(2,1)S(1)}, u32[]{:S(2)}, u32[]{:S(2)}) collective-permute-start(bf16[128,2048]{1,0:T(8,128)(2,1)S(1)} %multiply_convert_fusion), channel_id=1, source_target_pairs={{0,3},{1,0},{2,1},{3,2},{4,7},{5,4},{6,5},{7,6},{8,11},{9,8},{10,9... | collective-permute-start | bytes 1572872 | tf_op jit(solution)/shard_map/ppermute | solution.py:287
  98.8 10.4 %collective-permute-done.10 = bf16[128,2048]{1,0:T(8,128)(2,1)S(1)} collective-permute-done((bf16[128,2048]{1,0:T(8,128)(2,1)S(1)}, bf16[128,2048]{1,0:T(8,128)(2,1)S(1)}, u32[]{:S(2)}, u32[]{:S(2)}) %collective-permute-start.10) | collective-permute-done | bytes 524320 | tf_op jit(solution)/shard_map/ppermute | solution.py:287
  109.2 2.9 %collective-permute-start.13 = (bf16[64,2048]{1,0:T(8,128)(2,1)S(1)}, bf16[64,2048]{1,0:T(8,128)(2,1)S(1)}, u32[]{:S(2)}, u32[]{:S(2)}) collective-permute-start(bf16[64,2048]{1,0:T(8,128)(2,1)S(1)} %slice.132), channel_id=1, source_target_pairs={{0,3},{1,0},{2,1},{3,2},{4,7},{5,4},{6,5},{7,6},{8,11},{9,8},{10,9... | collective-permute-start | bytes 786440 | tf_op jit(solution)/shard_map/ppermute | solution.py:287
  112.3 3.7 %collective-permute-done.13 = bf16[64,2048]{1,0:T(8,128)(2,1)S(1)} collective-permute-done((bf16[64,2048]{1,0:T(8,128)(2,1)S(1)}, bf16[64,2048]{1,0:T(8,128)(2,1)S(1)}, u32[]{:S(2)}, u32[]{:S(2)}) %collective-permute-start.13) | collective-permute-done | bytes 262176 | tf_op jit(solution)/shard_map/ppermute | solution.py:287
  116.0 3.9 %collective-permute-done.12 = bf16[64,2048]{1,0:T(8,128)(2,1)} collective-permute-done((bf16[64,2048]{1,0:T(8,128)(2,1)S(1)}, bf16[64,2048]{1,0:T(8,128)(2,1)}, u32[]{:S(2)}, u32[]{:S(2)}) %collective-permute-start.12) | collective-permute-done | bytes 262176 | tf_op jit(solution)/shard_map/ppermute | solution.py:287
  120.0 4.0 %fusion = f32[128,1536]{1,0:T(8,128)S(1)} fusion(bf16[2048,2304]{1,0:T(8,128)(2,1)} %all-gather.2.cloned.1.call-done, bf16[64,2048]{1,0:T(8,128)(2,1)S(1)} %collective-permute-done.13, bf16[64,2048]{1,0:T(8,128)(2,1)} %collective-permute-done.12), kind=kOutput, calls=%fused_computation | convolution fusion | flops 806354944 | bytes 7602176 | tf_op jit(solution)/shard_map/dot_general | solution.py:359
  124.0 1.6 %copy-done.13 = bf16[2048,2304]{1,0:T(8,128)(2,1)S(1)} copy-done((bf16[2048,2304]{1,0:T(8,128)(2,1)S(1)}, bf16[2048,2304]{1,0:T(8,128)(2,1)}, u32[]{:S(2)}) %copy-start.13) | copy-done | bytes 9437208
  125.5 1.2 convolution_convert_fusion
  126.9 3.2 %collective-permute-start.17 = (bf16[64,2048]{1,0:T(8,128)(2,1)S(1)}, bf16[64,2048]{1,0:T(8,128)(2,1)S(1)}, u32[]{:S(2)}, u32[]{:S(2)}) collective-permute-start(bf16[64,2048]{1,0:T(8,128)(2,1)S(1)} %get-tuple-element.26), channel_id=1, source_target_pairs={{0,3},{1,0},{2,1},{3,2},{4,7},{5,4},{6,5},{7,6},{8,11},{9,8},{10,9... | collective-permute-start | bytes 786440 | tf_op jit(solution)/shard_map/ppermute | solution.py:287
  130.1 1.8 %fusion.2 = f32[256,1536]{1,0:T(8,128)S(1)} fusion(bf16[2048,2304]{1,0:T(8,128)(2,1)S(1)} %copy-done.13, bf16[128,2048]{1,0:T(8,128)(2,1)S(1)} %copy-done.9, bf16[128,2048]{1,0:T(8,128)(2,1)S(1)} %copy-done.11), kind=kOutput, calls=%fused_computation.2 | convolution fusion | flops 1612709888 | bytes 8912896 | tf_op jit(solution)/shard_map/dot_general | solution.py:359
  133.3 2.0 %collective-permute-start.16 = (bf16[64,2048]{1,0:T(8,128)(2,1)S(1)}, bf16[64,2048]{1,0:T(8,128)(2,1)S(1)}, u32[]{:S(2)}, u32[]{:S(2)}) collective-permute-start(bf16[64,2048]{1,0:T(8,128)(2,1)S(1)} %get-tuple-element.22), channel_id=1, source_target_pairs={{0,1},{1,2},{2,3},{3,0},{4,5},{5,6},{6,7},{7,4},{8,9},{9,10},{10,1... | collective-permute-start | bytes 786440 | tf_op jit(solution)/shard_map/ppermute | solution.py:287
  136.6 3.2 %collective-permute-start.18 = (bf16[64,2048]{1,0:T(8,128)(2,1)S(1)}, bf16[64,2048]{1,0:T(8,128)(2,1)S(1)}, u32[]{:S(2)}, u32[]{:S(2)}) collective-permute-start(bf16[64,2048]{1,0:T(8,128)(2,1)S(1)} %get-tuple-element.18), channel_id=1, source_target_pairs={{0,3},{1,0},{2,1},{3,2},{4,7},{5,4},{6,5},{7,6},{8,11},{9,8},{10,9... | collective-permute-start | bytes 786440 | tf_op jit(solution)/shard_map/ppermute | solution.py:287
  139.8 1.1 fusion.9
  140.9 1.1 collective-permute-done.11
  142.9 2.8 %collective-permute-done.15 = bf16[64,2048]{1,0:T(8,128)(2,1)S(1)} collective-permute-done((bf16[64,2048]{1,0:T(8,128)(2,1)S(1)}, bf16[64,2048]{1,0:T(8,128)(2,1)S(1)}, u32[]{:S(2)}, u32[]{:S(2)}) %collective-permute-start.15) | collective-permute-done | bytes 262176 | tf_op jit(solution)/shard_map/ppermute | solution.py:287
  (79 shorter events, 15.3 us)
Async XLA Ops:
  6.5 67.8 %copy-start = (bf16[512,2048]{1,0:T(8,128)(2,1)S(1)}, bf16[512,2048]{1,0:T(8,128)(2,1)}, u32[]{:S(2)}) copy-start(bf16[512,2048]{1,0:T(8,128)(2,1)} %param.31) | copy-start | bytes 6291460
  6.6 113.4 %all-gather.2.cloned.1.call-start = ((), (), s32[]{:S(2)}) async-start(), calls=%async_computation.1 | async-start | bytes 9732096 | tf_op jit(solution)/shard_map/all_gather | solution.py:261
  11.0 41.7 %all-to-all-start = ((bf16[32,16,128]{2,1,0:T(8,128)(2,1)}), bf16[32,16,128]{2,1,0:T(8,128)(2,1)S(1)}, u32[]{:S(2)}, u32[]{:S(2)}) async-start(bf16[32,16,128]{2,1,0:T(8,128)(2,1)} %get-tuple-element.11), calls=%async_computation | async-start | bytes 262144 | tf_op jit(solution)/shard_map/all_to_all | solution.py:262
  35.9 27.0 %copy-start.3 = (bf16[1024,512]{1,0:T(8,128)(2,1)S(1)}, bf16[1024,512]{1,0:T(8,128)(2,1)}, u32[]{:S(2)}) copy-start(bf16[1024,512]{1,0:T(8,128)(2,1)} %param.30) | copy-start | bytes 3145732
  57.5 14.7 %copy-start.4 = (bf16[1024,512]{1,0:T(8,128)(2,1)S(1)}, bf16[1024,512]{1,0:T(8,128)(2,1)}, u32[]{:S(2)}) copy-start(bf16[1024,512]{1,0:T(8,128)(2,1)} %param.29) | copy-start | bytes 3145732
  57.5 15.0 %collective-permute-start.2 = (bf16[512,256]{1,0:T(8,128)(2,1)}, bf16[512,256]{1,0:T(8,128)(2,1)S(1)}, u32[]{:S(2)}, u32[]{:S(2)}) collective-permute-start(bf16[512,256]{1,0:T(8,128)(2,1)} %ssm_finish.1), channel_id=1, source_target_pairs={{0,2},{1,3},{2,0},{3,1},{4,6},{5,7},{6,4},{7,5},{8,10},{9,11},{10,... | collective-permute-start | bytes 786440 | tf_op jit(solution)/shard_map/ppermute | solution.py:287
  60.9 12.2 %collective-permute-start.1 = (bf16[512,256]{1,0:T(8,128)(2,1)}, bf16[512,256]{1,0:T(8,128)(2,1)S(1)}, u32[]{:S(2)}, u32[]{:S(2)}) collective-permute-start(bf16[512,256]{1,0:T(8,128)(2,1)} %ssm_finish.1), channel_id=1, source_target_pairs={{0,3},{1,0},{2,1},{3,2},{4,7},{5,4},{6,5},{7,6},{8,11},{9,8},{10,9... | collective-permute-start | bytes 786440 | tf_op jit(solution)/shard_map/ppermute | solution.py:287
  61.8 10.0 %collective-permute-start = (bf16[512,256]{1,0:T(8,128)(2,1)}, bf16[512,256]{1,0:T(8,128)(2,1)S(1)}, u32[]{:S(2)}, u32[]{:S(2)}) collective-permute-start(bf16[512,256]{1,0:T(8,128)(2,1)} %ssm_finish.1), channel_id=1, source_target_pairs={{0,1},{1,2},{2,3},{3,0},{4,5},{5,6},{6,7},{7,4},{8,9},{9,10},{10,1... | collective-permute-start | bytes 786440 | tf_op jit(solution)/shard_map/ppermute | solution.py:287
  74.8 10.4 %collective-permute-start.4 = (bf16[64,2048]{1,0:T(8,128)(2,1)S(1)}, bf16[64,2048]{1,0:T(8,128)(2,1)S(1)}, u32[]{:S(2)}, u32[]{:S(2)}) collective-permute-start(bf16[64,2048]{1,0:T(8,128)(2,1)S(1)} %get-tuple-element.27), channel_id=1, source_target_pairs={{0,1},{1,2},{2,3},{3,0},{4,5},{5,6},{6,7},{7,4},{8,9},{9,10},{10,1... | collective-permute-start | bytes 786440 | tf_op jit(solution)/shard_map/ppermute | solution.py:287
  76.7 9.3 %collective-permute-start.7 = (bf16[64,2048]{1,0:T(8,128)(2,1)S(1)}, bf16[64,2048]{1,0:T(8,128)(2,1)S(1)}, u32[]{:S(2)}, u32[]{:S(2)}) collective-permute-start(bf16[64,2048]{1,0:T(8,128)(2,1)S(1)} %get-tuple-element.28), channel_id=1, source_target_pairs={{0,3},{1,0},{2,1},{3,2},{4,7},{5,4},{6,5},{7,6},{8,11},{9,8},{10,9... | collective-permute-start | bytes 786440 | tf_op jit(solution)/shard_map/ppermute | solution.py:287
  78.7 12.2 %collective-permute-start.6 = (bf16[64,2048]{1,0:T(8,128)(2,1)S(1)}, bf16[64,2048]{1,0:T(8,128)(2,1)S(1)}, u32[]{:S(2)}, u32[]{:S(2)}) collective-permute-start(bf16[64,2048]{1,0:T(8,128)(2,1)S(1)} %slice.196), channel_id=1, source_target_pairs={{0,1},{1,2},{2,3},{3,0},{4,5},{5,6},{6,7},{7,4},{8,9},{9,10},{10,1... | collective-permute-start | bytes 786440 | tf_op jit(solution)/shard_map/ppermute | solution.py:287
  79.8 11.7 %collective-permute-start.3 = (bf16[64,2048]{1,0:T(8,128)(2,1)S(1)}, bf16[64,2048]{1,0:T(8,128)(2,1)S(1)}, u32[]{:S(2)}, u32[]{:S(2)}) collective-permute-start(bf16[64,2048]{1,0:T(8,128)(2,1)S(1)} %slice.197), channel_id=1, source_target_pairs={{0,3},{1,0},{2,1},{3,2},{4,7},{5,4},{6,5},{7,6},{8,11},{9,8},{10,9... | collective-permute-start | bytes 786440 | tf_op jit(solution)/shard_map/ppermute | solution.py:287
  85.3 9.1 %collective-permute-start.5 = (bf16[64,2048]{1,0:T(8,128)(2,1)S(1)}, bf16[64,2048]{1,0:T(8,128)(2,1)S(1)}, u32[]{:S(2)}, u32[]{:S(2)}) collective-permute-start(bf16[64,2048]{1,0:T(8,128)(2,1)S(1)} %fusion.32), channel_id=1, source_target_pairs={{0,1},{1,2},{2,3},{3,0},{4,5},{5,6},{6,7},{7,4},{8,9},{9,10},{10,1... | collective-permute-start | bytes 786440 | tf_op jit(solution)/shard_map/ppermute | solution.py:287
  86.1 9.7 %copy-start.1 = (bf16[128,2048]{1,0:T(8,128)(2,1)S(1)}, bf16[128,2048]{1,0:T(8,128)(2,1)}, u32[]{:S(2)}) copy-start(bf16[128,2048]{1,0:T(8,128)(2,1)} %param.18) | copy-start | bytes 1572868
  86.1 9.5 %collective-permute-start.8 = (bf16[64,2048]{1,0:T(8,128)(2,1)S(1)}, bf16[64,2048]{1,0:T(8,128)(2,1)S(1)}, u32[]{:S(2)}, u32[]{:S(2)}) collective-permute-start(bf16[64,2048]{1,0:T(8,128)(2,1)S(1)} %fusion.30), channel_id=1, source_target_pairs={{0,3},{1,0},{2,1},{3,2},{4,7},{5,4},{6,5},{7,6},{8,11},{9,8},{10,9... | collective-permute-start | bytes 786440 | tf_op jit(solution)/shard_map/ppermute | solution.py:287
  89.2 6.8 %copy-start.12 = (f32[2048]{0:T(1024)S(1)}, f32[2048]{0:T(1024)}, u32[]{:S(2)}) copy-start(f32[2048]{0:T(1024)} %param.32) | copy-start | bytes 24580
  96.3 12.9 %collective-permute-start.10 = (bf16[128,2048]{1,0:T(8,128)(2,1)S(1)}, bf16[128,2048]{1,0:T(8,128)(2,1)S(1)}, u32[]{:S(2)}, u32[]{:S(2)}) collective-permute-start(bf16[128,2048]{1,0:T(8,128)(2,1)S(1)} %multiply_convert_fusion), channel_id=1, source_target_pairs={{0,3},{1,0},{2,1},{3,2},{4,7},{5,4},{6,5},{7,6},{8,11},{9,8},{10,9... | collective-permute-start | bytes 1572872 | tf_op jit(solution)/shard_map/ppermute | solution.py:287
  98.5 13.7 %collective-permute-start.9 = (bf16[128,2048]{1,0:T(8,128)(2,1)S(1)}, bf16[128,2048]{1,0:T(8,128)(2,1)S(1)}, u32[]{:S(2)}, u32[]{:S(2)}) collective-permute-start(bf16[128,2048]{1,0:T(8,128)(2,1)S(1)} %multiply_convert_fusion), channel_id=1, source_target_pairs={{0,1},{1,2},{2,3},{3,0},{4,5},{5,6},{6,7},{7,4},{8,9},{9,10},{10,1... | collective-permute-start | bytes 1572872 | tf_op jit(solution)/shard_map/ppermute | solution.py:287
  109.2 2.9 %copy-start.8 = (bf16[128,2048]{1,0:T(8,128)(2,1)}, bf16[128,2048]{1,0:T(8,128)(2,1)S(1)}, u32[]{:S(2)}) copy-start(bf16[128,2048]{1,0:T(8,128)(2,1)S(1)} %collective-permute-done.10) | copy-start | bytes 1572868
  109.2 6.8 %collective-permute-start.13 = (bf16[64,2048]{1,0:T(8,128)(2,1)S(1)}, bf16[64,2048]{1,0:T(8,128)(2,1)S(1)}, u32[]{:S(2)}, u32[]{:S(2)}) collective-permute-start(bf16[64,2048]{1,0:T(8,128)(2,1)S(1)} %slice.132), channel_id=1, source_target_pairs={{0,3},{1,0},{2,1},{3,2},{4,7},{5,4},{6,5},{7,6},{8,11},{9,8},{10,9... | collective-permute-start | bytes 786440 | tf_op jit(solution)/shard_map/ppermute | solution.py:287
  112.1 3.9 %copy-start.10 = (bf16[128,2048]{1,0:T(8,128)(2,1)}, bf16[128,2048]{1,0:T(8,128)(2,1)S(1)}, u32[]{:S(2)}) copy-start(bf16[128,2048]{1,0:T(8,128)(2,1)S(1)} %collective-permute-done.9) | copy-start | bytes 1572868
  112.2 7.8 %collective-permute-start.12 = (bf16[64,2048]{1,0:T(8,128)(2,1)S(1)}, bf16[64,2048]{1,0:T(8,128)(2,1)}, u32[]{:S(2)}, u32[]{:S(2)}) collective-permute-start(bf16[64,2048]{1,0:T(8,128)(2,1)S(1)} %slice.131), channel_id=1, source_target_pairs={{0,1},{1,2},{2,3},{3,0},{4,5},{5,6},{6,7},{7,4},{8,9},{9,10},{10,1... | collective-permute-start | bytes 786440 | tf_op jit(solution)/shard_map/ppermute | solution.py:287
  120.0 5.6 %copy-start.13 = (bf16[2048,2304]{1,0:T(8,128)(2,1)S(1)}, bf16[2048,2304]{1,0:T(8,128)(2,1)}, u32[]{:S(2)}) copy-start(bf16[2048,2304]{1,0:T(8,128)(2,1)} %all-gather.2.cloned.1.call-done) | copy-start | bytes 28311556
  125.5 4.6 %copy-start.9 = (bf16[128,2048]{1,0:T(8,128)(2,1)S(1)}, bf16[128,2048]{1,0:T(8,128)(2,1)}, u32[]{:S(2)}) copy-start(bf16[128,2048]{1,0:T(8,128)(2,1)} %copy-done.8) | copy-start | bytes 1572868
  125.5 4.6 %copy-start.11 = (bf16[128,2048]{1,0:T(8,128)(2,1)S(1)}, bf16[128,2048]{1,0:T(8,128)(2,1)}, u32[]{:S(2)}) copy-start(bf16[128,2048]{1,0:T(8,128)(2,1)} %copy-done.10) | copy-start | bytes 1572868
  126.7 9.5 %collective-permute-start.14 = (bf16[64,2048]{1,0:T(8,128)(2,1)S(1)}, bf16[64,2048]{1,0:T(8,128)(2,1)S(1)}, u32[]{:S(2)}, u32[]{:S(2)}) collective-permute-start(bf16[64,2048]{1,0:T(8,128)(2,1)S(1)} %get-tuple-element.25), channel_id=1, source_target_pairs={{0,1},{1,2},{2,3},{3,0},{4,5},{5,6},{6,7},{7,4},{8,9},{9,10},{10,1... | collective-permute-start | bytes 786440 | tf_op jit(solution)/shard_map/ppermute | solution.py:287
  126.9 9.4 %collective-permute-start.17 = (bf16[64,2048]{1,0:T(8,128)(2,1)S(1)}, bf16[64,2048]{1,0:T(8,128)(2,1)S(1)}, u32[]{:S(2)}, u32[]{:S(2)}) collective-permute-start(bf16[64,2048]{1,0:T(8,128)(2,1)S(1)} %get-tuple-element.26), channel_id=1, source_target_pairs={{0,3},{1,0},{2,1},{3,2},{4,7},{5,4},{6,5},{7,6},{8,11},{9,8},{10,9... | collective-permute-start | bytes 786440 | tf_op jit(solution)/shard_map/ppermute | solution.py:287
  133.1 8.9 %collective-permute-start.11 = (bf16[64,2048]{1,0:T(8,128)(2,1)S(1)}, bf16[64,2048]{1,0:T(8,128)(2,1)S(1)}, u32[]{:S(2)}, u32[]{:S(2)}) collective-permute-start(bf16[64,2048]{1,0:T(8,128)(2,1)S(1)} %get-tuple-element.21), channel_id=1, source_target_pairs={{0,3},{1,0},{2,1},{3,2},{4,7},{5,4},{6,5},{7,6},{8,11},{9,8},{10,9... | collective-permute-start | bytes 786440 | tf_op jit(solution)/shard_map/ppermute | solution.py:287
  133.3 9.6 %collective-permute-start.16 = (bf16[64,2048]{1,0:T(8,128)(2,1)S(1)}, bf16[64,2048]{1,0:T(8,128)(2,1)S(1)}, u32[]{:S(2)}, u32[]{:S(2)}) collective-permute-start(bf16[64,2048]{1,0:T(8,128)(2,1)S(1)} %get-tuple-element.22), channel_id=1, source_target_pairs={{0,1},{1,2},{2,3},{3,0},{4,5},{5,6},{6,7},{7,4},{8,9},{9,10},{10,1... | collective-permute-start | bytes 786440 | tf_op jit(solution)/shard_map/ppermute | solution.py:287
  136.4 9.3 %collective-permute-start.15 = (bf16[64,2048]{1,0:T(8,128)(2,1)S(1)}, bf16[64,2048]{1,0:T(8,128)(2,1)S(1)}, u32[]{:S(2)}, u32[]{:S(2)}) collective-permute-start(bf16[64,2048]{1,0:T(8,128)(2,1)S(1)} %get-tuple-element.17), channel_id=1, source_target_pairs={{0,1},{1,2},{2,3},{3,0},{4,5},{5,6},{6,7},{7,4},{8,9},{9,10},{10,1... | collective-permute-start | bytes 786440 | tf_op jit(solution)/shard_map/ppermute | solution.py:287
  136.6 9.3 %copy-start.2 = (bf16[128,2048]{1,0:T(8,128)(2,1)S(1)}, bf16[128,2048]{1,0:T(8,128)(2,1)}, u32[]{:S(2)}) copy-start(bf16[128,2048]{1,0:T(8,128)(2,1)} %param.18) | copy-start | bytes 1572868
  136.6 9.1 %collective-permute-start.18 = (bf16[64,2048]{1,0:T(8,128)(2,1)S(1)}, bf16[64,2048]{1,0:T(8,128)(2,1)S(1)}, u32[]{:S(2)}, u32[]{:S(2)}) collective-permute-start(bf16[64,2048]{1,0:T(8,128)(2,1)S(1)} %get-tuple-element.18), channel_id=1, source_target_pairs={{0,3},{1,0},{2,1},{3,2},{4,7},{5,4},{6,5},{7,6},{8,11},{9,8},{10,9... | collective-permute-start | bytes 786440 | tf_op jit(solution)/shard_map/ppermute | solution.py:287
  (4 other events, 6.3 us)
Sparse Core Ops, SparseCore 0:
  11.2 92.9 all-gather.1

commit v2 on v1

--- a/solution.py
+++ b/solution.py
@@ -121,13 +121,15 @@
     me_ref, decay_ref, freq_ref, log_step_ref, x_ref, b_re_ref, b_im_ref,
     gate_ref, up_ref, down_ref,
     end_ref, seg_ref, row_ref, weight_ref,
-    xf_ref, xp_ref, d_re_ref, d_im_ref,
+    xf_ref, xp_ref, d_re_ref, d_im_ref, sems,
 ):
     rows, flat = d_re_ref.shape
     length = rows // SEGMENTS
-    at = 0
-    for ref in (gate_ref, up_ref, down_ref):
-        weight_ref[:, at : at + ref.shape[1]] = ref[...]
+    at, copies = 0, []
+    for i, ref in enumerate((gate_ref, up_ref, down_ref)):
+        to = weight_ref.at[:, at : at + ref.shape[1]]
+        copies.append(pltpu.make_async_copy(ref, to, sems.at[i]))
+        copies[-1].start()
         at += ref.shape[1]
     bar, ratio = rates(decay_ref, freq_ref, log_step_ref)
     fill_drive(x_ref, b_re_ref, b_im_ref, xf_ref, xp_ref, d_re_ref, d_im_ref)
@@ -156,6 +158,8 @@
         state = tuple(
             jnp.where(later, new, old) for new, old in zip(times(block, state), state)
         )
+    for copy in copies:
+        copy.wait()
 
 
 def local_kernel(
@@ -203,13 +207,22 @@
 
 
 def finish_kernel(
-    piece_ref, row_ref, c_re_ref, c_im_ref, y_ref, power_ref, out_ref, t_ref
+    piece_ref, row_ref, c_re_ref, c_im_ref, local_ref, powers_ref, out_ref,
+    t_ref, y_ref, power_ref, sems,
 ):
+    copies = [
+        pltpu.make_async_copy(powers_ref, power_ref, sems.at[0]),
+        pltpu.make_async_copy(local_ref, y_ref, sems.at[1]),
+    ]
+    for copy in copies:
+        copy.start()
     pieces = jnp.sum(piece_ref[...].astype(F32), axis=0)
     half = pieces.shape[0] // 2
     total = from_tile(pieces[:half]), from_tile(pieces[half:])
     ratio = row_ref[2:3, :], row_ref[3:4, :]
     read = wide_read(c_re_ref, c_im_ref, times(ratio, total))
+    for copy in copies:
+        copy.wait()
     y = y_ref[...] + lax.dot_general(power_ref[...], read, NT, preferred_element_type=F32)
     y = jax.nn.gelu(y, approximate=True)
     length = y.shape[0] // SEGMENTS
@@ -246,6 +259,7 @@
         pltpu.VMEM((rows, flat), F32),
     ]
     whole = pl.BlockSpec(memory_space=pltpu.VMEM)
+    stored = pl.BlockSpec(memory_space=pl.ANY)
     end, seg, row, weight = pl.pallas_call(
         ends_kernel,
         out_shape=(
@@ -254,8 +268,9 @@
             shaped(4, flat),
             shaped(weights[0].shape[0], sum(w.shape[1] for w in weights), dtype=BF16),
         ),
-        in_specs=[pl.BlockSpec(memory_space=pltpu.SMEM), *[whole] * 9],
-        scratch_shapes=drive_scratch,
+        in_specs=[pl.BlockSpec(memory_space=pltpu.SMEM), *[whole] * 6, *[stored] * 3],
+        out_specs=(whole, whole, whole, stored),
+        scratch_shapes=[*drive_scratch, pltpu.SemaphoreType.DMA((3,))],
         name="ssm_ends",
     )(me, decay_real, frequency, log_row, state_input, *b, *weights)
     weight = lax.all_gather(weight, "sp", axis=0, tiled=True)
@@ -276,7 +291,14 @@
     acts = pl.pallas_call(
         finish_kernel,
         out_shape=shaped(rows, chans, dtype=BF16),
-        scratch_shapes=[pltpu.VMEM((chans // LANES, rows, LANES), F32)],
+        in_specs=[*[whole] * 4, stored, stored],
+        out_specs=whole,
+        scratch_shapes=[
+            pltpu.VMEM((chans // LANES, rows, LANES), F32),
+            pltpu.VMEM((rows, chans), F32),
+            pltpu.VMEM((rows, 2 * flat), BF16),
+            pltpu.SemaphoreType.DMA((2,)),
+        ],
         name="ssm_finish",
     )(pieces, row, *c, local, power)
     return acts, weight
@@ -292,12 +314,9 @@
 
 
 def gathered(own):
-    half = own.shape[0] // 2
-    left = ring(own, 1)
-    right = ring(own, -1)
-    far_top = ring(left[:half], 1)
-    far_low = ring(right[half:], -1)
-    return own, left, right, jnp.concatenate([far_top, far_low], axis=0)
+    left, right = ring(own, 1), ring(own, -1)
+    far = ring(own, 2)
+    return own, left, right, far
 
 
 def summed(far, right, left, own):
@@ -328,7 +347,7 @@
         read_real, read_imag, skip_gain, (mlp_gate, mlp_up, mlp_down.T),
     )
     both, down_weight = weight[:, : 2 * hidden_width], weight[:, 2 * hidden_width :]
-    places = dict(zip((0, 3, 1, 2), (acts, ring(acts, 1), ring(acts, -1), ring(acts, 2))))
+    places = dict(zip((0, 3, 1, 2), gathered(acts)))
 
     def project(w):
         total = None
@@ -360,10 +379,9 @@
         hidden = (jax.nn.silu(hidden[:, :hidden_width]) * hidden[:, hidden_width:]).astype(BF16)
         return lax.dot_general(hidden, down_weight, NT, preferred_element_type=F32)
 
-    near = feed(own)
     sides = feed(jnp.concatenate([left, right], axis=0))
     sides = lax.optimization_barrier(sides)
-    down = summed(feed(far), sides[owned:], sides[:owned], near)
+    down = summed(feed(far), sides[owned:], sides[:owned], feed(own))
     return (inner + 0.5 * down).astype(BF16)
 
 

time: 154 us -> 166 us (1.078)
  Pallas kernels: 14.7 us -> 22.8 us
  waiting for transfers between devices: 48.8 us -> 55.7 us
  starting transfers between devices: 54.8 us -> 49.7 us
  matrix products: 16.6 us -> 18.9 us
    pallas_call x1, Pallas kernels: 4.43 us -> 12 us  [activations(): pl.pallas_call(ends_kernel, out_shape=(shaped(peers, 2 * flat // LANES, L...]
    ppermute x19 -> x18, waiting for transfers between devices: 38.1 us -> 44.8 us  [ring(): lax.ppermute(array, 'tp', [(i, (i + by) % peers) for i in range(peers)])]
    ppermute x19 -> x18, starting transfers between devices: 30.1 us -> 25 us  [ring(): lax.ppermute(array, 'tp', [(i, (i + by) % peers) for i in range(peers)])]
    dot_general x3, matrix products: 6.77 us -> 9.16 us  [feed(): hidden = jnp.dot(rows, both, preferred_element_type=F32)]
  transfers between devices with their start and end apart: 21 -> 20, of which waited for: 13 -> 11; matrix products, arithmetic and copies ran while one was open for 8% -> 11% of each run, Pallas kernels for 7% -> 7%
where the time goes in v2:
time: 166 us
  waiting for transfers between devices  55.7 us (34%)
  starting transfers between devices  49.7 us (30%)
  Pallas kernels  22.8 us (14%)
  matrix products  18.9 us (11%)
  between operations  13.9 us (8%)
  other arithmetic  2.94 us (2%)
  local copies, waits for them, and re-layouts  1.87 us (1%)
    ppermute x18, waiting for transfers between devices, ring(): lax.ppermute(array, 'tp', [(i, (i + by) % peers) for i in range(peers)])  44.8 us
    ppermute x18, starting transfers between devices, ring(): lax.ppermute(array, 'tp', [(i, (i + by) % peers) for i in range(peers)])  25 us
    all_to_all x1, starting transfers between devices, activations(): pieces = lax.all_to_all(end, 'sp', 0, 0, tiled=True)  24.8 us
    pallas_call x1, Pallas kernels, activations(): pl.pallas_call(ends_kernel, out_shape=(shaped(peers, 2 * flat // LANES, L...  12 us
    all_to_all x1, waiting for transfers between devices, activations(): pieces = lax.all_to_all(end, 'sp', 0, 0, tiled=True)  10.8 us
    dot_general x3, matrix products, feed(): hidden = jnp.dot(rows, both, preferred_element_type=F32)  9.16 us
    pallas_call x1, Pallas kernels, activations(): pl.pallas_call(local_kernel, out_shape=(shaped(rows, chans), shaped(rows,...  6.13 us
    dot_general x8, matrix products, project(): jnp.dot(rows, rows_at(w, (me + place) % peers, chans), preferred_element_...  4.7 us
  transfers between devices with their start and end apart: 20, of which 11 were waited for; matrix products, arithmetic and copies ran while one was open for 11% of the time, Pallas kernels for 7%

profile of v2, /device:TPU:40, one launch (start us, length us, event | category | flops | bytes accessed | tf_op | source)
XLA Modules:
  0.0 165.9 jit_solution(12062248506572475027)
XLA Ops:
  6.6 12.0 %ssm_ends.1 = (bf16[32,16,128]{2,1,0:T(8,128)(2,1)}, f32[2,8,1024]{2,1,0:T(8,128)}, f32[4,1024]{1,0:T(4,128)}, bf16[64,2304]{1,0:T(8,128)(2,1)}) custom-call(s32[1]{0:T(128)} %bitcast.me_ref, f32[16,64]{1,0:T(8,128)} %decay_ref.1, f32[16,64]{1,0:T(8,128)} %freq_ref.1, f32[1,16]{1,0:T(1,128)} %bitcast.35, bf16[512,256]{1,0:T(8,128)(2,1)} %x_ref.3, ...), custom_call_target="tpu_custom_call" | custom-call | tf_op jit(solution)/shard_map/ssm_ends/pallas_call | solution.py:263
  18.6 24.8 %all-to-all-start = ((bf16[32,16,128]{2,1,0:T(8,128)(2,1)}), bf16[32,16,128]{2,1,0:T(8,128)(2,1)S(1)}, u32[]{:S(2)}, u32[]{:S(2)}) async-start(bf16[32,16,128]{2,1,0:T(8,128)(2,1)} %get-tuple-element.11), calls=%async_computation | async-start | bytes 262144 | tf_op jit(solution)/shard_map/all_to_all | solution.py:277
  43.5 6.1 %ssm_local.1 = (f32[512,256]{1,0:T(8,128)}, bf16[512,2048]{1,0:T(8,128)(2,1)}) custom-call(f32[4,1024]{1,0:T(4,128)} %get-tuple-element.12.row_ref, f32[2,8,1024]{2,1,0:T(8,128)} %get-tuple-element.13.seg_ref, bf16[512,256]{1,0:T(8,128)(2,1)} %x_ref.3, f32[256,64]{1,0:T(8,128)} %bitcast.27, f32[256,64]{1,0:T(8,128)} %bitcast.29, f32[256,64]{1,0:T(8,128)} %bitcast.30, ...), custom_call_target="tpu_custom_call" | custom-call | flops 1073741824 | bytes 4194304 | tf_op jit(solution)/shard_map/ssm_local/pallas_call | solution.py:278
  49.6 10.8 %all-to-all-done.piece_ref = bf16[32,16,128]{2,1,0:T(8,128)(2,1)S(1)} async-done(((bf16[32,16,128]{2,1,0:T(8,128)(2,1)}), bf16[32,16,128]{2,1,0:T(8,128)(2,1)S(1)}, u32[]{:S(2)}, u32[]{:S(2)}) %all-to-all-start) | async-done | bytes 131104 | tf_op jit(solution)/shard_map/all_to_all | solution.py:277
  61.0 4.7 %ssm_finish.1 = bf16[512,256]{1,0:T(8,128)(2,1)} custom-call(bf16[32,16,128]{2,1,0:T(8,128)(2,1)} %copy-done.5, f32[4,1024]{1,0:T(4,128)} %get-tuple-element.12.row_ref, f32[256,64]{1,0:T(8,128)} %bitcast.31, f32[256,64]{1,0:T(8,128)} %bitcast.33, f32[512,256]{1,0:T(8,128)} %get-tuple-element.14.local_ref, bf16[512,2048]{1,0:T(8,128)(2,1)} %get-tuple-element.15.powers_ref), custom_call_target="tpu_custom_call" | custom-call | tf_op jit(solution)/shard_map/ssm_finish/pallas_call | solution.py:291
  65.7 1.8 %collective-permute-start = (bf16[512,256]{1,0:T(8,128)(2,1)}, bf16[512,256]{1,0:T(8,128)(2,1)S(1)}, u32[]{:S(2)}, u32[]{:S(2)}) collective-permute-start(bf16[512,256]{1,0:T(8,128)(2,1)} %ssm_finish.1), channel_id=1, source_target_pairs={{0,1},{1,2},{2,3},{3,0},{4,5},{5,6},{6,7},{7,4},{8,9},{9,10},{10,1... | collective-permute-start | bytes 786440 | tf_op jit(solution)/shard_map/ppermute | solution.py:309
  67.5 3.0 %collective-permute-start.2 = (bf16[512,256]{1,0:T(8,128)(2,1)}, bf16[512,256]{1,0:T(8,128)(2,1)S(1)}, u32[]{:S(2)}, u32[]{:S(2)}) collective-permute-start(bf16[512,256]{1,0:T(8,128)(2,1)} %ssm_finish.1), channel_id=1, source_target_pairs={{0,2},{1,3},{2,0},{3,1},{4,6},{5,7},{6,4},{7,5},{8,10},{9,11},{10,... | collective-permute-start | bytes 786440 | tf_op jit(solution)/shard_map/ppermute | solution.py:309
  70.5 1.3 collective-permute-start.1
  71.8 1.4 fusion.48
  73.2 1.2 fusion.42
  74.4 1.1 collective-permute-done
  76.2 5.2 %collective-permute-done.2 = bf16[512,256]{1,0:T(8,128)(2,1)S(1)} collective-permute-done((bf16[512,256]{1,0:T(8,128)(2,1)}, bf16[512,256]{1,0:T(8,128)(2,1)S(1)}, u32[]{:S(2)}, u32[]{:S(2)}) %collective-permute-start.2) | collective-permute-done | bytes 262176 | tf_op jit(solution)/shard_map/ppermute | solution.py:309
  83.7 1.4 collective-permute-start.7
  86.3 2.7 %collective-permute-start.3 = (bf16[64,2048]{1,0:T(8,128)(2,1)S(1)}, bf16[64,2048]{1,0:T(8,128)(2,1)S(1)}, u32[]{:S(2)}, u32[]{:S(2)}) collective-permute-start(bf16[64,2048]{1,0:T(8,128)(2,1)S(1)} %slice.187), channel_id=1, source_target_pairs={{0,3},{1,0},{2,1},{3,2},{4,7},{5,4},{6,5},{7,6},{8,11},{9,8},{10,9... | collective-permute-start | bytes 786440 | tf_op jit(solution)/shard_map/ppermute | solution.py:309
  89.6 3.1 %collective-permute-done.7 = bf16[64,2048]{1,0:T(8,128)(2,1)S(1)} collective-permute-done((bf16[64,2048]{1,0:T(8,128)(2,1)S(1)}, bf16[64,2048]{1,0:T(8,128)(2,1)S(1)}, u32[]{:S(2)}, u32[]{:S(2)}) %collective-permute-start.7) | collective-permute-done | bytes 262176 | tf_op jit(solution)/shard_map/ppermute | solution.py:309
  92.8 2.9 %collective-permute-start.8 = (bf16[64,2048]{1,0:T(8,128)(2,1)S(1)}, bf16[64,2048]{1,0:T(8,128)(2,1)S(1)}, u32[]{:S(2)}, u32[]{:S(2)}) collective-permute-start(bf16[64,2048]{1,0:T(8,128)(2,1)S(1)} %fusion.30), channel_id=1, source_target_pairs={{0,3},{1,0},{2,1},{3,2},{4,7},{5,4},{6,5},{7,6},{8,11},{9,8},{10,9... | collective-permute-start | bytes 786440 | tf_op jit(solution)/shard_map/ppermute | solution.py:309
  96.3 2.0 %collective-permute-done.3 = bf16[64,2048]{1,0:T(8,128)(2,1)S(1)} collective-permute-done((bf16[64,2048]{1,0:T(8,128)(2,1)S(1)}, bf16[64,2048]{1,0:T(8,128)(2,1)S(1)}, u32[]{:S(2)}, u32[]{:S(2)}) %collective-permute-start.3) | collective-permute-done | bytes 262176 | tf_op jit(solution)/shard_map/ppermute | solution.py:309
  98.3 2.8 %collective-permute-done.6 = bf16[64,2048]{1,0:T(8,128)(2,1)S(1)} collective-permute-done((bf16[64,2048]{1,0:T(8,128)(2,1)S(1)}, bf16[64,2048]{1,0:T(8,128)(2,1)S(1)}, u32[]{:S(2)}, u32[]{:S(2)}) %collective-permute-start.6) | collective-permute-done | bytes 262176 | tf_op jit(solution)/shard_map/ppermute | solution.py:309
  101.7 3.4 %collective-permute-done.5 = bf16[64,2048]{1,0:T(8,128)(2,1)S(1)} collective-permute-done((bf16[64,2048]{1,0:T(8,128)(2,1)S(1)}, bf16[64,2048]{1,0:T(8,128)(2,1)S(1)}, u32[]{:S(2)}, u32[]{:S(2)}) %collective-permute-start.5) | collective-permute-done | bytes 262176 | tf_op jit(solution)/shard_map/ppermute | solution.py:309
  106.9 1.7 %collective-permute-start.9 = (bf16[128,2048]{1,0:T(8,128)(2,1)}, bf16[128,2048]{1,0:T(8,128)(2,1)}, u32[]{:S(2)}, u32[]{:S(2)}) collective-permute-start(bf16[128,2048]{1,0:T(8,128)(2,1)} %multiply_convert_fusion), channel_id=1, source_target_pairs={{0,1},{1,2},{2,3},{3,0},{4,5},{5,6},{6,7},{7,4},{8,9},{9,10},{10,1... | collective-permute-start | bytes 1572872 | tf_op jit(solution)/shard_map/ppermute | solution.py:309
  108.6 13.1 %collective-permute-done.10 = bf16[128,2048]{1,0:T(8,128)(2,1)} collective-permute-done((bf16[128,2048]{1,0:T(8,128)(2,1)}, bf16[128,2048]{1,0:T(8,128)(2,1)}, u32[]{:S(2)}, u32[]{:S(2)}) %collective-permute-start.10) | collective-permute-done | bytes 524320 | tf_op jit(solution)/shard_map/ppermute | solution.py:309
  121.7 10.4 %collective-permute-done.9 = bf16[128,2048]{1,0:T(8,128)(2,1)} collective-permute-done((bf16[128,2048]{1,0:T(8,128)(2,1)}, bf16[128,2048]{1,0:T(8,128)(2,1)}, u32[]{:S(2)}, u32[]{:S(2)}) %collective-permute-start.9) | collective-permute-done | bytes 524320 | tf_op jit(solution)/shard_map/ppermute | solution.py:309
  132.1 5.0 %fusion.2 = f32[256,1536]{1,0:T(8,128)S(1)} fusion(bf16[2048,2304]{1,0:T(8,128)(2,1)} %all-gather.2.cloned.1.call-done, bf16[128,2048]{1,0:T(8,128)(2,1)} %collective-permute-done.10, bf16[128,2048]{1,0:T(8,128)(2,1)} %collective-permute-done.9), kind=kOutput, calls=%fused_computation.2 | convolution fusion | flops 1612709888 | bytes 8912896 | tf_op jit(solution)/shard_map/dot_general | solution.py:378
  137.9 1.0 fusion.7
  138.9 2.1 %fusion = f32[128,1536]{1,0:T(8,128)S(1)} fusion(bf16[128,2048]{1,0:T(8,128)(2,1)} %collective-permute-done.12, bf16[2048,2304]{1,0:T(8,128)(2,1)S(1)} %copy-done.7), kind=kOutput, calls=%fused_computation | convolution fusion | flops 805306368 | bytes 7602176 | tf_op jit(solution)/shard_map/dot_general | solution.py:378
  141.0 1.1 convolution_convert_fusion
  142.4 3.2 %collective-permute-start.16 = (bf16[64,2048]{1,0:T(8,128)(2,1)S(1)}, bf16[64,2048]{1,0:T(8,128)(2,1)S(1)}, u32[]{:S(2)}, u32[]{:S(2)}) collective-permute-start(bf16[64,2048]{1,0:T(8,128)(2,1)S(1)} %get-tuple-element.26), channel_id=1, source_target_pairs={{0,3},{1,0},{2,1},{3,2},{4,7},{5,4},{6,5},{7,6},{8,11},{9,8},{10,9... | collective-permute-start | bytes 786440 | tf_op jit(solution)/shard_map/ppermute | solution.py:309
  145.9 2.0 %collective-permute-start.15 = (bf16[64,2048]{1,0:T(8,128)(2,1)S(1)}, bf16[64,2048]{1,0:T(8,128)(2,1)S(1)}, u32[]{:S(2)}, u32[]{:S(2)}) collective-permute-start(bf16[64,2048]{1,0:T(8,128)(2,1)S(1)} %get-tuple-element.22), channel_id=1, source_target_pairs={{0,1},{1,2},{2,3},{3,0},{4,5},{5,6},{6,7},{7,4},{8,9},{9,10},{10,1... | collective-permute-start | bytes 786440 | tf_op jit(solution)/shard_map/ppermute | solution.py:309
  147.9 2.1 %fusion.4 = f32[128,1536]{1,0:T(8,128)S(1)} fusion(bf16[128,2048]{1,0:T(8,128)(2,1)} %multiply_convert_fusion, bf16[2048,2304]{1,0:T(8,128)(2,1)S(1)} %copy-done.7), kind=kOutput, calls=%fused_computation.4 | convolution fusion | flops 805306368 | bytes 7602176 | tf_op jit(solution)/shard_map/dot_general | solution.py:378
  150.3 3.3 %collective-permute-start.17 = (bf16[64,2048]{1,0:T(8,128)(2,1)S(1)}, bf16[64,2048]{1,0:T(8,128)(2,1)S(1)}, u32[]{:S(2)}, u32[]{:S(2)}) collective-permute-start(bf16[64,2048]{1,0:T(8,128)(2,1)S(1)} %get-tuple-element.18), channel_id=1, source_target_pairs={{0,3},{1,0},{2,1},{3,2},{4,7},{5,4},{6,5},{7,6},{8,11},{9,8},{10,9... | collective-permute-start | bytes 786440 | tf_op jit(solution)/shard_map/ppermute | solution.py:309
  153.5 1.1 fusion.9
  154.7 3.1 %collective-permute-done.14 = bf16[64,2048]{1,0:T(8,128)(2,1)S(1)} collective-permute-done((bf16[64,2048]{1,0:T(8,128)(2,1)S(1)}, bf16[64,2048]{1,0:T(8,128)(2,1)S(1)}, u32[]{:S(2)}, u32[]{:S(2)}) %collective-permute-start.14) | collective-permute-done | bytes 262176 | tf_op jit(solution)/shard_map/ppermute | solution.py:309
  (63 shorter events, 11.0 us)
Async XLA Ops:
  6.5 76.6 %copy-start = (bf16[512,2048]{1,0:T(8,128)(2,1)S(1)}, bf16[512,2048]{1,0:T(8,128)(2,1)}, u32[]{:S(2)}) copy-start(bf16[512,2048]{1,0:T(8,128)(2,1)} %param.31) | copy-start | bytes 6291460
  6.6 125.6 %all-gather.2.cloned.1.call-start = ((), (), s32[]{:S(2)}) async-start(), calls=%async_computation.1 | async-start | bytes 9732096 | tf_op jit(solution)/shard_map/all_gather | solution.py:276
  18.6 41.7 %all-to-all-start = ((bf16[32,16,128]{2,1,0:T(8,128)(2,1)}), bf16[32,16,128]{2,1,0:T(8,128)(2,1)S(1)}, u32[]{:S(2)}, u32[]{:S(2)}) async-start(bf16[32,16,128]{2,1,0:T(8,128)(2,1)} %get-tuple-element.11), calls=%async_computation | async-start | bytes 262144 | tf_op jit(solution)/shard_map/all_to_all | solution.py:277
  49.6 23.6 %copy-start.3 = (bf16[1024,512]{1,0:T(8,128)(2,1)S(1)}, bf16[1024,512]{1,0:T(8,128)(2,1)}, u32[]{:S(2)}) copy-start(bf16[1024,512]{1,0:T(8,128)(2,1)} %param.30) | copy-start | bytes 3145732
  60.4 0.6 copy-start.5
  65.7 9.9 %copy-start.4 = (bf16[1024,512]{1,0:T(8,128)(2,1)S(1)}, bf16[1024,512]{1,0:T(8,128)(2,1)}, u32[]{:S(2)}) copy-start(bf16[1024,512]{1,0:T(8,128)(2,1)} %param.29) | copy-start | bytes 3145732
  65.7 9.8 %collective-permute-start = (bf16[512,256]{1,0:T(8,128)(2,1)}, bf16[512,256]{1,0:T(8,128)(2,1)S(1)}, u32[]{:S(2)}, u32[]{:S(2)}) collective-permute-start(bf16[512,256]{1,0:T(8,128)(2,1)} %ssm_finish.1), channel_id=1, source_target_pairs={{0,1},{1,2},{2,3},{3,0},{4,5},{5,6},{6,7},{7,4},{8,9},{9,10},{10,1... | collective-permute-start | bytes 786440 | tf_op jit(solution)/shard_map/ppermute | solution.py:309
  67.5 13.8 %collective-permute-start.2 = (bf16[512,256]{1,0:T(8,128)(2,1)}, bf16[512,256]{1,0:T(8,128)(2,1)S(1)}, u32[]{:S(2)}, u32[]{:S(2)}) collective-permute-start(bf16[512,256]{1,0:T(8,128)(2,1)} %ssm_finish.1), channel_id=1, source_target_pairs={{0,2},{1,3},{2,0},{3,1},{4,6},{5,7},{6,4},{7,5},{8,10},{9,11},{10,... | collective-permute-start | bytes 786440 | tf_op jit(solution)/shard_map/ppermute | solution.py:309
  70.5 11.4 %collective-permute-start.1 = (bf16[512,256]{1,0:T(8,128)(2,1)}, bf16[512,256]{1,0:T(8,128)(2,1)S(1)}, u32[]{:S(2)}, u32[]{:S(2)}) collective-permute-start(bf16[512,256]{1,0:T(8,128)(2,1)} %ssm_finish.1), channel_id=1, source_target_pairs={{0,3},{1,0},{2,1},{3,2},{4,7},{5,4},{6,5},{7,6},{8,11},{9,8},{10,9... | collective-permute-start | bytes 786440 | tf_op jit(solution)/shard_map/ppermute | solution.py:309
  81.6 1.1 copy-start.8
  83.7 9.0 %collective-permute-start.7 = (bf16[64,2048]{1,0:T(8,128)(2,1)S(1)}, bf16[64,2048]{1,0:T(8,128)(2,1)S(1)}, u32[]{:S(2)}, u32[]{:S(2)}) collective-permute-start(bf16[64,2048]{1,0:T(8,128)(2,1)S(1)} %get-tuple-element.28), channel_id=1, source_target_pairs={{0,3},{1,0},{2,1},{3,2},{4,7},{5,4},{6,5},{7,6},{8,11},{9,8},{10,9... | collective-permute-start | bytes 786440 | tf_op jit(solution)/shard_map/ppermute | solution.py:309
  85.1 10.6 %collective-permute-start.4 = (bf16[64,2048]{1,0:T(8,128)(2,1)S(1)}, bf16[64,2048]{1,0:T(8,128)(2,1)S(1)}, u32[]{:S(2)}, u32[]{:S(2)}) collective-permute-start(bf16[64,2048]{1,0:T(8,128)(2,1)S(1)} %get-tuple-element.27), channel_id=1, source_target_pairs={{0,1},{1,2},{2,3},{3,0},{4,5},{5,6},{6,7},{7,4},{8,9},{9,10},{10,1... | collective-permute-start | bytes 786440 | tf_op jit(solution)/shard_map/ppermute | solution.py:309
  86.3 12.0 %collective-permute-start.3 = (bf16[64,2048]{1,0:T(8,128)(2,1)S(1)}, bf16[64,2048]{1,0:T(8,128)(2,1)S(1)}, u32[]{:S(2)}, u32[]{:S(2)}) collective-permute-start(bf16[64,2048]{1,0:T(8,128)(2,1)S(1)} %slice.187), channel_id=1, source_target_pairs={{0,3},{1,0},{2,1},{3,2},{4,7},{5,4},{6,5},{7,6},{8,11},{9,8},{10,9... | collective-permute-start | bytes 786440 | tf_op jit(solution)/shard_map/ppermute | solution.py:309
  89.4 11.7 %collective-permute-start.6 = (bf16[64,2048]{1,0:T(8,128)(2,1)S(1)}, bf16[64,2048]{1,0:T(8,128)(2,1)S(1)}, u32[]{:S(2)}, u32[]{:S(2)}) collective-permute-start(bf16[64,2048]{1,0:T(8,128)(2,1)S(1)} %slice.186), channel_id=1, source_target_pairs={{0,1},{1,2},{2,3},{3,0},{4,5},{5,6},{6,7},{7,4},{8,9},{9,10},{10,1... | collective-permute-start | bytes 786440 | tf_op jit(solution)/shard_map/ppermute | solution.py:309
  92.8 9.0 %collective-permute-start.8 = (bf16[64,2048]{1,0:T(8,128)(2,1)S(1)}, bf16[64,2048]{1,0:T(8,128)(2,1)S(1)}, u32[]{:S(2)}, u32[]{:S(2)}) collective-permute-start(bf16[64,2048]{1,0:T(8,128)(2,1)S(1)} %fusion.30), channel_id=1, source_target_pairs={{0,3},{1,0},{2,1},{3,2},{4,7},{5,4},{6,5},{7,6},{8,11},{9,8},{10,9... | collective-permute-start | bytes 786440 | tf_op jit(solution)/shard_map/ppermute | solution.py:309
  95.7 9.6 %copy-start.1 = (bf16[128,2048]{1,0:T(8,128)(2,1)S(1)}, bf16[128,2048]{1,0:T(8,128)(2,1)}, u32[]{:S(2)}) copy-start(bf16[128,2048]{1,0:T(8,128)(2,1)} %param.18) | copy-start | bytes 1572868
  95.7 9.4 %collective-permute-start.5 = (bf16[64,2048]{1,0:T(8,128)(2,1)S(1)}, bf16[64,2048]{1,0:T(8,128)(2,1)S(1)}, u32[]{:S(2)}, u32[]{:S(2)}) collective-permute-start(bf16[64,2048]{1,0:T(8,128)(2,1)S(1)} %fusion.32), channel_id=1, source_target_pairs={{0,1},{1,2},{2,3},{3,0},{4,5},{5,6},{6,7},{7,4},{8,9},{9,10},{10,1... | collective-permute-start | bytes 786440 | tf_op jit(solution)/shard_map/ppermute | solution.py:309
  96.3 9.3 %copy-start.6 = (f32[2048]{0:T(1024)S(1)}, f32[2048]{0:T(1024)}, u32[]{:S(2)}) copy-start(f32[2048]{0:T(1024)} %param.32) | copy-start | bytes 24580
  106.6 15.1 %collective-permute-start.10 = (bf16[128,2048]{1,0:T(8,128)(2,1)}, bf16[128,2048]{1,0:T(8,128)(2,1)}, u32[]{:S(2)}, u32[]{:S(2)}) collective-permute-start(bf16[128,2048]{1,0:T(8,128)(2,1)} %multiply_convert_fusion), channel_id=1, source_target_pairs={{0,3},{1,0},{2,1},{3,2},{4,7},{5,4},{6,5},{7,6},{8,11},{9,8},{10,9... | collective-permute-start | bytes 1572872 | tf_op jit(solution)/shard_map/ppermute | solution.py:309
  106.9 25.2 %collective-permute-start.9 = (bf16[128,2048]{1,0:T(8,128)(2,1)}, bf16[128,2048]{1,0:T(8,128)(2,1)}, u32[]{:S(2)}, u32[]{:S(2)}) collective-permute-start(bf16[128,2048]{1,0:T(8,128)(2,1)} %multiply_convert_fusion), channel_id=1, source_target_pairs={{0,1},{1,2},{2,3},{3,0},{4,5},{5,6},{6,7},{7,4},{8,9},{9,10},{10,1... | collective-permute-start | bytes 1572872 | tf_op jit(solution)/shard_map/ppermute | solution.py:309
  108.6 30.3 %collective-permute-start.12 = (bf16[128,2048]{1,0:T(8,128)(2,1)}, bf16[128,2048]{1,0:T(8,128)(2,1)}, u32[]{:S(2)}, u32[]{:S(2)}) collective-permute-start(bf16[128,2048]{1,0:T(8,128)(2,1)} %multiply_convert_fusion), channel_id=1, source_target_pairs={{0,2},{1,3},{2,0},{3,1},{4,6},{5,7},{6,4},{7,5},{8,10},{9,11},{10,... | collective-permute-start | bytes 1572872 | tf_op jit(solution)/shard_map/ppermute | solution.py:309
  132.1 5.8 %copy-start.7 = (bf16[2048,2304]{1,0:T(8,128)(2,1)S(1)}, bf16[2048,2304]{1,0:T(8,128)(2,1)}, u32[]{:S(2)}) copy-start(bf16[2048,2304]{1,0:T(8,128)(2,1)} %all-gather.2.cloned.1.call-done) | copy-start | bytes 28311556
  142.2 7.8 %collective-permute-start.13 = (bf16[64,2048]{1,0:T(8,128)(2,1)S(1)}, bf16[64,2048]{1,0:T(8,128)(2,1)S(1)}, u32[]{:S(2)}, u32[]{:S(2)}) collective-permute-start(bf16[64,2048]{1,0:T(8,128)(2,1)S(1)} %get-tuple-element.25), channel_id=1, source_target_pairs={{0,1},{1,2},{2,3},{3,0},{4,5},{5,6},{6,7},{7,4},{8,9},{9,10},{10,1... | collective-permute-start | bytes 786440 | tf_op jit(solution)/shard_map/ppermute | solution.py:309
  142.4 7.6 %collective-permute-start.16 = (bf16[64,2048]{1,0:T(8,128)(2,1)S(1)}, bf16[64,2048]{1,0:T(8,128)(2,1)S(1)}, u32[]{:S(2)}, u32[]{:S(2)}) collective-permute-start(bf16[64,2048]{1,0:T(8,128)(2,1)S(1)} %get-tuple-element.26), channel_id=1, source_target_pairs={{0,3},{1,0},{2,1},{3,2},{4,7},{5,4},{6,5},{7,6},{8,11},{9,8},{10,9... | collective-permute-start | bytes 786440 | tf_op jit(solution)/shard_map/ppermute | solution.py:309
  145.8 8.9 %collective-permute-start.11 = (bf16[64,2048]{1,0:T(8,128)(2,1)S(1)}, bf16[64,2048]{1,0:T(8,128)(2,1)S(1)}, u32[]{:S(2)}, u32[]{:S(2)}) collective-permute-start(bf16[64,2048]{1,0:T(8,128)(2,1)S(1)} %get-tuple-element.21), channel_id=1, source_target_pairs={{0,3},{1,0},{2,1},{3,2},{4,7},{5,4},{6,5},{7,6},{8,11},{9,8},{10,9... | collective-permute-start | bytes 786440 | tf_op jit(solution)/shard_map/ppermute | solution.py:309
  145.9 8.8 %collective-permute-start.15 = (bf16[64,2048]{1,0:T(8,128)(2,1)S(1)}, bf16[64,2048]{1,0:T(8,128)(2,1)S(1)}, u32[]{:S(2)}, u32[]{:S(2)}) collective-permute-start(bf16[64,2048]{1,0:T(8,128)(2,1)S(1)} %get-tuple-element.22), channel_id=1, source_target_pairs={{0,1},{1,2},{2,3},{3,0},{4,5},{5,6},{6,7},{7,4},{8,9},{9,10},{10,1... | collective-permute-start | bytes 786440 | tf_op jit(solution)/shard_map/ppermute | solution.py:309
  150.1 7.7 %collective-permute-start.14 = (bf16[64,2048]{1,0:T(8,128)(2,1)S(1)}, bf16[64,2048]{1,0:T(8,128)(2,1)S(1)}, u32[]{:S(2)}, u32[]{:S(2)}) collective-permute-start(bf16[64,2048]{1,0:T(8,128)(2,1)S(1)} %get-tuple-element.17), channel_id=1, source_target_pairs={{0,1},{1,2},{2,3},{3,0},{4,5},{5,6},{6,7},{7,4},{8,9},{9,10},{10,1... | collective-permute-start | bytes 786440 | tf_op jit(solution)/shard_map/ppermute | solution.py:309
  150.3 7.8 %copy-start.2 = (bf16[128,2048]{1,0:T(8,128)(2,1)S(1)}, bf16[128,2048]{1,0:T(8,128)(2,1)}, u32[]{:S(2)}) copy-start(bf16[128,2048]{1,0:T(8,128)(2,1)} %param.18) | copy-start | bytes 1572868
  150.3 7.5 %collective-permute-start.17 = (bf16[64,2048]{1,0:T(8,128)(2,1)S(1)}, bf16[64,2048]{1,0:T(8,128)(2,1)S(1)}, u32[]{:S(2)}, u32[]{:S(2)}) collective-permute-start(bf16[64,2048]{1,0:T(8,128)(2,1)S(1)} %get-tuple-element.18), channel_id=1, source_target_pairs={{0,3},{1,0},{2,1},{3,2},{4,7},{5,4},{6,5},{7,6},{8,11},{9,8},{10,9... | collective-permute-start | bytes 786440 | tf_op jit(solution)/shard_map/ppermute | solution.py:309
Sparse Core Ops, SparseCore 0:
  18.7 92.8 all-gather.1

commit v3 on v1

--- a/solution.py
+++ b/solution.py
@@ -8,6 +8,7 @@
 EPSILON = 1e-06
 SEGMENTS = 8
 LANES = 128
+PART = 32
 F32 = jnp.float32
 BF16 = jnp.bfloat16
 NT = (((1,), (1,)), ((), ()))
@@ -69,7 +70,7 @@
     return (as_row(bar[0]), as_row(bar[1])), (as_row(ratio[0]), as_row(ratio[1]))
 
 
-def fill_drive(x_ref, b_re_ref, b_im_ref, xf_ref, xp_ref, d_re_ref, d_im_ref):
+def fill_drive(x_ref, b_re_ref, b_im_ref, xf_ref, xp_ref, d_re_ref, d_im_ref, wide_ref):
     rows, chans = x_ref.shape
     states = b_re_ref.shape[1]
     flat = d_re_ref.shape[1]
@@ -86,25 +87,36 @@
 
         lax.fori_loop(0, length, permute, 0, unroll=8)
     x = xp_ref[...].astype(BF16)
-    shape = (chans, flat)
-    own = iota(shape, 0) >> bits(chans // groups) == iota(shape, 1) >> bits(states)
     for b_ref, d_ref in ((b_re_ref, d_re_ref), (b_im_ref, d_im_ref)):
-        wide = jnp.where(own, along_lanes(b_ref[...], groups), 0.0).astype(BF16)
-        d_ref[...] = jnp.dot(x, wide, preferred_element_type=F32)
-
-
-def wide_read(c_re_ref, c_im_ref, factor):
+
+        def widen(i, _, b_ref=b_ref):
+            at = pl.ds(pl.multiple_of(i * PART, PART), PART)
+            wide = along_lanes(b_ref[at, :], groups)
+            own = (iota(wide.shape, 0) + i * PART) >> bits(chans // groups)
+            own = own == iota(wide.shape, 1) >> bits(states)
+            wide_ref[at, :] = jnp.where(own, wide, 0.0).astype(BF16)
+            return 0
+
+        lax.fori_loop(0, chans // PART, widen, 0)
+        d_ref[...] = jnp.dot(x, wide_ref[...], preferred_element_type=F32)
+
+
+def wide_read(c_re_ref, c_im_ref, factor, read_ref):
     chans, states = c_re_ref.shape
     flat = factor[0].shape[1]
     groups = flat // states
     width = chans // groups
-    shape = (chans, flat)
-    own = iota(shape, 0) >> bits(width) == iota(shape, 1) >> bits(states)
-    c = along_lanes(c_re_ref[...], groups), along_lanes(c_im_ref[...], groups)
-    re, im = times(c, factor)
-    return jnp.concatenate(
-        [jnp.where(own, re, 0.0).astype(BF16), jnp.where(own, -im, 0.0).astype(BF16)], axis=1
-    )
+
+    def widen(i, _):
+        at = pl.ds(pl.multiple_of(i * PART, PART), PART)
+        c = along_lanes(c_re_ref[at, :], groups), along_lanes(c_im_ref[at, :], groups)
+        re, im = times(c, factor)
+        own = (iota(re.shape, 0) + i * PART) >> bits(width) == iota(re.shape, 1) >> bits(states)
+        read_ref[at, :flat] = jnp.where(own, re, 0.0).astype(BF16)
+        read_ref[at, flat:] = jnp.where(own, -im, 0.0).astype(BF16)
+        return 0
+
+    lax.fori_loop(0, chans // PART, widen, 0)
 
 
 def as_tile(row):
@@ -121,7 +133,7 @@
     me_ref, decay_ref, freq_ref, log_step_ref, x_ref, b_re_ref, b_im_ref,
     gate_ref, up_ref, down_ref,
     end_ref, seg_ref, row_ref, weight_ref,
-    xf_ref, xp_ref, d_re_ref, d_im_ref,
+    xf_ref, xp_ref, d_re_ref, d_im_ref, wide_ref,
 ):
     rows, flat = d_re_ref.shape
     length = rows // SEGMENTS
@@ -130,7 +142,7 @@
         weight_ref[:, at : at + ref.shape[1]] = ref[...]
         at += ref.shape[1]
     bar, ratio = rates(decay_ref, freq_ref, log_step_ref)
-    fill_drive(x_ref, b_re_ref, b_im_ref, xf_ref, xp_ref, d_re_ref, d_im_ref)
+    fill_drive(x_ref, b_re_ref, b_im_ref, xf_ref, xp_ref, d_re_ref, d_im_ref, wide_ref)
     lam = tuple(jnp.broadcast_to(part, (SEGMENTS, flat)) for part in bar)
 
     def advance(j, state):
@@ -138,7 +150,7 @@
         return plus(times(lam, state), (d_re_ref[at, :], d_im_ref[at, :]))
 
     zero = jnp.zeros((SEGMENTS, flat), F32)
-    ends = lax.fori_loop(0, length, advance, (zero, zero), unroll=4)
+    ends = lax.fori_loop(0, length, advance, (zero, zero), unroll=2)
     over = squared(bar, bits(length))
     carry = jnp.zeros((1, flat), F32), jnp.zeros((1, flat), F32)
     for s in range(SEGMENTS):
@@ -161,11 +173,11 @@
 def local_kernel(
     row_ref, seg_ref, x_ref, b_re_ref, b_im_ref, c_re_ref, c_im_ref, skip_ref,
     y_ref, power_ref,
-    xf_ref, xp_ref, d_re_ref, d_im_ref, s_ref, w_ref,
+    xf_ref, xp_ref, d_re_ref, d_im_ref, wide_ref, read_ref, s_ref, w_ref,
 ):
     rows, flat = d_re_ref.shape
     length = rows // SEGMENTS
-    fill_drive(x_ref, b_re_ref, b_im_ref, xf_ref, xp_ref, d_re_ref, d_im_ref)
+    fill_drive(x_ref, b_re_ref, b_im_ref, xf_ref, xp_ref, d_re_ref, d_im_ref, wide_ref)
     bar = row_ref[0:1, :], row_ref[1:2, :]
     ratio = row_ref[2:3, :], row_ref[3:4, :]
     lam = tuple(jnp.broadcast_to(part, (SEGMENTS, flat)) for part in bar)
@@ -180,7 +192,7 @@
             s_ref[at, i * flat : (i + 1) * flat] = both.astype(BF16)
         return second
 
-    lax.fori_loop(0, length // 2, advance, (seg_ref[0], seg_ref[1]), unroll=2)
+    lax.fori_loop(0, length // 2, advance, (seg_ref[0], seg_ref[1]))
     over = squared(bar, bits(length))
     power = jnp.ones((1, flat), F32), jnp.zeros((1, flat), F32)
     for s in range(SEGMENTS):
@@ -196,23 +208,23 @@
             power_ref[at, i * flat : (i + 1) * flat] = both.astype(BF16)
         return second
 
-    lax.fori_loop(0, length // 2, raise_power, (w_ref[0], w_ref[1]), unroll=2)
-    read = wide_read(c_re_ref, c_im_ref, ratio)
-    out = lax.dot_general(s_ref[...], read, NT, preferred_element_type=F32)
+    lax.fori_loop(0, length // 2, raise_power, (w_ref[0], w_ref[1]))
+    wide_read(c_re_ref, c_im_ref, ratio, read_ref)
+    out = lax.dot_general(s_ref[...], read_ref[...], NT, preferred_element_type=F32)
     y_ref[...] = out + skip_ref[...] * xp_ref[...]
 
 
 def finish_kernel(
-    piece_ref, row_ref, c_re_ref, c_im_ref, y_ref, power_ref, out_ref, t_ref
+    piece_ref, row_ref, c_re_ref, c_im_ref, y_ref, power_ref, out_ref, t_ref, read_ref
 ):
     pieces = jnp.sum(piece_ref[...].astype(F32), axis=0)
     half = pieces.shape[0] // 2
     total = from_tile(pieces[:half]), from_tile(pieces[half:])
     ratio = row_ref[2:3, :], row_ref[3:4, :]
-    read = wide_read(c_re_ref, c_im_ref, times(ratio, total))
-    y = y_ref[...] + lax.dot_general(power_ref[...], read, NT, preferred_element_type=F32)
+    wide_read(c_re_ref, c_im_ref, times(ratio, total), read_ref)
+    y = y_ref[...] + lax.dot_general(power_ref[...], read_ref[...], NT, preferred_element_type=F32)
+    length = y.shape[0] // SEGMENTS
     y = jax.nn.gelu(y, approximate=True)
-    length = y.shape[0] // SEGMENTS
     for i in range(y.shape[1] // LANES):
         at = slice(i * LANES, (i + 1) * LANES)
         for j in range(length):
@@ -244,6 +256,7 @@
         pltpu.VMEM((rows, chans), F32),
         pltpu.VMEM((rows, flat), F32),
         pltpu.VMEM((rows, flat), F32),
+        pltpu.VMEM((chans, flat), BF16),
     ]
     whole = pl.BlockSpec(memory_space=pltpu.VMEM)
     end, seg, row, weight = pl.pallas_call(
@@ -265,6 +278,7 @@
         out_shape=(shaped(rows, chans), shaped(rows, 2 * flat, dtype=BF16)),
         scratch_shapes=[
             *drive_scratch,
+            pltpu.VMEM((chans, 2 * flat), BF16),
             pltpu.VMEM((rows, 2 * flat), BF16),
             pltpu.VMEM((2, SEGMENTS, flat), F32),
         ],
@@ -276,7 +290,10 @@
     acts = pl.pallas_call(
         finish_kernel,
         out_shape=shaped(rows, chans, dtype=BF16),
-        scratch_shapes=[pltpu.VMEM((chans // LANES, rows, LANES), F32)],
+        scratch_shapes=[
+            pltpu.VMEM((chans // LANES, rows, LANES), F32),
+            pltpu.VMEM((chans, 2 * flat), BF16),
+        ],
         name="ssm_finish",
     )(pieces, row, *c, local, power)
     return acts, weight
@@ -291,13 +308,14 @@
     return lax.dynamic_slice_in_dim(array, index * size, size, 0)
 
 
-def gathered(own):
-    half = own.shape[0] // 2
-    left = ring(own, 1)
-    right = ring(own, -1)
-    far_top = ring(left[:half], 1)
-    far_low = ring(right[half:], -1)
-    return own, left, right, jnp.concatenate([far_top, far_low], axis=0)
+def gathered(top, low):
+    left_top = ring(top, 1)
+    right_low = ring(low, -1)
+    left_low = ring(low, 1)
+    right_top = ring(top, -1)
+    far_top = ring(left_top, 1)
+    far_low = ring(right_low, -1)
+    return (left_top, left_low), (right_top, right_low), (far_top, far_low)
 
 
 def summed(far, right, left, own):
@@ -311,7 +329,19 @@
     from_right_low = ring((left[half:] + passing_down.astype(F32)).astype(BF16), -1)
     top = own[:half] + from_right_top.astype(F32) + from_left_top.astype(F32)
     low = own[half:] + from_left_low.astype(F32) + from_right_low.astype(F32)
-    return jnp.concatenate([top, low], axis=0)
+    return top, low
+
+
+def summed_late(far, right, left, own):
+    half = own.shape[0] // 2
+    far = far.astype(BF16)
+    passing_up = ring(far[:half], 1)
+    passing_down = ring(far[half:], -1)
+    right = right + jnp.pad(passing_up, ((0, half), (0, 0))).astype(F32)
+    left = left + jnp.pad(passing_down, ((half, 0), (0, 0))).astype(F32)
+    from_left, from_right = ring(right.astype(BF16), 1), ring(left.astype(BF16), -1)
+    total = own + from_left.astype(F32) + from_right.astype(F32)
+    return total[:half], total[half:]
 
 
 def shards(
@@ -328,7 +358,9 @@
         read_real, read_imag, skip_gain, (mlp_gate, mlp_up, mlp_down.T),
     )
     both, down_weight = weight[:, : 2 * hidden_width], weight[:, 2 * hidden_width :]
-    places = dict(zip((0, 3, 1, 2), (acts, ring(acts, 1), ring(acts, -1), ring(acts, 2))))
+    places = dict(
+        zip((0, 3, 1, 2), (acts, ring(acts, 1), ring(acts, -1), ring(acts, 2)))
+    )
 
     def project(w):
         total = None
@@ -350,21 +382,26 @@
 
     far = mix(2)
     branch = summed(far, mix(1), mix(3), mix(0))
-    inner = residual.astype(F32) + branch
-    scale = lax.rsqrt(jnp.mean(inner * inner, axis=-1, keepdims=True) + EPSILON)
-    normed = (inner * scale * norm_gain).astype(BF16)
-    own, left, right, far = gathered(normed)
+    half = owned // 2
+    inner, normed = [], []
+    for i, part in enumerate(branch):
+        inner.append(residual[i * half : (i + 1) * half].astype(F32) + part)
+        scale = lax.rsqrt(jnp.mean(inner[i] * inner[i], axis=-1, keepdims=True) + EPSILON)
+        normed.append((inner[i] * scale * norm_gain).astype(BF16))
+    left, right, far = gathered(*normed)
 
     def feed(rows):
         hidden = jnp.dot(rows, both, preferred_element_type=F32)
         hidden = (jax.nn.silu(hidden[:, :hidden_width]) * hidden[:, hidden_width:]).astype(BF16)
         return lax.dot_general(hidden, down_weight, NT, preferred_element_type=F32)
 
-    near = feed(own)
-    sides = feed(jnp.concatenate([left, right], axis=0))
-    sides = lax.optimization_barrier(sides)
-    down = summed(feed(far), sides[owned:], sides[:owned], near)
-    return (inner + 0.5 * down).astype(BF16)
+    sides = feed(jnp.concatenate([*left, *right], axis=0))
+    far = feed(jnp.concatenate(far, axis=0))
+    own = feed(jnp.concatenate(normed, axis=0))
+    down = summed_late(far, sides[owned:], sides[:owned], own)
+    return jnp.concatenate(
+        [(i + 0.5 * part).astype(BF16) for i, part in zip(inner, down)], axis=0
+    )
 
 
 def solution(mesh):

time: 154 us -> 155 us (level)
  waiting for transfers between devices: 48.8 us -> 40.5 us
  Pallas kernels: 14.7 us -> 19.4 us
  matrix products: 16.6 us -> 18.7 us
    ppermute x19, waiting for transfers between devices: 38.1 us -> 32.1 us  [ring(): lax.ppermute(array, 'tp', [(i, (i + by) % peers) for i in range(peers)])]
    pallas_call x1, Pallas kernels: 6.19 us -> 8.56 us  [activations(): pl.pallas_call(local_kernel, out_shape=(shaped(rows, chans), shaped(rows,...]
    all_to_all x1, waiting for transfers between devices: 10.7 us -> 8.33 us  [activations(): pieces = lax.all_to_all(end, 'sp', 0, 0, tiled=True)]
    dot_general x3, matrix products: 6.77 us -> 8.82 us  [feed(): hidden = jnp.dot(rows, both, preferred_element_type=F32)]
    unnamed x30 -> x26, local copies, waits for them, and re-layouts: 2.54 us -> 3.53 us
  transfers between devices with their start and end apart: 21 -> 21, of which waited for: 13 -> 11; matrix products, arithmetic and copies ran while one was open for 8% -> 13% of each run, Pallas kernels for 7% -> 9%
where the time goes in v3:
time: 155 us
  starting transfers between devices  55.9 us (36%)
  waiting for transfers between devices  40.5 us (26%)
  Pallas kernels  19.4 us (13%)
  matrix products  18.7 us (12%)
  between operations  13.8 us (9%)
  local copies, waits for them, and re-layouts  3.67 us (2%)
  other arithmetic  2.75 us (2%)
    ppermute x19, waiting for transfers between devices, ring(): lax.ppermute(array, 'tp', [(i, (i + by) % peers) for i in range(peers)])  32.1 us
    ppermute x19, starting transfers between devices, ring(): lax.ppermute(array, 'tp', [(i, (i + by) % peers) for i in range(peers)])  31.1 us
    all_to_all x1, starting transfers between devices, activations(): pieces = lax.all_to_all(end, 'sp', 0, 0, tiled=True)  24.8 us
    dot_general x3, matrix products, feed(): hidden = jnp.dot(rows, both, preferred_element_type=F32)  8.82 us
    pallas_call x1, Pallas kernels, activations(): pl.pallas_call(local_kernel, out_shape=(shaped(rows, chans), shaped(rows,...  8.56 us
    all_to_all x1, waiting for transfers between devices, activations(): pieces = lax.all_to_all(end, 'sp', 0, 0, tiled=True)  8.33 us
    pallas_call x1, Pallas kernels, activations(): pl.pallas_call(ends_kernel, out_shape=(shaped(peers, 2 * flat // LANES, L...  5.91 us
    pallas_call x1, Pallas kernels, activations(): pl.pallas_call(finish_kernel, out_shape=shaped(rows, chans, dtype=BF16),...  4.94 us
  transfers between devices with their start and end apart: 21, of which 11 were waited for; matrix products, arithmetic and copies ran while one was open for 13% of the time, Pallas kernels for 9%

profile of v3, /device:TPU:40, one launch (start us, length us, event | category | flops | bytes accessed | tf_op | source)
XLA Modules:
  0.0 154.7 jit_solution(14108294205977029641)
XLA Ops:
  6.6 5.9 %ssm_ends.1 = (bf16[32,16,128]{2,1,0:T(8,128)(2,1)}, f32[2,8,1024]{2,1,0:T(8,128)}, f32[4,1024]{1,0:T(4,128)}, bf16[64,2304]{1,0:T(8,128)(2,1)}) custom-call(s32[1]{0:T(128)} %bitcast.me_ref, f32[16,64]{1,0:T(8,128)} %decay_ref.1, f32[16,64]{1,0:T(8,128)} %freq_ref.1, f32[1,16]{1,0:T(1,128)} %bitcast.33, bf16[512,256]{1,0:T(8,128)(2,1)} %x_ref.3, ...), custom_call_target="tpu_custom_call" | custom-call | tf_op jit(solution)/shard_map/ssm_ends/pallas_call | solution.py:262
  12.5 24.8 %all-to-all-start = ((bf16[32,16,128]{2,1,0:T(8,128)(2,1)}), bf16[32,16,128]{2,1,0:T(8,128)(2,1)S(1)}, u32[]{:S(2)}, u32[]{:S(2)}) async-start(bf16[32,16,128]{2,1,0:T(8,128)(2,1)} %get-tuple-element.11), calls=%async_computation | async-start | bytes 262144 | tf_op jit(solution)/shard_map/all_to_all | solution.py:275
  37.4 8.6 %ssm_local.1 = (f32[512,256]{1,0:T(8,128)}, bf16[512,2048]{1,0:T(8,128)(2,1)}) custom-call(f32[4,1024]{1,0:T(4,128)} %get-tuple-element.12.row_ref, f32[2,8,1024]{2,1,0:T(8,128)} %get-tuple-element.13.seg_ref, bf16[512,256]{1,0:T(8,128)(2,1)} %x_ref.3, f32[256,64]{1,0:T(8,128)} %bitcast.25, f32[256,64]{1,0:T(8,128)} %bitcast.27, f32[256,64]{1,0:T(8,128)} %bitcast.28, ...), custom_call_target="tpu_custom_call" | custom-call | flops 1073741824 | bytes 4194304 | tf_op jit(solution)/shard_map/ssm_local/pallas_call | solution.py:276
  45.9 8.3 %all-to-all-done.piece_ref = bf16[32,16,128]{2,1,0:T(8,128)(2,1)S(1)} async-done(((bf16[32,16,128]{2,1,0:T(8,128)(2,1)}), bf16[32,16,128]{2,1,0:T(8,128)(2,1)S(1)}, u32[]{:S(2)}, u32[]{:S(2)}) %all-to-all-start) | async-done | bytes 131104 | tf_op jit(solution)/shard_map/all_to_all | solution.py:275
  54.9 4.9 %ssm_finish.1 = bf16[512,256]{1,0:T(8,128)(2,1)} custom-call(bf16[32,16,128]{2,1,0:T(8,128)(2,1)} %copy-done.3, f32[4,1024]{1,0:T(4,128)} %get-tuple-element.12.row_ref, f32[256,64]{1,0:T(8,128)} %bitcast.29, f32[256,64]{1,0:T(8,128)} %bitcast.31, f32[512,256]{1,0:T(8,128)} %get-tuple-element.14.y_ref, bf16[512,2048]{1,0:T(8,128)(2,1)} %get-tuple-element.15.power_ref), custom_call_target="tpu_custom_call" | custom-call | tf_op jit(solution)/shard_map/ssm_finish/pallas_call | solution.py:290
  59.9 3.4 %collective-permute-start.2 = (bf16[512,256]{1,0:T(8,128)(2,1)}, bf16[512,256]{1,0:T(8,128)(2,1)S(1)}, u32[]{:S(2)}, u32[]{:S(2)}) collective-permute-start(bf16[512,256]{1,0:T(8,128)(2,1)} %ssm_finish.1), channel_id=1, source_target_pairs={{0,2},{1,3},{2,0},{3,1},{4,6},{5,7},{6,4},{7,5},{8,10},{9,11},{10,... | collective-permute-start | bytes 786440 | tf_op jit(solution)/shard_map/ppermute | solution.py:304
  65.3 1.3 fusion.54
  66.6 1.4 fusion.60
  68.0 6.2 %collective-permute-done = bf16[512,256]{1,0:T(8,128)(2,1)S(1)} collective-permute-done((bf16[512,256]{1,0:T(8,128)(2,1)}, bf16[512,256]{1,0:T(8,128)(2,1)S(1)}, u32[]{:S(2)}, u32[]{:S(2)}) %collective-permute-start) | collective-permute-done | bytes 262176 | tf_op jit(solution)/shard_map/ppermute | solution.py:304
  77.5 1.9 %collective-permute-start.4 = (bf16[64,2048]{1,0:T(8,128)(2,1)S(1)}, bf16[64,2048]{1,0:T(8,128)(2,1)S(1)}, u32[]{:S(2)}, u32[]{:S(2)}) collective-permute-start(bf16[64,2048]{1,0:T(8,128)(2,1)S(1)} %get-tuple-element.29), channel_id=1, source_target_pairs={{0,1},{1,2},{2,3},{3,0},{4,5},{5,6},{6,7},{7,4},{8,9},{9,10},{10,1... | collective-permute-start | bytes 786440 | tf_op jit(solution)/shard_map/ppermute | solution.py:304
  79.4 1.4 collective-permute-start.7
  82.5 2.8 %collective-permute-start.3 = (bf16[64,2048]{1,0:T(8,128)(2,1)S(1)}, bf16[64,2048]{1,0:T(8,128)(2,1)S(1)}, u32[]{:S(2)}, u32[]{:S(2)}) collective-permute-start(bf16[64,2048]{1,0:T(8,128)(2,1)S(1)} %slice.187), channel_id=1, source_target_pairs={{0,3},{1,0},{2,1},{3,2},{4,7},{5,4},{6,5},{7,6},{8,11},{9,8},{10,9... | collective-permute-start | bytes 786440 | tf_op jit(solution)/shard_map/ppermute | solution.py:304
  85.2 2.7 %collective-permute-done.4 = bf16[64,2048]{1,0:T(8,128)(2,1)S(1)} collective-permute-done((bf16[64,2048]{1,0:T(8,128)(2,1)S(1)}, bf16[64,2048]{1,0:T(8,128)(2,1)S(1)}, u32[]{:S(2)}, u32[]{:S(2)}) %collective-permute-start.4) | collective-permute-done | bytes 262176 | tf_op jit(solution)/shard_map/ppermute | solution.py:304
  88.8 2.8 %collective-permute-start.8 = (bf16[64,2048]{1,0:T(8,128)(2,1)S(1)}, bf16[64,2048]{1,0:T(8,128)(2,1)S(1)}, u32[]{:S(2)}, u32[]{:S(2)}) collective-permute-start(bf16[64,2048]{1,0:T(8,128)(2,1)S(1)} %fusion.34), channel_id=1, source_target_pairs={{0,3},{1,0},{2,1},{3,2},{4,7},{5,4},{6,5},{7,6},{8,11},{9,8},{10,9... | collective-permute-start | bytes 786440 | tf_op jit(solution)/shard_map/ppermute | solution.py:304
  92.0 1.6 %collective-permute-done.6 = bf16[64,2048]{1,0:T(8,128)(2,1)S(1)} collective-permute-done((bf16[64,2048]{1,0:T(8,128)(2,1)S(1)}, bf16[64,2048]{1,0:T(8,128)(2,1)S(1)}, u32[]{:S(2)}, u32[]{:S(2)}) %collective-permute-start.6) | collective-permute-done | bytes 262176 | tf_op jit(solution)/shard_map/ppermute | solution.py:304
  94.2 2.9 %collective-permute-done.5 = bf16[64,2048]{1,0:T(8,128)(2,1)S(1)} collective-permute-done((bf16[64,2048]{1,0:T(8,128)(2,1)S(1)}, bf16[64,2048]{1,0:T(8,128)(2,1)S(1)}, u32[]{:S(2)}, u32[]{:S(2)}) %collective-permute-start.5) | collective-permute-done | bytes 262176 | tf_op jit(solution)/shard_map/ppermute | solution.py:304
  99.5 1.7 %collective-permute-start.9 = (bf16[64,2048]{1,0:T(8,128)(2,1)S(1)}, bf16[64,2048]{1,0:T(8,128)(2,1)S(1)}, u32[]{:S(2)}, u32[]{:S(2)}) collective-permute-start(bf16[64,2048]{1,0:T(8,128)(2,1)S(1)} %get-tuple-element.31), channel_id=1, source_target_pairs={{0,1},{1,2},{2,3},{3,0},{4,5},{5,6},{6,7},{7,4},{8,9},{9,10},{10,1... | collective-permute-start | bytes 786440 | tf_op jit(solution)/shard_map/ppermute | solution.py:304
  101.2 1.5 collective-permute-start.12
  102.7 4.8 %collective-permute-done.9 = bf16[64,2048]{1,0:T(8,128)(2,1)S(1)} collective-permute-done((bf16[64,2048]{1,0:T(8,128)(2,1)S(1)}, bf16[64,2048]{1,0:T(8,128)(2,1)S(1)}, u32[]{:S(2)}, u32[]{:S(2)}) %collective-permute-start.9) | collective-permute-done | bytes 262176 | tf_op jit(solution)/shard_map/ppermute | solution.py:304
  108.4 2.5 %collective-permute-start.14 = (bf16[64,2048]{1,0:T(8,128)(2,1)S(1)}, bf16[64,2048]{1,0:T(8,128)(2,1)}, u32[]{:S(2)}, u32[]{:S(2)}) collective-permute-start(bf16[64,2048]{1,0:T(8,128)(2,1)S(1)} %collective-permute-done.12), channel_id=1, source_target_pairs={{0,3},{1,0},{2,1},{3,2},{4,7},{5,4},{6,5},{7,6},{8,11},{9,8},{10,9... | collective-permute-start | bytes 786440 | tf_op jit(solution)/shard_map/ppermute | solution.py:304
  111.0 1.9 %collective-permute-start.10 = (bf16[64,2048]{1,0:T(8,128)(2,1)}, bf16[64,2048]{1,0:T(8,128)(2,1)}, u32[]{:S(2)}, u32[]{:S(2)}) collective-permute-start(bf16[64,2048]{1,0:T(8,128)(2,1)} %get-tuple-element.32), channel_id=1, source_target_pairs={{0,1},{1,2},{2,3},{3,0},{4,5},{5,6},{6,7},{7,4},{8,9},{9,10},{10,1... | collective-permute-start | bytes 786440 | tf_op jit(solution)/shard_map/ppermute | solution.py:304
  112.9 4.9 %collective-permute-done.13 = bf16[64,2048]{1,0:T(8,128)(2,1)S(1)} collective-permute-done((bf16[64,2048]{1,0:T(8,128)(2,1)S(1)}, bf16[64,2048]{1,0:T(8,128)(2,1)S(1)}, u32[]{:S(2)}, u32[]{:S(2)}) %collective-permute-start.13) | collective-permute-done | bytes 262176 | tf_op jit(solution)/shard_map/ppermute | solution.py:304
  118.6 4.1 %fusion = f32[128,1536]{1,0:T(8,128)S(1)} fusion(bf16[2048,2304]{1,0:T(8,128)(2,1)} %all-gather.2.cloned.1.call-done, bf16[64,2048]{1,0:T(8,128)(2,1)} %collective-permute-done.14, bf16[64,2048]{1,0:T(8,128)(2,1)} %copy-done.12), kind=kOutput, calls=%fused_computation | convolution fusion | flops 806354944 | bytes 7602176 | tf_op jit(solution)/shard_map/dot_general | solution.py:394
  122.7 1.5 copy-done.6
  124.2 1.2 convolution_convert_fusion
  125.6 3.2 %collective-permute-start.17 = (bf16[64,2048]{1,0:T(8,128)(2,1)S(1)}, bf16[64,2048]{1,0:T(8,128)(2,1)S(1)}, u32[]{:S(2)}, u32[]{:S(2)}) collective-permute-start(bf16[64,2048]{1,0:T(8,128)(2,1)S(1)} %get-tuple-element.28), channel_id=1, source_target_pairs={{0,3},{1,0},{2,1},{3,2},{4,7},{5,4},{6,5},{7,6},{8,11},{9,8},{10,9... | collective-permute-start | bytes 786440 | tf_op jit(solution)/shard_map/ppermute | solution.py:304
  128.8 2.8 %fusion.2 = f32[256,1536]{1,0:T(8,128)S(1)} fusion(bf16[2048,2304]{1,0:T(8,128)(2,1)S(1)} %copy-done.6, bf16[64,2048]{1,0:T(8,128)(2,1)S(1)} %copy-done.11, bf16[64,2048]{1,0:T(8,128)(2,1)} %collective-permute-done.11, bf16[64,2048]{1,0:T(8,128)(2,1)} %collective-permute-done.10, bf16[64,2048]{1,0:T(8,128)(2,1)S(1)} %copy-done.9), kind=kOutput, calls=%fused_computation.2 | convolution fusion | flops 1614807040 | bytes 8912896 | tf_op jit(solution)/shard_map/dot_general | solution.py:394
  132.6 3.3 %collective-permute-done.15 = bf16[64,2048]{1,0:T(8,128)(2,1)S(1)} collective-permute-done((bf16[64,2048]{1,0:T(8,128)(2,1)S(1)}, bf16[64,2048]{1,0:T(8,128)(2,1)S(1)}, u32[]{:S(2)}, u32[]{:S(2)}) %collective-permute-start.15) | collective-permute-done | bytes 262176 | tf_op jit(solution)/shard_map/ppermute | solution.py:304
  136.3 3.3 %collective-permute-start.18 = (bf16[128,2048]{1,0:T(8,128)(2,1)S(1)}, bf16[128,2048]{1,0:T(8,128)(2,1)S(1)}, u32[]{:S(2)}, u32[]{:S(2)}) collective-permute-start(bf16[128,2048]{1,0:T(8,128)(2,1)S(1)} %get-tuple-element.22), channel_id=1, source_target_pairs={{0,3},{1,0},{2,1},{3,2},{4,7},{5,4},{6,5},{7,6},{8,11},{9,8},{10,9... | collective-permute-start | bytes 1572872 | tf_op jit(solution)/shard_map/ppermute | solution.py:304
  139.6 1.9 %fusion.4 = f32[128,1536]{1,0:T(8,128)S(1)} fusion(bf16[2048,2304]{1,0:T(8,128)(2,1)S(1)} %copy-done.6, bf16[64,2048]{1,0:T(8,128)(2,1)} %get-tuple-element.32, bf16[64,2048]{1,0:T(8,128)(2,1)S(1)} %get-tuple-element.31), kind=kOutput, calls=%fused_computation.4 | convolution fusion | flops 806354944 | bytes 7602176 | tf_op jit(solution)/shard_map/dot_general | solution.py:394
  141.6 1.2 fusion.9
  142.7 3.9 %collective-permute-done.16 = bf16[128,2048]{1,0:T(8,128)(2,1)S(1)} collective-permute-done((bf16[128,2048]{1,0:T(8,128)(2,1)S(1)}, bf16[128,2048]{1,0:T(8,128)(2,1)S(1)}, u32[]{:S(2)}, u32[]{:S(2)}) %collective-permute-start.16) | collective-permute-done | bytes 524320 | tf_op jit(solution)/shard_map/ppermute | solution.py:304
  (71 shorter events, 16.2 us)
Async XLA Ops:
  6.5 70.4 %copy-start = (bf16[512,2048]{1,0:T(8,128)(2,1)S(1)}, bf16[512,2048]{1,0:T(8,128)(2,1)}, u32[]{:S(2)}) copy-start(bf16[512,2048]{1,0:T(8,128)(2,1)} %param.31) | copy-start | bytes 6291460
  6.6 112.0 %all-gather.2.cloned.1.call-start = ((), (), s32[]{:S(2)}) async-start(), calls=%async_computation.1 | async-start | bytes 9732096 | tf_op jit(solution)/shard_map/all_gather | solution.py:274
  12.5 41.7 %all-to-all-start = ((bf16[32,16,128]{2,1,0:T(8,128)(2,1)}), bf16[32,16,128]{2,1,0:T(8,128)(2,1)S(1)}, u32[]{:S(2)}, u32[]{:S(2)}) async-start(bf16[32,16,128]{2,1,0:T(8,128)(2,1)} %get-tuple-element.11), calls=%async_computation | async-start | bytes 262144 | tf_op jit(solution)/shard_map/all_to_all | solution.py:275
  45.9 19.4 %copy-start.1 = (bf16[1024,512]{1,0:T(8,128)(2,1)S(1)}, bf16[1024,512]{1,0:T(8,128)(2,1)}, u32[]{:S(2)}) copy-start(bf16[1024,512]{1,0:T(8,128)(2,1)} %param.30) | copy-start | bytes 3145732
  59.9 15.0 %collective-permute-start.2 = (bf16[512,256]{1,0:T(8,128)(2,1)}, bf16[512,256]{1,0:T(8,128)(2,1)S(1)}, u32[]{:S(2)}, u32[]{:S(2)}) collective-permute-start(bf16[512,256]{1,0:T(8,128)(2,1)} %ssm_finish.1), channel_id=1, source_target_pairs={{0,2},{1,3},{2,0},{3,1},{4,6},{5,7},{6,4},{7,5},{8,10},{9,11},{10,... | collective-permute-start | bytes 786440 | tf_op jit(solution)/shard_map/ppermute | solution.py:304
  63.3 12.2 %collective-permute-start.1 = (bf16[512,256]{1,0:T(8,128)(2,1)}, bf16[512,256]{1,0:T(8,128)(2,1)S(1)}, u32[]{:S(2)}, u32[]{:S(2)}) collective-permute-start(bf16[512,256]{1,0:T(8,128)(2,1)} %ssm_finish.1), channel_id=1, source_target_pairs={{0,3},{1,0},{2,1},{3,2},{4,7},{5,4},{6,5},{7,6},{8,11},{9,8},{10,9... | collective-permute-start | bytes 786440 | tf_op jit(solution)/shard_map/ppermute | solution.py:304
  64.2 10.0 %collective-permute-start = (bf16[512,256]{1,0:T(8,128)(2,1)}, bf16[512,256]{1,0:T(8,128)(2,1)S(1)}, u32[]{:S(2)}, u32[]{:S(2)}) collective-permute-start(bf16[512,256]{1,0:T(8,128)(2,1)} %ssm_finish.1), channel_id=1, source_target_pairs={{0,1},{1,2},{2,3},{3,0},{4,5},{5,6},{6,7},{7,4},{8,9},{9,10},{10,1... | collective-permute-start | bytes 786440 | tf_op jit(solution)/shard_map/ppermute | solution.py:304
  66.6 7.9 %copy-start.2 = (bf16[1024,512]{1,0:T(8,128)(2,1)S(1)}, bf16[1024,512]{1,0:T(8,128)(2,1)}, u32[]{:S(2)}) copy-start(bf16[1024,512]{1,0:T(8,128)(2,1)} %param.29) | copy-start | bytes 3145732
  75.4 1.1 copy-start.7
  77.5 10.5 %collective-permute-start.4 = (bf16[64,2048]{1,0:T(8,128)(2,1)S(1)}, bf16[64,2048]{1,0:T(8,128)(2,1)S(1)}, u32[]{:S(2)}, u32[]{:S(2)}) collective-permute-start(bf16[64,2048]{1,0:T(8,128)(2,1)S(1)} %get-tuple-element.29), channel_id=1, source_target_pairs={{0,1},{1,2},{2,3},{3,0},{4,5},{5,6},{6,7},{7,4},{8,9},{9,10},{10,1... | collective-permute-start | bytes 786440 | tf_op jit(solution)/shard_map/ppermute | solution.py:304
  79.4 9.4 %collective-permute-start.7 = (bf16[64,2048]{1,0:T(8,128)(2,1)S(1)}, bf16[64,2048]{1,0:T(8,128)(2,1)S(1)}, u32[]{:S(2)}, u32[]{:S(2)}) collective-permute-start(bf16[64,2048]{1,0:T(8,128)(2,1)S(1)} %get-tuple-element.30), channel_id=1, source_target_pairs={{0,3},{1,0},{2,1},{3,2},{4,7},{5,4},{6,5},{7,6},{8,11},{9,8},{10,9... | collective-permute-start | bytes 786440 | tf_op jit(solution)/shard_map/ppermute | solution.py:304
  81.3 12.3 %collective-permute-start.6 = (bf16[64,2048]{1,0:T(8,128)(2,1)S(1)}, bf16[64,2048]{1,0:T(8,128)(2,1)S(1)}, u32[]{:S(2)}, u32[]{:S(2)}) collective-permute-start(bf16[64,2048]{1,0:T(8,128)(2,1)S(1)} %slice.186), channel_id=1, source_target_pairs={{0,1},{1,2},{2,3},{3,0},{4,5},{5,6},{6,7},{7,4},{8,9},{9,10},{10,1... | collective-permute-start | bytes 786440 | tf_op jit(solution)/shard_map/ppermute | solution.py:304
  82.5 11.7 %collective-permute-start.3 = (bf16[64,2048]{1,0:T(8,128)(2,1)S(1)}, bf16[64,2048]{1,0:T(8,128)(2,1)S(1)}, u32[]{:S(2)}, u32[]{:S(2)}) collective-permute-start(bf16[64,2048]{1,0:T(8,128)(2,1)S(1)} %slice.187), channel_id=1, source_target_pairs={{0,3},{1,0},{2,1},{3,2},{4,7},{5,4},{6,5},{7,6},{8,11},{9,8},{10,9... | collective-permute-start | bytes 786440 | tf_op jit(solution)/shard_map/ppermute | solution.py:304
  88.0 10.2 %copy-start.4 = (bf16[128,2048]{1,0:T(8,128)(2,1)S(1)}, bf16[128,2048]{1,0:T(8,128)(2,1)}, u32[]{:S(2)}) copy-start(bf16[128,2048]{1,0:T(8,128)(2,1)} %param.18) | copy-start | bytes 1572868
  88.0 9.0 %collective-permute-start.5 = (bf16[64,2048]{1,0:T(8,128)(2,1)S(1)}, bf16[64,2048]{1,0:T(8,128)(2,1)S(1)}, u32[]{:S(2)}, u32[]{:S(2)}) collective-permute-start(bf16[64,2048]{1,0:T(8,128)(2,1)S(1)} %fusion.37), channel_id=1, source_target_pairs={{0,1},{1,2},{2,3},{3,0},{4,5},{5,6},{6,7},{7,4},{8,9},{9,10},{10,1... | collective-permute-start | bytes 786440 | tf_op jit(solution)/shard_map/ppermute | solution.py:304
  88.8 9.4 %collective-permute-start.8 = (bf16[64,2048]{1,0:T(8,128)(2,1)S(1)}, bf16[64,2048]{1,0:T(8,128)(2,1)S(1)}, u32[]{:S(2)}, u32[]{:S(2)}) collective-permute-start(bf16[64,2048]{1,0:T(8,128)(2,1)S(1)} %fusion.34), channel_id=1, source_target_pairs={{0,3},{1,0},{2,1},{3,2},{4,7},{5,4},{6,5},{7,6},{8,11},{9,8},{10,9... | collective-permute-start | bytes 786440 | tf_op jit(solution)/shard_map/ppermute | solution.py:304
  92.0 6.7 %copy-start.5 = (f32[2048]{0:T(1024)S(1)}, f32[2048]{0:T(1024)}, u32[]{:S(2)}) copy-start(f32[2048]{0:T(1024)} %param.32) | copy-start | bytes 24580
  99.5 8.1 %collective-permute-start.9 = (bf16[64,2048]{1,0:T(8,128)(2,1)S(1)}, bf16[64,2048]{1,0:T(8,128)(2,1)S(1)}, u32[]{:S(2)}, u32[]{:S(2)}) collective-permute-start(bf16[64,2048]{1,0:T(8,128)(2,1)S(1)} %get-tuple-element.31), channel_id=1, source_target_pairs={{0,1},{1,2},{2,3},{3,0},{4,5},{5,6},{6,7},{7,4},{8,9},{9,10},{10,1... | collective-permute-start | bytes 786440 | tf_op jit(solution)/shard_map/ppermute | solution.py:304
  101.2 7.2 %collective-permute-start.12 = (bf16[64,2048]{1,0:T(8,128)(2,1)}, bf16[64,2048]{1,0:T(8,128)(2,1)S(1)}, u32[]{:S(2)}, u32[]{:S(2)}) collective-permute-start(bf16[64,2048]{1,0:T(8,128)(2,1)} %get-tuple-element.32), channel_id=1, source_target_pairs={{0,3},{1,0},{2,1},{3,2},{4,7},{5,4},{6,5},{7,6},{8,11},{9,8},{10,9... | collective-permute-start | bytes 786440 | tf_op jit(solution)/shard_map/ppermute | solution.py:304
  107.6 0.8 copy-start.8
  107.6 10.3 %collective-permute-start.13 = (bf16[64,2048]{1,0:T(8,128)(2,1)S(1)}, bf16[64,2048]{1,0:T(8,128)(2,1)S(1)}, u32[]{:S(2)}, u32[]{:S(2)}) collective-permute-start(bf16[64,2048]{1,0:T(8,128)(2,1)S(1)} %collective-permute-done.9), channel_id=1, source_target_pairs={{0,1},{1,2},{2,3},{3,0},{4,5},{5,6},{6,7},{7,4},{8,9},{9,10},{10,1... | collective-permute-start | bytes 786440 | tf_op jit(solution)/shard_map/ppermute | solution.py:304
  108.4 9.5 %copy-start.10 = (bf16[64,2048]{1,0:T(8,128)(2,1)}, bf16[64,2048]{1,0:T(8,128)(2,1)S(1)}, u32[]{:S(2)}) copy-start(bf16[64,2048]{1,0:T(8,128)(2,1)S(1)} %collective-permute-done.12) | copy-start | bytes 786436
  108.4 10.2 %collective-permute-start.14 = (bf16[64,2048]{1,0:T(8,128)(2,1)S(1)}, bf16[64,2048]{1,0:T(8,128)(2,1)}, u32[]{:S(2)}, u32[]{:S(2)}) collective-permute-start(bf16[64,2048]{1,0:T(8,128)(2,1)S(1)} %collective-permute-done.12), channel_id=1, source_target_pairs={{0,3},{1,0},{2,1},{3,2},{4,7},{5,4},{6,5},{7,6},{8,11},{9,8},{10,9... | collective-permute-start | bytes 786440 | tf_op jit(solution)/shard_map/ppermute | solution.py:304
  110.9 17.8 %collective-permute-start.11 = (bf16[64,2048]{1,0:T(8,128)(2,1)S(1)}, bf16[64,2048]{1,0:T(8,128)(2,1)}, u32[]{:S(2)}, u32[]{:S(2)}) collective-permute-start(bf16[64,2048]{1,0:T(8,128)(2,1)S(1)} %get-tuple-element.31), channel_id=1, source_target_pairs={{0,3},{1,0},{2,1},{3,2},{4,7},{5,4},{6,5},{7,6},{8,11},{9,8},{10,9... | collective-permute-start | bytes 786440 | tf_op jit(solution)/shard_map/ppermute | solution.py:304
  111.0 17.7 %collective-permute-start.10 = (bf16[64,2048]{1,0:T(8,128)(2,1)}, bf16[64,2048]{1,0:T(8,128)(2,1)}, u32[]{:S(2)}, u32[]{:S(2)}) collective-permute-start(bf16[64,2048]{1,0:T(8,128)(2,1)} %get-tuple-element.32), channel_id=1, source_target_pairs={{0,1},{1,2},{2,3},{3,0},{4,5},{5,6},{6,7},{7,4},{8,9},{9,10},{10,1... | collective-permute-start | bytes 786440 | tf_op jit(solution)/shard_map/ppermute | solution.py:304
  118.6 5.6 %copy-start.6 = (bf16[2048,2304]{1,0:T(8,128)(2,1)S(1)}, bf16[2048,2304]{1,0:T(8,128)(2,1)}, u32[]{:S(2)}) copy-start(bf16[2048,2304]{1,0:T(8,128)(2,1)} %all-gather.2.cloned.1.call-done) | copy-start | bytes 28311556
  124.2 4.6 %copy-start.9 = (bf16[64,2048]{1,0:T(8,128)(2,1)S(1)}, bf16[64,2048]{1,0:T(8,128)(2,1)}, u32[]{:S(2)}) copy-start(bf16[64,2048]{1,0:T(8,128)(2,1)} %copy-done.8) | copy-start | bytes 786436
  124.2 4.6 %copy-start.11 = (bf16[64,2048]{1,0:T(8,128)(2,1)S(1)}, bf16[64,2048]{1,0:T(8,128)(2,1)}, u32[]{:S(2)}) copy-start(bf16[64,2048]{1,0:T(8,128)(2,1)} %copy-done.10) | copy-start | bytes 786436
  125.4 10.5 %collective-permute-start.15 = (bf16[64,2048]{1,0:T(8,128)(2,1)S(1)}, bf16[64,2048]{1,0:T(8,128)(2,1)S(1)}, u32[]{:S(2)}, u32[]{:S(2)}) collective-permute-start(bf16[64,2048]{1,0:T(8,128)(2,1)S(1)} %get-tuple-element.27), channel_id=1, source_target_pairs={{0,1},{1,2},{2,3},{3,0},{4,5},{5,6},{6,7},{7,4},{8,9},{9,10},{10,1... | collective-permute-start | bytes 786440 | tf_op jit(solution)/shard_map/ppermute | solution.py:304
  125.6 10.4 %collective-permute-start.17 = (bf16[64,2048]{1,0:T(8,128)(2,1)S(1)}, bf16[64,2048]{1,0:T(8,128)(2,1)S(1)}, u32[]{:S(2)}, u32[]{:S(2)}) collective-permute-start(bf16[64,2048]{1,0:T(8,128)(2,1)S(1)} %get-tuple-element.28), channel_id=1, source_target_pairs={{0,3},{1,0},{2,1},{3,2},{4,7},{5,4},{6,5},{7,6},{8,11},{9,8},{10,9... | collective-permute-start | bytes 786440 | tf_op jit(solution)/shard_map/ppermute | solution.py:304
  136.1 10.5 %collective-permute-start.16 = (bf16[128,2048]{1,0:T(8,128)(2,1)S(1)}, bf16[128,2048]{1,0:T(8,128)(2,1)S(1)}, u32[]{:S(2)}, u32[]{:S(2)}) collective-permute-start(bf16[128,2048]{1,0:T(8,128)(2,1)S(1)} %get-tuple-element.21), channel_id=1, source_target_pairs={{0,1},{1,2},{2,3},{3,0},{4,5},{5,6},{6,7},{7,4},{8,9},{9,10},{10,1... | collective-permute-start | bytes 1572872 | tf_op jit(solution)/shard_map/ppermute | solution.py:304
  136.3 10.4 %collective-permute-start.18 = (bf16[128,2048]{1,0:T(8,128)(2,1)S(1)}, bf16[128,2048]{1,0:T(8,128)(2,1)S(1)}, u32[]{:S(2)}, u32[]{:S(2)}) collective-permute-start(bf16[128,2048]{1,0:T(8,128)(2,1)S(1)} %get-tuple-element.22), channel_id=1, source_target_pairs={{0,3},{1,0},{2,1},{3,2},{4,7},{5,4},{6,5},{7,6},{8,11},{9,8},{10,9... | collective-permute-start | bytes 1572872 | tf_op jit(solution)/shard_map/ppermute | solution.py:304
  (2 other events, 1.4 us)
Sparse Core Ops, SparseCore 0:
  12.6 93.0 all-gather.1

commit v4 on v1

--- a/solution.py
+++ b/solution.py
@@ -291,13 +291,14 @@
     return lax.dynamic_slice_in_dim(array, index * size, size, 0)
 
 
-def gathered(own):
-    half = own.shape[0] // 2
-    left = ring(own, 1)
-    right = ring(own, -1)
-    far_top = ring(left[:half], 1)
-    far_low = ring(right[half:], -1)
-    return own, left, right, jnp.concatenate([far_top, far_low], axis=0)
+def gathered(top, low):
+    left_top = ring(top, 1)
+    right_low = ring(low, -1)
+    left_low = ring(low, 1)
+    right_top = ring(top, -1)
+    far_top = ring(left_top, 1)
+    far_low = ring(right_low, -1)
+    return (left_top, left_low), (right_top, right_low), (far_top, far_low)
 
 
 def summed(far, right, left, own):
@@ -311,7 +312,19 @@
     from_right_low = ring((left[half:] + passing_down.astype(F32)).astype(BF16), -1)
     top = own[:half] + from_right_top.astype(F32) + from_left_top.astype(F32)
     low = own[half:] + from_left_low.astype(F32) + from_right_low.astype(F32)
-    return jnp.concatenate([top, low], axis=0)
+    return top, low
+
+
+def summed_late(far, right, left, own):
+    half = own.shape[0] // 2
+    far = far.astype(BF16)
+    passing_up = ring(far[:half], 1)
+    passing_down = ring(far[half:], -1)
+    right = right + jnp.pad(passing_up, ((0, half), (0, 0))).astype(F32)
+    left = left + jnp.pad(passing_down, ((half, 0), (0, 0))).astype(F32)
+    from_left, from_right = ring(right.astype(BF16), 1), ring(left.astype(BF16), -1)
+    total = own + from_left.astype(F32) + from_right.astype(F32)
+    return total[:half], total[half:]
 
 
 def shards(
@@ -328,7 +341,9 @@
         read_real, read_imag, skip_gain, (mlp_gate, mlp_up, mlp_down.T),
     )
     both, down_weight = weight[:, : 2 * hidden_width], weight[:, 2 * hidden_width :]
-    places = dict(zip((0, 3, 1, 2), (acts, ring(acts, 1), ring(acts, -1), ring(acts, 2))))
+    places = dict(
+        zip((0, 3, 1, 2), (acts, ring(acts, 1), ring(acts, -1), ring(acts, 2)))
+    )
 
     def project(w):
         total = None
@@ -350,21 +365,26 @@
 
     far = mix(2)
     branch = summed(far, mix(1), mix(3), mix(0))
-    inner = residual.astype(F32) + branch
-    scale = lax.rsqrt(jnp.mean(inner * inner, axis=-1, keepdims=True) + EPSILON)
-    normed = (inner * scale * norm_gain).astype(BF16)
-    own, left, right, far = gathered(normed)
+    half = owned // 2
+    inner, normed = [], []
+    for i, part in enumerate(branch):
+        inner.append(residual[i * half : (i + 1) * half].astype(F32) + part)
+        scale = lax.rsqrt(jnp.mean(inner[i] * inner[i], axis=-1, keepdims=True) + EPSILON)
+        normed.append((inner[i] * scale * norm_gain).astype(BF16))
+    left, right, far = gathered(*normed)
 
     def feed(rows):
         hidden = jnp.dot(rows, both, preferred_element_type=F32)
         hidden = (jax.nn.silu(hidden[:, :hidden_width]) * hidden[:, hidden_width:]).astype(BF16)
         return lax.dot_general(hidden, down_weight, NT, preferred_element_type=F32)
 
-    near = feed(own)
-    sides = feed(jnp.concatenate([left, right], axis=0))
-    sides = lax.optimization_barrier(sides)
-    down = summed(feed(far), sides[owned:], sides[:owned], near)
-    return (inner + 0.5 * down).astype(BF16)
+    sides = feed(jnp.concatenate([*left, *right], axis=0))
+    far = feed(jnp.concatenate(far, axis=0))
+    own = feed(jnp.concatenate(normed, axis=0))
+    down = summed_late(far, sides[owned:], sides[:owned], own)
+    return jnp.concatenate(
+        [(i + 0.5 * part).astype(BF16) for i, part in zip(inner, down)], axis=0
+    )
 
 
 def solution(mesh):

time: 154 us -> 153 us (level)
  waiting for transfers between devices: 48.8 us -> 42.8 us
  matrix products: 16.6 us -> 18.7 us
    ppermute x19, waiting for transfers between devices: 38.1 us -> 32 us  [ring(): lax.ppermute(array, 'tp', [(i, (i + by) % peers) for i in range(peers)])]
    dot_general x3, matrix products: 6.77 us -> 8.82 us  [feed(): hidden = jnp.dot(rows, both, preferred_element_type=F32)]
    unnamed x30 -> x26, local copies, waits for them, and re-layouts: 2.54 us -> 3.52 us
  transfers between devices with their start and end apart: 21 -> 21, of which waited for: 13 -> 11; matrix products, arithmetic and copies ran while one was open for 8% -> 13% of each run, Pallas kernels for 7% -> 7%
where the time goes in v4:
time: 153 us; the launch traced here: 152 us
  starting transfers between devices  55.9 us (37%)
  waiting for transfers between devices  42.8 us (28%)
  matrix products  18.7 us (12%)
  Pallas kernels  14.6 us (10%)
  between operations  13.8 us (9%)
  local copies, waits for them, and re-layouts  3.65 us (2%)
  other arithmetic  2.75 us (2%)
    ppermute x19, waiting for transfers between devices, ring(): lax.ppermute(array, 'tp', [(i, (i + by) % peers) for i in range(peers)])  32 us
    ppermute x19, starting transfers between devices, ring(): lax.ppermute(array, 'tp', [(i, (i + by) % peers) for i in range(peers)])  31.1 us
    all_to_all x1, starting transfers between devices, activations(): pieces = lax.all_to_all(end, 'sp', 0, 0, tiled=True)  24.8 us
    all_to_all x1, waiting for transfers between devices, activations(): pieces = lax.all_to_all(end, 'sp', 0, 0, tiled=True)  10.8 us
    dot_general x3, matrix products, feed(): hidden = jnp.dot(rows, both, preferred_element_type=F32)  8.82 us
    pallas_call x1, Pallas kernels, activations(): pl.pallas_call(local_kernel, out_shape=(shaped(rows, chans), shaped(rows,...  6.13 us
    dot_general x8, matrix products, project(): jnp.dot(rows, rows_at(w, (me + place) % peers, chans), preferred_element_...  4.81 us
    pallas_call x1, Pallas kernels, activations(): pl.pallas_call(ends_kernel, out_shape=(shaped(peers, 2 * flat // LANES, L...  4.39 us
  transfers between devices with their start and end apart: 21, of which 11 were waited for; matrix products, arithmetic and copies ran while one was open for 13% of the time, Pallas kernels for 7%

profile of v4, /device:TPU:40, one launch (start us, length us, event | category | flops | bytes accessed | tf_op | source)
XLA Modules:
  0.0 152.2 jit_solution(4470740998864618933)
XLA Ops:
  6.6 4.4 %ssm_ends.1 = (bf16[32,16,128]{2,1,0:T(8,128)(2,1)}, f32[2,8,1024]{2,1,0:T(8,128)}, f32[4,1024]{1,0:T(4,128)}, bf16[64,2304]{1,0:T(8,128)(2,1)}) custom-call(s32[1]{0:T(128)} %bitcast.me_ref, f32[16,64]{1,0:T(8,128)} %decay_ref.1, f32[16,64]{1,0:T(8,128)} %freq_ref.1, f32[1,16]{1,0:T(1,128)} %bitcast.33, bf16[512,256]{1,0:T(8,128)(2,1)} %x_ref.3, ...), custom_call_target="tpu_custom_call" | custom-call | tf_op jit(solution)/shard_map/ssm_ends/pallas_call | solution.py:249
  11.0 24.8 %all-to-all-start = ((bf16[32,16,128]{2,1,0:T(8,128)(2,1)}), bf16[32,16,128]{2,1,0:T(8,128)(2,1)S(1)}, u32[]{:S(2)}, u32[]{:S(2)}) async-start(bf16[32,16,128]{2,1,0:T(8,128)(2,1)} %get-tuple-element.11), calls=%async_computation | async-start | bytes 262144 | tf_op jit(solution)/shard_map/all_to_all | solution.py:262
  35.9 6.1 %ssm_local.1 = (f32[512,256]{1,0:T(8,128)}, bf16[512,2048]{1,0:T(8,128)(2,1)}) custom-call(f32[4,1024]{1,0:T(4,128)} %get-tuple-element.12.row_ref, f32[2,8,1024]{2,1,0:T(8,128)} %get-tuple-element.13.seg_ref, bf16[512,256]{1,0:T(8,128)(2,1)} %x_ref.3, f32[256,64]{1,0:T(8,128)} %bitcast.25, f32[256,64]{1,0:T(8,128)} %bitcast.27, f32[256,64]{1,0:T(8,128)} %bitcast.28, ...), custom_call_target="tpu_custom_call" | custom-call | flops 1073741824 | bytes 4194304 | tf_op jit(solution)/shard_map/ssm_local/pallas_call | solution.py:263
  42.0 10.8 %all-to-all-done.piece_ref = bf16[32,16,128]{2,1,0:T(8,128)(2,1)S(1)} async-done(((bf16[32,16,128]{2,1,0:T(8,128)(2,1)}), bf16[32,16,128]{2,1,0:T(8,128)(2,1)S(1)}, u32[]{:S(2)}, u32[]{:S(2)}) %all-to-all-start) | async-done | bytes 131104 | tf_op jit(solution)/shard_map/all_to_all | solution.py:262
  53.4 4.1 %ssm_finish.1 = bf16[512,256]{1,0:T(8,128)(2,1)} custom-call(bf16[32,16,128]{2,1,0:T(8,128)(2,1)} %copy-done.3, f32[4,1024]{1,0:T(4,128)} %get-tuple-element.12.row_ref, f32[256,64]{1,0:T(8,128)} %bitcast.29, f32[256,64]{1,0:T(8,128)} %bitcast.31, f32[512,256]{1,0:T(8,128)} %get-tuple-element.14.y_ref, bf16[512,2048]{1,0:T(8,128)(2,1)} %get-tuple-element.15.power_ref), custom_call_target="tpu_custom_call" | custom-call | tf_op jit(solution)/shard_map/ssm_finish/pallas_call | solution.py:276
  57.5 3.4 %collective-permute-start.2 = (bf16[512,256]{1,0:T(8,128)(2,1)}, bf16[512,256]{1,0:T(8,128)(2,1)S(1)}, u32[]{:S(2)}, u32[]{:S(2)}) collective-permute-start(bf16[512,256]{1,0:T(8,128)(2,1)} %ssm_finish.1), channel_id=1, source_target_pairs={{0,2},{1,3},{2,0},{3,1},{4,6},{5,7},{6,4},{7,5},{8,10},{9,11},{10,... | collective-permute-start | bytes 786440 | tf_op jit(solution)/shard_map/ppermute | solution.py:287
  62.9 1.3 fusion.54
  64.2 1.4 fusion.60
  65.6 6.2 %collective-permute-done = bf16[512,256]{1,0:T(8,128)(2,1)S(1)} collective-permute-done((bf16[512,256]{1,0:T(8,128)(2,1)}, bf16[512,256]{1,0:T(8,128)(2,1)S(1)}, u32[]{:S(2)}, u32[]{:S(2)}) %collective-permute-start) | collective-permute-done | bytes 262176 | tf_op jit(solution)/shard_map/ppermute | solution.py:287
  75.1 1.9 %collective-permute-start.4 = (bf16[64,2048]{1,0:T(8,128)(2,1)S(1)}, bf16[64,2048]{1,0:T(8,128)(2,1)S(1)}, u32[]{:S(2)}, u32[]{:S(2)}) collective-permute-start(bf16[64,2048]{1,0:T(8,128)(2,1)S(1)} %get-tuple-element.29), channel_id=1, source_target_pairs={{0,1},{1,2},{2,3},{3,0},{4,5},{5,6},{6,7},{7,4},{8,9},{9,10},{10,1... | collective-permute-start | bytes 786440 | tf_op jit(solution)/shard_map/ppermute | solution.py:287
  77.0 1.5 collective-permute-start.7
  80.1 2.8 %collective-permute-start.3 = (bf16[64,2048]{1,0:T(8,128)(2,1)S(1)}, bf16[64,2048]{1,0:T(8,128)(2,1)S(1)}, u32[]{:S(2)}, u32[]{:S(2)}) collective-permute-start(bf16[64,2048]{1,0:T(8,128)(2,1)S(1)} %slice.187), channel_id=1, source_target_pairs={{0,3},{1,0},{2,1},{3,2},{4,7},{5,4},{6,5},{7,6},{8,11},{9,8},{10,9... | collective-permute-start | bytes 786440 | tf_op jit(solution)/shard_map/ppermute | solution.py:287
  82.9 2.7 %collective-permute-done.4 = bf16[64,2048]{1,0:T(8,128)(2,1)S(1)} collective-permute-done((bf16[64,2048]{1,0:T(8,128)(2,1)S(1)}, bf16[64,2048]{1,0:T(8,128)(2,1)S(1)}, u32[]{:S(2)}, u32[]{:S(2)}) %collective-permute-start.4) | collective-permute-done | bytes 262176 | tf_op jit(solution)/shard_map/ppermute | solution.py:287
  86.4 2.8 %collective-permute-start.8 = (bf16[64,2048]{1,0:T(8,128)(2,1)S(1)}, bf16[64,2048]{1,0:T(8,128)(2,1)S(1)}, u32[]{:S(2)}, u32[]{:S(2)}) collective-permute-start(bf16[64,2048]{1,0:T(8,128)(2,1)S(1)} %fusion.34), channel_id=1, source_target_pairs={{0,3},{1,0},{2,1},{3,2},{4,7},{5,4},{6,5},{7,6},{8,11},{9,8},{10,9... | collective-permute-start | bytes 786440 | tf_op jit(solution)/shard_map/ppermute | solution.py:287
  89.7 1.6 %collective-permute-done.6 = bf16[64,2048]{1,0:T(8,128)(2,1)S(1)} collective-permute-done((bf16[64,2048]{1,0:T(8,128)(2,1)S(1)}, bf16[64,2048]{1,0:T(8,128)(2,1)S(1)}, u32[]{:S(2)}, u32[]{:S(2)}) %collective-permute-start.6) | collective-permute-done | bytes 262176 | tf_op jit(solution)/shard_map/ppermute | solution.py:287
  91.8 2.9 %collective-permute-done.5 = bf16[64,2048]{1,0:T(8,128)(2,1)S(1)} collective-permute-done((bf16[64,2048]{1,0:T(8,128)(2,1)S(1)}, bf16[64,2048]{1,0:T(8,128)(2,1)S(1)}, u32[]{:S(2)}, u32[]{:S(2)}) %collective-permute-start.5) | collective-permute-done | bytes 262176 | tf_op jit(solution)/shard_map/ppermute | solution.py:287
  94.7 1.2 collective-permute-done.8
  97.1 1.7 %collective-permute-start.9 = (bf16[64,2048]{1,0:T(8,128)(2,1)S(1)}, bf16[64,2048]{1,0:T(8,128)(2,1)S(1)}, u32[]{:S(2)}, u32[]{:S(2)}) collective-permute-start(bf16[64,2048]{1,0:T(8,128)(2,1)S(1)} %get-tuple-element.31), channel_id=1, source_target_pairs={{0,1},{1,2},{2,3},{3,0},{4,5},{5,6},{6,7},{7,4},{8,9},{9,10},{10,1... | collective-permute-start | bytes 786440 | tf_op jit(solution)/shard_map/ppermute | solution.py:287
  98.9 1.5 collective-permute-start.12
  100.4 4.8 %collective-permute-done.9 = bf16[64,2048]{1,0:T(8,128)(2,1)S(1)} collective-permute-done((bf16[64,2048]{1,0:T(8,128)(2,1)S(1)}, bf16[64,2048]{1,0:T(8,128)(2,1)S(1)}, u32[]{:S(2)}, u32[]{:S(2)}) %collective-permute-start.9) | collective-permute-done | bytes 262176 | tf_op jit(solution)/shard_map/ppermute | solution.py:287
  106.0 2.5 %collective-permute-start.14 = (bf16[64,2048]{1,0:T(8,128)(2,1)S(1)}, bf16[64,2048]{1,0:T(8,128)(2,1)}, u32[]{:S(2)}, u32[]{:S(2)}) collective-permute-start(bf16[64,2048]{1,0:T(8,128)(2,1)S(1)} %collective-permute-done.12), channel_id=1, source_target_pairs={{0,3},{1,0},{2,1},{3,2},{4,7},{5,4},{6,5},{7,6},{8,11},{9,8},{10,9... | collective-permute-start | bytes 786440 | tf_op jit(solution)/shard_map/ppermute | solution.py:287
  108.7 1.9 %collective-permute-start.10 = (bf16[64,2048]{1,0:T(8,128)(2,1)}, bf16[64,2048]{1,0:T(8,128)(2,1)}, u32[]{:S(2)}, u32[]{:S(2)}) collective-permute-start(bf16[64,2048]{1,0:T(8,128)(2,1)} %get-tuple-element.32), channel_id=1, source_target_pairs={{0,1},{1,2},{2,3},{3,0},{4,5},{5,6},{6,7},{7,4},{8,9},{9,10},{10,1... | collective-permute-start | bytes 786440 | tf_op jit(solution)/shard_map/ppermute | solution.py:287
  110.6 4.8 %collective-permute-done.13 = bf16[64,2048]{1,0:T(8,128)(2,1)S(1)} collective-permute-done((bf16[64,2048]{1,0:T(8,128)(2,1)S(1)}, bf16[64,2048]{1,0:T(8,128)(2,1)S(1)}, u32[]{:S(2)}, u32[]{:S(2)}) %collective-permute-start.13) | collective-permute-done | bytes 262176 | tf_op jit(solution)/shard_map/ppermute | solution.py:287
  116.0 4.1 %fusion = f32[128,1536]{1,0:T(8,128)S(1)} fusion(bf16[2048,2304]{1,0:T(8,128)(2,1)} %all-gather.2.cloned.1.call-done, bf16[64,2048]{1,0:T(8,128)(2,1)} %collective-permute-done.14, bf16[64,2048]{1,0:T(8,128)(2,1)} %copy-done.12), kind=kOutput, calls=%fused_computation | convolution fusion | flops 806354944 | bytes 7602176 | tf_op jit(solution)/shard_map/dot_general | solution.py:377
  120.1 1.5 %copy-done.6 = bf16[2048,2304]{1,0:T(8,128)(2,1)S(1)} copy-done((bf16[2048,2304]{1,0:T(8,128)(2,1)S(1)}, bf16[2048,2304]{1,0:T(8,128)(2,1)}, u32[]{:S(2)}) %copy-start.6) | copy-done | bytes 9437208
  123.3 3.0 %collective-permute-start.17 = (bf16[64,2048]{1,0:T(8,128)(2,1)S(1)}, bf16[64,2048]{1,0:T(8,128)(2,1)S(1)}, u32[]{:S(2)}, u32[]{:S(2)}) collective-permute-start(bf16[64,2048]{1,0:T(8,128)(2,1)S(1)} %get-tuple-element.28), channel_id=1, source_target_pairs={{0,3},{1,0},{2,1},{3,2},{4,7},{5,4},{6,5},{7,6},{8,11},{9,8},{10,9... | collective-permute-start | bytes 786440 | tf_op jit(solution)/shard_map/ppermute | solution.py:287
  126.2 2.8 %fusion.2 = f32[256,1536]{1,0:T(8,128)S(1)} fusion(bf16[2048,2304]{1,0:T(8,128)(2,1)S(1)} %copy-done.6, bf16[64,2048]{1,0:T(8,128)(2,1)S(1)} %copy-done.11, bf16[64,2048]{1,0:T(8,128)(2,1)} %collective-permute-done.11, bf16[64,2048]{1,0:T(8,128)(2,1)} %collective-permute-done.10, bf16[64,2048]{1,0:T(8,128)(2,1)S(1)} %copy-done.9), kind=kOutput, calls=%fused_computation.2 | convolution fusion | flops 1614807040 | bytes 8912896 | tf_op jit(solution)/shard_map/dot_general | solution.py:377
  130.1 3.3 %collective-permute-done.15 = bf16[64,2048]{1,0:T(8,128)(2,1)S(1)} collective-permute-done((bf16[64,2048]{1,0:T(8,128)(2,1)S(1)}, bf16[64,2048]{1,0:T(8,128)(2,1)S(1)}, u32[]{:S(2)}, u32[]{:S(2)}) %collective-permute-start.15) | collective-permute-done | bytes 262176 | tf_op jit(solution)/shard_map/ppermute | solution.py:287
  133.8 3.3 %collective-permute-start.18 = (bf16[128,2048]{1,0:T(8,128)(2,1)S(1)}, bf16[128,2048]{1,0:T(8,128)(2,1)S(1)}, u32[]{:S(2)}, u32[]{:S(2)}) collective-permute-start(bf16[128,2048]{1,0:T(8,128)(2,1)S(1)} %get-tuple-element.22), channel_id=1, source_target_pairs={{0,3},{1,0},{2,1},{3,2},{4,7},{5,4},{6,5},{7,6},{8,11},{9,8},{10,9... | collective-permute-start | bytes 1572872 | tf_op jit(solution)/shard_map/ppermute | solution.py:287
  137.1 1.9 %fusion.4 = f32[128,1536]{1,0:T(8,128)S(1)} fusion(bf16[2048,2304]{1,0:T(8,128)(2,1)S(1)} %copy-done.6, bf16[64,2048]{1,0:T(8,128)(2,1)} %get-tuple-element.32, bf16[64,2048]{1,0:T(8,128)(2,1)S(1)} %get-tuple-element.31), kind=kOutput, calls=%fused_computation.4 | convolution fusion | flops 806354944 | bytes 7602176 | tf_op jit(solution)/shard_map/dot_general | solution.py:377
  139.0 1.2 fusion.9
  140.2 3.9 %collective-permute-done.16 = bf16[128,2048]{1,0:T(8,128)(2,1)S(1)} collective-permute-done((bf16[128,2048]{1,0:T(8,128)(2,1)S(1)}, bf16[128,2048]{1,0:T(8,128)(2,1)S(1)}, u32[]{:S(2)}, u32[]{:S(2)}) %collective-permute-start.16) | collective-permute-done | bytes 524320 | tf_op jit(solution)/shard_map/ppermute | solution.py:287
  (71 shorter events, 16.5 us)
Async XLA Ops:
  6.5 68.0 %copy-start = (bf16[512,2048]{1,0:T(8,128)(2,1)S(1)}, bf16[512,2048]{1,0:T(8,128)(2,1)}, u32[]{:S(2)}) copy-start(bf16[512,2048]{1,0:T(8,128)(2,1)} %param.31) | copy-start | bytes 6291460
  6.6 109.5 %all-gather.2.cloned.1.call-start = ((), (), s32[]{:S(2)}) async-start(), calls=%async_computation.1 | async-start | bytes 9732096 | tf_op jit(solution)/shard_map/all_gather | solution.py:261
  11.0 41.7 %all-to-all-start = ((bf16[32,16,128]{2,1,0:T(8,128)(2,1)}), bf16[32,16,128]{2,1,0:T(8,128)(2,1)S(1)}, u32[]{:S(2)}, u32[]{:S(2)}) async-start(bf16[32,16,128]{2,1,0:T(8,128)(2,1)} %get-tuple-element.11), calls=%async_computation | async-start | bytes 262144 | tf_op jit(solution)/shard_map/all_to_all | solution.py:262
  42.0 20.9 %copy-start.1 = (bf16[1024,512]{1,0:T(8,128)(2,1)S(1)}, bf16[1024,512]{1,0:T(8,128)(2,1)}, u32[]{:S(2)}) copy-start(bf16[1024,512]{1,0:T(8,128)(2,1)} %param.30) | copy-start | bytes 3145732
  57.5 15.0 %collective-permute-start.2 = (bf16[512,256]{1,0:T(8,128)(2,1)}, bf16[512,256]{1,0:T(8,128)(2,1)S(1)}, u32[]{:S(2)}, u32[]{:S(2)}) collective-permute-start(bf16[512,256]{1,0:T(8,128)(2,1)} %ssm_finish.1), channel_id=1, source_target_pairs={{0,2},{1,3},{2,0},{3,1},{4,6},{5,7},{6,4},{7,5},{8,10},{9,11},{10,... | collective-permute-start | bytes 786440 | tf_op jit(solution)/shard_map/ppermute | solution.py:287
  60.9 12.2 %collective-permute-start.1 = (bf16[512,256]{1,0:T(8,128)(2,1)}, bf16[512,256]{1,0:T(8,128)(2,1)S(1)}, u32[]{:S(2)}, u32[]{:S(2)}) collective-permute-start(bf16[512,256]{1,0:T(8,128)(2,1)} %ssm_finish.1), channel_id=1, source_target_pairs={{0,3},{1,0},{2,1},{3,2},{4,7},{5,4},{6,5},{7,6},{8,11},{9,8},{10,9... | collective-permute-start | bytes 786440 | tf_op jit(solution)/shard_map/ppermute | solution.py:287
  61.8 10.0 %collective-permute-start = (bf16[512,256]{1,0:T(8,128)(2,1)}, bf16[512,256]{1,0:T(8,128)(2,1)S(1)}, u32[]{:S(2)}, u32[]{:S(2)}) collective-permute-start(bf16[512,256]{1,0:T(8,128)(2,1)} %ssm_finish.1), channel_id=1, source_target_pairs={{0,1},{1,2},{2,3},{3,0},{4,5},{5,6},{6,7},{7,4},{8,9},{9,10},{10,1... | collective-permute-start | bytes 786440 | tf_op jit(solution)/shard_map/ppermute | solution.py:287
  64.2 8.0 %copy-start.2 = (bf16[1024,512]{1,0:T(8,128)(2,1)S(1)}, bf16[1024,512]{1,0:T(8,128)(2,1)}, u32[]{:S(2)}) copy-start(bf16[1024,512]{1,0:T(8,128)(2,1)} %param.29) | copy-start | bytes 3145732
  73.1 1.0 copy-start.7
  75.1 10.5 %collective-permute-start.4 = (bf16[64,2048]{1,0:T(8,128)(2,1)S(1)}, bf16[64,2048]{1,0:T(8,128)(2,1)S(1)}, u32[]{:S(2)}, u32[]{:S(2)}) collective-permute-start(bf16[64,2048]{1,0:T(8,128)(2,1)S(1)} %get-tuple-element.29), channel_id=1, source_target_pairs={{0,1},{1,2},{2,3},{3,0},{4,5},{5,6},{6,7},{7,4},{8,9},{9,10},{10,1... | collective-permute-start | bytes 786440 | tf_op jit(solution)/shard_map/ppermute | solution.py:287
  77.0 9.4 %collective-permute-start.7 = (bf16[64,2048]{1,0:T(8,128)(2,1)S(1)}, bf16[64,2048]{1,0:T(8,128)(2,1)S(1)}, u32[]{:S(2)}, u32[]{:S(2)}) collective-permute-start(bf16[64,2048]{1,0:T(8,128)(2,1)S(1)} %get-tuple-element.30), channel_id=1, source_target_pairs={{0,3},{1,0},{2,1},{3,2},{4,7},{5,4},{6,5},{7,6},{8,11},{9,8},{10,9... | collective-permute-start | bytes 786440 | tf_op jit(solution)/shard_map/ppermute | solution.py:287
  78.9 12.3 %collective-permute-start.6 = (bf16[64,2048]{1,0:T(8,128)(2,1)S(1)}, bf16[64,2048]{1,0:T(8,128)(2,1)S(1)}, u32[]{:S(2)}, u32[]{:S(2)}) collective-permute-start(bf16[64,2048]{1,0:T(8,128)(2,1)S(1)} %slice.186), channel_id=1, source_target_pairs={{0,1},{1,2},{2,3},{3,0},{4,5},{5,6},{6,7},{7,4},{8,9},{9,10},{10,1... | collective-permute-start | bytes 786440 | tf_op jit(solution)/shard_map/ppermute | solution.py:287
  80.1 11.7 %collective-permute-start.3 = (bf16[64,2048]{1,0:T(8,128)(2,1)S(1)}, bf16[64,2048]{1,0:T(8,128)(2,1)S(1)}, u32[]{:S(2)}, u32[]{:S(2)}) collective-permute-start(bf16[64,2048]{1,0:T(8,128)(2,1)S(1)} %slice.187), channel_id=1, source_target_pairs={{0,3},{1,0},{2,1},{3,2},{4,7},{5,4},{6,5},{7,6},{8,11},{9,8},{10,9... | collective-permute-start | bytes 786440 | tf_op jit(solution)/shard_map/ppermute | solution.py:287
  85.7 10.2 %copy-start.4 = (bf16[128,2048]{1,0:T(8,128)(2,1)S(1)}, bf16[128,2048]{1,0:T(8,128)(2,1)}, u32[]{:S(2)}) copy-start(bf16[128,2048]{1,0:T(8,128)(2,1)} %param.18) | copy-start | bytes 1572868
  85.7 9.0 %collective-permute-start.5 = (bf16[64,2048]{1,0:T(8,128)(2,1)S(1)}, bf16[64,2048]{1,0:T(8,128)(2,1)S(1)}, u32[]{:S(2)}, u32[]{:S(2)}) collective-permute-start(bf16[64,2048]{1,0:T(8,128)(2,1)S(1)} %fusion.37), channel_id=1, source_target_pairs={{0,1},{1,2},{2,3},{3,0},{4,5},{5,6},{6,7},{7,4},{8,9},{9,10},{10,1... | collective-permute-start | bytes 786440 | tf_op jit(solution)/shard_map/ppermute | solution.py:287
  86.4 9.4 %collective-permute-start.8 = (bf16[64,2048]{1,0:T(8,128)(2,1)S(1)}, bf16[64,2048]{1,0:T(8,128)(2,1)S(1)}, u32[]{:S(2)}, u32[]{:S(2)}) collective-permute-start(bf16[64,2048]{1,0:T(8,128)(2,1)S(1)} %fusion.34), channel_id=1, source_target_pairs={{0,3},{1,0},{2,1},{3,2},{4,7},{5,4},{6,5},{7,6},{8,11},{9,8},{10,9... | collective-permute-start | bytes 786440 | tf_op jit(solution)/shard_map/ppermute | solution.py:287
  89.6 6.6 %copy-start.5 = (f32[2048]{0:T(1024)S(1)}, f32[2048]{0:T(1024)}, u32[]{:S(2)}) copy-start(f32[2048]{0:T(1024)} %param.32) | copy-start | bytes 24580
  97.1 8.1 %collective-permute-start.9 = (bf16[64,2048]{1,0:T(8,128)(2,1)S(1)}, bf16[64,2048]{1,0:T(8,128)(2,1)S(1)}, u32[]{:S(2)}, u32[]{:S(2)}) collective-permute-start(bf16[64,2048]{1,0:T(8,128)(2,1)S(1)} %get-tuple-element.31), channel_id=1, source_target_pairs={{0,1},{1,2},{2,3},{3,0},{4,5},{5,6},{6,7},{7,4},{8,9},{9,10},{10,1... | collective-permute-start | bytes 786440 | tf_op jit(solution)/shard_map/ppermute | solution.py:287
  98.9 7.2 %collective-permute-start.12 = (bf16[64,2048]{1,0:T(8,128)(2,1)}, bf16[64,2048]{1,0:T(8,128)(2,1)S(1)}, u32[]{:S(2)}, u32[]{:S(2)}) collective-permute-start(bf16[64,2048]{1,0:T(8,128)(2,1)} %get-tuple-element.32), channel_id=1, source_target_pairs={{0,3},{1,0},{2,1},{3,2},{4,7},{5,4},{6,5},{7,6},{8,11},{9,8},{10,9... | collective-permute-start | bytes 786440 | tf_op jit(solution)/shard_map/ppermute | solution.py:287
  105.2 0.9 copy-start.8
  105.2 10.2 %collective-permute-start.13 = (bf16[64,2048]{1,0:T(8,128)(2,1)S(1)}, bf16[64,2048]{1,0:T(8,128)(2,1)S(1)}, u32[]{:S(2)}, u32[]{:S(2)}) collective-permute-start(bf16[64,2048]{1,0:T(8,128)(2,1)S(1)} %collective-permute-done.9), channel_id=1, source_target_pairs={{0,1},{1,2},{2,3},{3,0},{4,5},{5,6},{6,7},{7,4},{8,9},{9,10},{10,1... | collective-permute-start | bytes 786440 | tf_op jit(solution)/shard_map/ppermute | solution.py:287
  106.0 9.3 %copy-start.10 = (bf16[64,2048]{1,0:T(8,128)(2,1)}, bf16[64,2048]{1,0:T(8,128)(2,1)S(1)}, u32[]{:S(2)}) copy-start(bf16[64,2048]{1,0:T(8,128)(2,1)S(1)} %collective-permute-done.12) | copy-start | bytes 786436
  106.0 10.0 %collective-permute-start.14 = (bf16[64,2048]{1,0:T(8,128)(2,1)S(1)}, bf16[64,2048]{1,0:T(8,128)(2,1)}, u32[]{:S(2)}, u32[]{:S(2)}) collective-permute-start(bf16[64,2048]{1,0:T(8,128)(2,1)S(1)} %collective-permute-done.12), channel_id=1, source_target_pairs={{0,3},{1,0},{2,1},{3,2},{4,7},{5,4},{6,5},{7,6},{8,11},{9,8},{10,9... | collective-permute-start | bytes 786440 | tf_op jit(solution)/shard_map/ppermute | solution.py:287
  108.5 17.7 %collective-permute-start.11 = (bf16[64,2048]{1,0:T(8,128)(2,1)S(1)}, bf16[64,2048]{1,0:T(8,128)(2,1)}, u32[]{:S(2)}, u32[]{:S(2)}) collective-permute-start(bf16[64,2048]{1,0:T(8,128)(2,1)S(1)} %get-tuple-element.31), channel_id=1, source_target_pairs={{0,3},{1,0},{2,1},{3,2},{4,7},{5,4},{6,5},{7,6},{8,11},{9,8},{10,9... | collective-permute-start | bytes 786440 | tf_op jit(solution)/shard_map/ppermute | solution.py:287
  108.7 17.6 %collective-permute-start.10 = (bf16[64,2048]{1,0:T(8,128)(2,1)}, bf16[64,2048]{1,0:T(8,128)(2,1)}, u32[]{:S(2)}, u32[]{:S(2)}) collective-permute-start(bf16[64,2048]{1,0:T(8,128)(2,1)} %get-tuple-element.32), channel_id=1, source_target_pairs={{0,1},{1,2},{2,3},{3,0},{4,5},{5,6},{6,7},{7,4},{8,9},{9,10},{10,1... | collective-permute-start | bytes 786440 | tf_op jit(solution)/shard_map/ppermute | solution.py:287
  116.0 5.6 %copy-start.6 = (bf16[2048,2304]{1,0:T(8,128)(2,1)S(1)}, bf16[2048,2304]{1,0:T(8,128)(2,1)}, u32[]{:S(2)}) copy-start(bf16[2048,2304]{1,0:T(8,128)(2,1)} %all-gather.2.cloned.1.call-done) | copy-start | bytes 28311556
  121.7 4.6 %copy-start.9 = (bf16[64,2048]{1,0:T(8,128)(2,1)S(1)}, bf16[64,2048]{1,0:T(8,128)(2,1)}, u32[]{:S(2)}) copy-start(bf16[64,2048]{1,0:T(8,128)(2,1)} %copy-done.8) | copy-start | bytes 786436
  121.7 4.6 %copy-start.11 = (bf16[64,2048]{1,0:T(8,128)(2,1)S(1)}, bf16[64,2048]{1,0:T(8,128)(2,1)}, u32[]{:S(2)}) copy-start(bf16[64,2048]{1,0:T(8,128)(2,1)} %copy-done.10) | copy-start | bytes 786436
  122.9 10.5 %collective-permute-start.15 = (bf16[64,2048]{1,0:T(8,128)(2,1)S(1)}, bf16[64,2048]{1,0:T(8,128)(2,1)S(1)}, u32[]{:S(2)}, u32[]{:S(2)}) collective-permute-start(bf16[64,2048]{1,0:T(8,128)(2,1)S(1)} %get-tuple-element.27), channel_id=1, source_target_pairs={{0,1},{1,2},{2,3},{3,0},{4,5},{5,6},{6,7},{7,4},{8,9},{9,10},{10,1... | collective-permute-start | bytes 786440 | tf_op jit(solution)/shard_map/ppermute | solution.py:287
  123.3 10.1 %collective-permute-start.17 = (bf16[64,2048]{1,0:T(8,128)(2,1)S(1)}, bf16[64,2048]{1,0:T(8,128)(2,1)S(1)}, u32[]{:S(2)}, u32[]{:S(2)}) collective-permute-start(bf16[64,2048]{1,0:T(8,128)(2,1)S(1)} %get-tuple-element.28), channel_id=1, source_target_pairs={{0,3},{1,0},{2,1},{3,2},{4,7},{5,4},{6,5},{7,6},{8,11},{9,8},{10,9... | collective-permute-start | bytes 786440 | tf_op jit(solution)/shard_map/ppermute | solution.py:287
  133.6 10.5 %collective-permute-start.16 = (bf16[128,2048]{1,0:T(8,128)(2,1)S(1)}, bf16[128,2048]{1,0:T(8,128)(2,1)S(1)}, u32[]{:S(2)}, u32[]{:S(2)}) collective-permute-start(bf16[128,2048]{1,0:T(8,128)(2,1)S(1)} %get-tuple-element.21), channel_id=1, source_target_pairs={{0,1},{1,2},{2,3},{3,0},{4,5},{5,6},{6,7},{7,4},{8,9},{9,10},{10,1... | collective-permute-start | bytes 1572872 | tf_op jit(solution)/shard_map/ppermute | solution.py:287
  133.8 10.4 %collective-permute-start.18 = (bf16[128,2048]{1,0:T(8,128)(2,1)S(1)}, bf16[128,2048]{1,0:T(8,128)(2,1)S(1)}, u32[]{:S(2)}, u32[]{:S(2)}) collective-permute-start(bf16[128,2048]{1,0:T(8,128)(2,1)S(1)} %get-tuple-element.22), channel_id=1, source_target_pairs={{0,3},{1,0},{2,1},{3,2},{4,7},{5,4},{6,5},{7,6},{8,11},{9,8},{10,9... | collective-permute-start | bytes 1572872 | tf_op jit(solution)/shard_map/ppermute | solution.py:287
  (2 other events, 1.4 us)
Sparse Core Ops, SparseCore 0:
  11.1 92.8 all-gather.1
